TPU v7x, 512 devices: a whole 4x8x8 slice. The times are simulated.
512 devices in a mesh: sp: 128 (over z, y, core), tp: 4 (over x).
Axes of the slice: x: 4, y: 8, z: 8, core: 2. Of those that a mesh axis runs over, the one named last changes fastest.
Arguments:
- tokens: bfloat16 [32768, 4096], P('sp'), may hold values from -6 to 6
- norm_gain: float32 [4096], replicated, may hold values from 0.1 to 1.9
- w_query: bfloat16 [4096, 512], P('sp', 'tp'), may hold values from -0.09375 to 0.09375
- w_key: bfloat16 [4096, 512], P('sp', 'tp'), may hold values from -0.09375 to 0.09375
- w_value: bfloat16 [4096, 1024], P('sp', 'tp'), may hold values from -0.09375 to 0.09375
- w_gates: bfloat16 [4096, 2, 2, 4], P(None, None, None, 'tp'), may hold values from -0.09375 to 0.09375
- input_bias: float32 [2, 4], P(None, 'tp'), may hold values from -2 to 90
- forget_bias: float32 [2, 4], P(None, 'tp'), as said below
- decay_shift: float32 [2, 32768, 4], P(None, 'sp', 'tp'), may hold values from -2.5 to 0
- head_gain: float32 [1024], P('tp'), may hold values from 0.1 to 1.9
- w_conv_b: bfloat16 [4096, 1024], P('sp', 'tp'), may hold values from -0.09375 to 0.09375
- w_conv_c: bfloat16 [4096, 1024], P('sp', 'tp'), may hold values from -0.09375 to 0.09375
- w_conv_in: bfloat16 [4096, 1024], P('sp', 'tp'), may hold values from -0.09375 to 0.09375
- conv_taps: bfloat16 [3, 1024], P(None, 'tp'), may hold values from -3.5 to 3.5
- w_out: bfloat16 [2048, 4096], P('sp', 'tp'), may hold values from -0.125 to 0.125
Outputs:
- mixed_out: bfloat16 [32768, 4096], P('sp', 'tp')
Inputs may be any that keep to these rules, and one draw needn't show every extreme that they name: `forget_bias`: at most the natural logarithm of 32768 plus 2.
All inputs are finite; a program needn't handle non-finite values.
Results may differ from a plain program's by a relative error of at most 0.02.
Values may be sent and summed in bfloat16 or wider, within the bound.
No kernel may reach another device: no remote copies, remote signals or barrier semaphores. Data moves between devices by JAX's collectives and lax.ppermute only.
A program may use at most 128 MiB of HBM per device.

v0:
```python
import jax
import jax.numpy as jnp
from jax import lax
from jax.experimental import pallas as pl
from jax.experimental.pallas import tpu as pltpu
from jax.sharding import Mesh
from jax.sharding import PartitionSpec as P


DQK = 128
DV = 256
SP = ("sp_0", "sp_1", "sp_2")
PLANE = ("sp_1", "sp_2")
EPS = 1e-06
LOWEST = -1e30
F32 = jnp.float32
BF16 = jnp.bfloat16


def row_norm(tokens, norm_gain):
    values = tokens.astype(F32)
    inverse_rms = lax.rsqrt(jnp.mean(values * values, axis=-1, keepdims=True) + EPS)
    return (values * inverse_rms * norm_gain).astype(BF16)


def swapped(value, axes):
    return lax.all_to_all(value, axes, split_axis=0, concat_axis=0, tiled=True)


def neighbour_rows(last, initial):
    size = lax.axis_size(SP)
    up = [(i, i + 1) for i in range(size - 1)]
    before = lax.ppermute(last, SP, up)
    after = lax.ppermute(initial, SP, [(j, i) for i, j in up])
    return before, after


ROWS = 48
NORMERS = 32
NUMBERS = (34, 40)


def in_terms(number):
    high = number.astype(BF16)
    rest = number - high.astype(F32)
    middle = rest.astype(BF16)
    low = (rest - middle.astype(F32)).astype(BF16)
    return [high, middle, low]


def from_terms(block, row):
    return block[row : row + 1] + block[row + 1 : row + 2] + block[row + 2 : row + 3]


def numbered_rows(normers, numbers):
    rows = [n.astype(BF16) for n in normers]
    for pair in numbers:
        for number in pair:
            rows += in_terms(number)
    rows.append(jnp.zeros((ROWS - NORMERS - len(rows), 128), BF16))
    return jnp.concatenate(rows, axis=0)


ARRIVAL = (0, -1, 1, -2, 2, -3, 3, -4)
GROUPS = (3, 4, 1)


def pack_kernel(query_ref, key_ref, value_ref, outer_ref, inner_ref, given_ref, out_ref, whole_ref, block_ref):
    at = 0
    for ref in (query_ref, inner_ref, given_ref, outer_ref):
        whole_ref[:, at : at + ref.shape[1]] = ref[...]
        at += ref.shape[1]
    depth, columns = out_ref.shape
    for side in range(2):
        whole_ref[side * depth : (side + 1) * depth, at:] = out_ref[
            :, side * columns // 2 : (side + 1) * columns // 2
        ]
    for z in range(block_ref.shape[0]):
        block_ref[z, :, :DQK] = key_ref[...]
        block_ref[z, :, DQK:] = value_ref[...]


def gate_kernel(forget_ref, gate_ref, row_ref, column_ref, number_ref):
    length = forget_ref.shape[1]
    at = lax.broadcasted_iota(jnp.int32, (1, length), 1)
    running, update, numbers = [], [], []
    for d in range(2):
        value = forget_ref[d : d + 1]
        step = 1
        while step < length:
            moved = pltpu.roll(value, length - step if d else step, 1)
            inside = (at < length - step) if d else (at >= step)
            value = value + jnp.where(inside, moved, 0.0)
            step *= 2
        total = value[:, :1] if d else value[:, length - 1 :]
        log_update = total - value + gate_ref[d : d + 1]
        most = jnp.max(log_update, axis=1, keepdims=True)
        running.append(value)
        update.append(jnp.exp(log_update - most))
        numbers += [total, most]
    row_ref[...] = jnp.concatenate([*running, gate_ref[...]], axis=0)
    column_ref[...] = jnp.concatenate([*update, *running, *update, *running], axis=0).T
    for n, number in enumerate(numbers):
        number_ref[n : n + 1] = jnp.broadcast_to(number, (1, 128))


def state_kernel(place_ref, normed_ref, update_ref, number_ref, *refs):
    groups = len(GROUPS)
    state_ref, key_ref, value_ref, weight_ref = refs[2 * groups :]
    core, row = place_ref[0], place_ref[1]
    for side in range(2):
        cell = 1 - core if side else core
        arrivals = iter(ARRIVAL)
        for group_ref in refs[side * groups : (side + 1) * groups]:
            _, planes, depth, _ = group_ref.shape
            for k in range(group_ref.shape[0]):
                y = (row + next(arrivals) + 8) % 8
                for z in range(planes):
                    start = ((z * 8 + y) * 2 + cell) * depth
                    weight_ref[pl.ds(pl.multiple_of(start, depth), depth), :] = group_ref[k, z]
    both = jnp.dot(normed_ref[...], weight_ref[...], preferred_element_type=F32)
    both = both.astype(BF16)
    keys, values = both[:, :DQK], both[:, DQK:]
    key_ref[...] = keys
    value_ref[...] = values
    members = state_ref.shape[0]
    share = DV // members
    normers = []
    for d in range(2):
        weighted = keys.astype(F32) * update_ref[:, d : d + 1]
        normers.append(jnp.sum(weighted, axis=0, keepdims=True))
        memory = lax.dot_general(
            values, weighted.astype(BF16), (((0,), (0,)), ((), ())), preferred_element_type=F32
        )
        state_ref[:, d * share : (d + 1) * share, :] = memory.astype(BF16).reshape(
            members, share, DQK
        )
    numbers = [[number_ref[2 * d + n : 2 * d + n + 1] for n in range(2)] for d in range(2)]
    rows = numbered_rows(normers, numbers)
    for j in range(members):
        state_ref[j, NORMERS:, :] = rows


def passed(carry, block, d):
    memory, normer, total, most = carry
    block_total = from_terms(block, NUMBERS[d])
    block_most = from_terms(block, NUMBERS[d] + 3)
    new = jnp.maximum(most + block_total, block_most)
    old_weight = jnp.exp(most + block_total - new)
    block_weight = jnp.exp(block_most - new)
    share = memory.shape[0]
    memory = old_weight * memory + block_weight * block[d * share : (d + 1) * share]
    normer = old_weight * normer + block_weight * block[NORMERS + d : NORMERS + d + 1]
    return memory, normer, total + block_total, new


def nothing(share):
    row = jnp.zeros((1, 128), F32)
    return jnp.zeros((share, 128), F32), row, row, jnp.full((1, 128), LOWEST, F32)


def plane_kernel(state_ref, near_ref, plane_ref):
    members = state_ref.shape[0]
    share = NORMERS // 2
    ends = []
    for d in range(2):
        carry = nothing(share)
        for i in reversed(range(members)) if d else range(members):
            near_ref[i, d * share : (d + 1) * share, :] = carry[0]
            for n in range(3):
                near_ref[i, NORMERS + 2 * n + d : NORMERS + 2 * n + d + 1, :] = carry[1 + n]
            carry = passed(carry, state_ref[i].astype(F32), d)
        ends.append(carry)
    rows = numbered_rows([e[1] for e in ends], [e[2:] for e in ends])
    for z in range(plane_ref.shape[0]):
        for d in range(2):
            plane_ref[z, d * share : (d + 1) * share, :] = ends[d][0].astype(BF16)
        plane_ref[z, NORMERS:, :] = rows


def far_kernel(place_ref, near_ref, planes_ref, start_ref):
    planes, members = planes_ref.shape[0], near_ref.shape[0]
    share = NORMERS // 2
    place = place_ref[0]
    far = []
    for d in range(2):
        carry = nothing(share)
        for z in reversed(range(planes)) if d else range(planes):
            earlier = (z > place) if d else (z < place)
            after = passed(carry, planes_ref[z].astype(F32), d)
            carry = tuple(jnp.where(earlier, a, c) for a, c in zip(after, carry))
        far.append(carry)
    for i in range(members):
        normers, numbers = [], []
        for d in range(2):
            memory, normer, _, most = far[d]
            at = [NORMERS + 2 * n + d for n in range(3)]
            near_normer, head, near_most = (near_ref[i, r : r + 1, :] for r in at)
            moved = most + head
            new = jnp.maximum(moved, near_most)
            far_weight = jnp.exp(moved - new)
            near_weight = jnp.exp(near_most - new)
            near = near_ref[i, d * share : (d + 1) * share, :]
            start_ref[i, d * share : (d + 1) * share, :] = (
                near_weight * near + far_weight * memory
            ).astype(BF16)
            normers.append(near_weight * near_normer + far_weight * normer)
            numbers.append([new])
        rows = [n.astype(BF16) for n in normers]
        for (number,) in numbers:
            rows += in_terms(number)
        rows.append(jnp.zeros((ROWS - NORMERS - len(rows), 128), BF16))
        start_ref[i, NORMERS:, :] = jnp.concatenate(rows, axis=0)


def read_kernel(query_ref, key_ref, value_ref, column_ref, row_ref, gain_ref, start_ref, out_ref):
    length = query_ref.shape[0]
    queries = query_ref[...]
    values = value_ref[...]
    scale = DQK ** (-0.5)
    products = scale * lax.dot_general(
        queries, key_ref[...], (((1,), (1,)), ((), ())), preferred_element_type=F32
    )
    t = lax.broadcasted_iota(jnp.int32, (length, length), 0)
    s = lax.broadcasted_iota(jnp.int32, (length, length), 1)
    share = NORMERS // 2
    last = start_ref[0, NORMERS:, :].astype(F32)
    summed = None
    for d in range(2):
        memory = start_ref[:, d * share : (d + 1) * share, :].reshape(DV, DQK)
        normer = last[d : d + 1]
        stable = from_terms(last, 2 + 3 * d)[:, :1]
        running = column_ref[:, 2 + d : 3 + d]
        seen = (t <= s) if d else (t >= s)
        log_weight = jnp.where(
            seen, running - row_ref[d : d + 1, :] + row_ref[2 + d : 3 + d, :], -jnp.inf
        )
        carried = running + stable
        highest = jnp.maximum(carried, jnp.max(log_weight, axis=-1, keepdims=True))
        scores = products * jnp.exp(log_weight - highest)
        carry_weight = scale * jnp.exp(carried - highest)
        numerator = jnp.dot(scores.astype(BF16), values, preferred_element_type=F32)
        numerator += carry_weight * lax.dot_general(
            queries, memory, (((1,), (1,)), ((), ())), preferred_element_type=F32
        )
        denominator = jnp.sum(scores, axis=-1, keepdims=True)
        denominator += carry_weight * jnp.sum(
            queries.astype(F32) * normer, axis=-1, keepdims=True
        )
        result = numerator / jnp.maximum(jnp.abs(denominator), jnp.exp(-highest))
        summed = result if summed is None else summed + result
    inverse_rms = lax.rsqrt(jnp.mean(summed * summed, axis=-1, keepdims=True) + EPS)
    out = (summed * inverse_rms * gain_ref[...]).astype(BF16)
    for k in range(out_ref.shape[0]):
        out_ref[k] = out


WIDE = DQK + 3 * DV
CHUNKS = 8


def project_kernel(
    normed_ref, edge_ref, tap_ref, whole_ref, query_ref, conv_ref, weight_ref, total_ref, sems
):
    depth = weight_ref.shape[1]
    length = query_ref.shape[0]

    def fetch(k):
        return pltpu.make_async_copy(
            whole_ref.at[pl.ds(k * depth, depth), pl.ds(0, WIDE)], weight_ref.at[k], sems.at[k]
        )

    for k in range(CHUNKS):
        fetch(k).start()
    for k in range(CHUNKS):
        fetch(k).wait()
        at = slice(k * depth, (k + 1) * depth)
        rows = jnp.concatenate([normed_ref[:, at], edge_ref[:, at]], axis=0)
        product = jnp.dot(rows, weight_ref[k], preferred_element_type=F32)
        if k:
            total_ref[...] += product
        else:
            total_ref[...] = product
    query_ref[...] = total_ref[:length, :DQK].astype(BF16)
    inner = total_ref[:, DQK : DQK + DV].astype(BF16).astype(F32)
    given = total_ref[:, DQK + DV : DQK + 2 * DV].astype(BF16).astype(F32)
    outer = total_ref[:length, DQK + 2 * DV :].astype(BF16).astype(F32)
    mixed = (inner * given).astype(BF16).astype(F32)
    here = mixed[:length]
    at = lax.broadcasted_iota(jnp.int32, (length, DV), 0)
    before = jnp.where(at == 0, mixed[length : length + 1], pltpu.roll(here, 1, 0))
    after = jnp.where(
        at == length - 1, mixed[length + 1 : length + 2], pltpu.roll(here, length - 1, 0)
    )
    taps = tap_ref[...].astype(F32)
    filtered = taps[0:1] * before + taps[1:2] * here + taps[2:3] * after
    conv_ref[...] = (outer * filtered).astype(BF16)


def output_kernel(place_ref, lstm_ref, *refs):
    parts, (whole_ref, out_ref, weight_ref, sems) = refs[:4], refs[4:]
    place = place_ref[0]
    sources = [(k * 32, lstm_ref.at[k]) for k in range(4)]
    for part_ref, offset in zip(parts, (0, -1, 1, 2)):
        sources.append(((place + offset + 4) % 4 * 32 + 16, part_ref))

    def fetch(n, side):
        return pltpu.make_async_copy(
            whole_ref.at[pl.ds(sources[n][0], 16), side, :, pl.ds(WIDE, 512)],
            weight_ref.at[n, side],
            sems.at[n, side],
        )

    for side in range(2):
        for n in range(8):
            fetch(n, side).start()
    for side in range(2):
        total = None
        for n in range(8):
            fetch(n, side).wait()
            weight = weight_ref[n, side].reshape(DV, 512)
            product = jnp.dot(sources[n][1][...], weight, preferred_element_type=F32)
            total = product if total is None else total + product
        out_ref[:, side * 512 : (side + 1) * 512] = total.astype(BF16)


def ring(size, step):
    return [(i, (i + step) % size) for i in range(size)]


def on_core(kernel, out, *operands, scalars=0, remote=0, scratch=(), limit=20):
    vmem = pl.BlockSpec(memory_space=pltpu.VMEM)
    smem = pl.BlockSpec(memory_space=pltpu.SMEM)
    return pl.pallas_call(
        kernel,
        out_shape=out,
        in_specs=[smem] * scalars
        + [vmem] * (len(operands) - scalars - remote)
        + [pl.BlockSpec(memory_space=pltpu.HBM)] * remote,
        out_specs=jax.tree.map(lambda _: vmem, out),
        scratch_shapes=scratch,
        compiler_params=pltpu.CompilerParams(vmem_limit_bytes=limit * 2**20),
    )(*operands)


def body(
    tokens,
    norm_gain,
    w_query,
    w_key,
    w_value,
    w_gates,
    input_bias,
    forget_bias,
    decay_shift,
    head_gain,
    w_conv_b,
    w_conv_c,
    w_conv_in,
    conv_taps,
    w_out,
):
    length = tokens.shape[0]
    size = lax.axis_size(SP)
    planes = lax.axis_size("sp_0")
    members = size // planes
    plane = lax.axis_index("sp_0")
    depth = w_out.shape[0]
    half = w_out.shape[1] // 2
    packed, block = on_core(
        pack_kernel,
        (
            jax.ShapeDtypeStruct((w_key.shape[0], WIDE + half), BF16),
            jax.ShapeDtypeStruct((planes, w_key.shape[0], DQK + DV), BF16),
        ),
        w_query,
        w_key,
        w_value,
        w_conv_b,
        w_conv_c,
        w_conv_in,
        w_out,
    )
    block = swapped(block, "sp_0")
    whole = lax.all_gather(packed, SP, axis=0, tiled=True)
    core = lax.axis_index("sp_2")
    row = lax.axis_index("sp_1")
    normed = row_norm(tokens, norm_gain)

    block, normed = lax.optimization_barrier((block, normed))
    up = down = block
    pieces = [block]
    for k in range(4):
        up = lax.ppermute(up, "sp_1", ring(8, 1))
        pieces.append(up)
        if k < 3:
            down = lax.ppermute(down, "sp_1", ring(8, -1))
            pieces.append(down)
    groups, at = [], 0
    for count in GROUPS:
        groups.append(jnp.stack(pieces[at : at + count]))
        at += count
    for count, group in zip(GROUPS, tuple(groups)):
        groups.append(lax.ppermute(group, "sp_2", ring(2, 1)))

    gates = lax.dot_general(
        w_gates.reshape(-1, 4), normed, (((0,), (1,)), ((), ())), preferred_element_type=F32
    ).reshape(2, 2, length)
    in_gate = gates[:, 0] + input_bias
    log_forget = jax.nn.log_sigmoid(gates[:, 1] + forget_bias) + decay_shift[:, :, 0]
    rows, columns, numbers = on_core(
        gate_kernel,
        (
            jax.ShapeDtypeStruct((4, length), F32),
            jax.ShapeDtypeStruct((length, 8), F32),
            jax.ShapeDtypeStruct((4, 128), F32),
        ),
        log_forget,
        in_gate,
    )
    block = jax.ShapeDtypeStruct((members, ROWS, 128), BF16)
    state, keys, values = on_core(
        state_kernel,
        (
            block,
            jax.ShapeDtypeStruct((length, DQK), BF16),
            jax.ShapeDtypeStruct((length, DV), BF16),
        ),
        jnp.stack([core, row]),
        normed,
        columns,
        numbers,
        *groups,
        scalars=1,
        scratch=[pltpu.VMEM((normed.shape[1], DQK + DV), BF16)],
    )
    last, initial, keys = lax.optimization_barrier((normed[-1:], normed[:1], keys))
    state = swapped(state, PLANE)
    before, after = neighbour_rows(last, initial)
    edges = jnp.concatenate([before, after, jnp.zeros((14, normed.shape[1]), BF16)], axis=0)
    near, plane_state = on_core(
        plane_kernel,
        (
            jax.ShapeDtypeStruct((members, ROWS, 128), F32),
            jax.ShapeDtypeStruct((planes, ROWS, 128), BF16),
        ),
        state,
    )
    far = swapped(plane_state, "sp_0")
    queries, conv_out = on_core(
        project_kernel,
        (
            jax.ShapeDtypeStruct((length, DQK), BF16),
            jax.ShapeDtypeStruct((length, DV), BF16),
        ),
        normed,
        edges,
        conv_taps,
        whole,
        remote=1,
        scratch=[
            pltpu.VMEM((CHUNKS, whole.shape[0] // CHUNKS, WIDE), BF16),
            pltpu.VMEM((length + edges.shape[0], WIDE), F32),
            pltpu.SemaphoreType.DMA((CHUNKS,)),
        ],
        limit=54,
    )
    far, queries, conv_out = lax.optimization_barrier((far, queries, conv_out))
    start = on_core(far_kernel, block, plane[None], near, far, scalars=1)
    start = swapped(start, PLANE)
    parts = [conv_out] + [lax.ppermute(conv_out, "tp", ring(4, n)) for n in (1, -1, 2)]
    start, *parts = lax.optimization_barrier((start, *parts))
    lstm_out = on_core(
        read_kernel,
        jax.ShapeDtypeStruct((4, length, DV), BF16),
        queries,
        keys,
        values,
        columns,
        rows,
        head_gain[None],
        start,
    )
    lstm_all = swapped(lstm_out, "tp")
    whole = whole.reshape(size, 2, depth, -1)
    return on_core(
        output_kernel,
        jax.ShapeDtypeStruct((length, 2 * half), BF16),
        lax.axis_index("tp")[None],
        lstm_all,
        *parts,
        whole,
        scalars=1,
        remote=1,
        scratch=[
            pltpu.VMEM((8, 2, 16, depth, half), BF16),
            pltpu.SemaphoreType.DMA((8, 2)),
        ],
        limit=58,
    )


def solution(mesh):
    torus = Mesh(mesh.devices.reshape(8, 8, 2, mesh.shape["tp"]), (*SP, "tp"))
    placed = (
        P(SP, None),
        P(),
        P(SP, "tp"),
        P(SP, "tp"),
        P(SP, "tp"),
        P(None, None, None, "tp"),
        P(None, "tp"),
        P(None, "tp"),
        P(None, SP, "tp"),
        P("tp"),
        P(SP, "tp"),
        P(SP, "tp"),
        P(SP, "tp"),
        P(None, "tp"),
        P(SP, "tp"),
    )

    return jax.shard_map(body, mesh=torus, in_specs=placed, out_specs=P(SP, "tp"), check_vma=False)
```

profile of v0, /device:TPU:1, one launch (start us, length us, event | category | flops | bytes accessed | tf_op | source)
XLA Modules:
  0.0 173.0 jit_solution(11204338890925511283)
XLA Ops:
  12.3 10.9 %all-to-all-start = ((bf16[8,32,384]{2,1,0:T(8,128)(2,1)}), bf16[8,32,384]{2,1,0:T(8,128)(2,1)S(1)}, u32[]{:S(2)}, u32[]{:S(2)}) async-start(bf16[8,32,384]{2,1,0:T(8,128)(2,1)} %get-tuple-element.30), calls=%async_computation | async-start | bytes 393216 | tf_op jit(solution)/shard_map/all_to_all | solution.py:27
  26.1 6.1 %all-to-all-done = bf16[8,32,384]{2,1,0:T(8,128)(2,1)S(1)} async-done(((bf16[8,32,384]{2,1,0:T(8,128)(2,1)}), bf16[8,32,384]{2,1,0:T(8,128)(2,1)S(1)}, u32[]{:S(2)}, u32[]{:S(2)}) %all-to-all-start) | async-done | bytes 196640 | tf_op jit(solution)/shard_map/all_to_all | solution.py:27
  32.2 3.2 %collective-permute-start = (bf16[8,32,384]{2,1,0:T(8,128)(2,1)S(1)}, bf16[8,32,384]{2,1,0:T(8,128)(2,1)}, u32[]{:S(2)}, u32[]{:S(2)}) collective-permute-start(bf16[8,32,384]{2,1,0:T(8,128)(2,1)S(1)} %all-to-all-done), channel_id=1, source_target_pairs={{0,8},{8,16},{16,24},{24,32},{32,40},{40,48},{48,56},{56,0},{1,9},... | collective-permute-start | bytes 589832 | tf_op jit(solution)/shard_map/ppermute | solution.py:394
  35.4 3.8 %collective-permute-start.1 = (bf16[8,32,384]{2,1,0:T(8,128)(2,1)S(1)}, bf16[8,32,384]{2,1,0:T(8,128)(2,1)}, u32[]{:S(2)}, u32[]{:S(2)}) collective-permute-start(bf16[8,32,384]{2,1,0:T(8,128)(2,1)S(1)} %all-to-all-done), channel_id=1, source_target_pairs={{0,56},{8,0},{16,8},{24,16},{32,24},{40,32},{48,40},{56,48},{1,57}... | collective-permute-start | bytes 589832 | tf_op jit(solution)/shard_map/ppermute | solution.py:397
  42.4 5.0 %collective-permute-start.3 = (bf16[8,32,384]{2,1,0:T(8,128)(2,1)}, bf16[8,32,384]{2,1,0:T(8,128)(2,1)S(1)}, u32[]{:S(2)}, u32[]{:S(2)}) collective-permute-start(bf16[8,32,384]{2,1,0:T(8,128)(2,1)} %collective-permute-done.1), channel_id=1, source_target_pairs={{0,56},{8,0},{16,8},{24,16},{32,24},{40,32},{48,40},{56,48},{1,57}... | collective-permute-start | bytes 589832 | tf_op jit(solution)/shard_map/ppermute | solution.py:397
  50.9 4.9 %collective-permute-start.5 = (bf16[8,32,384]{2,1,0:T(8,128)(2,1)S(1)}, bf16[8,32,384]{2,1,0:T(8,128)(2,1)S(1)}, u32[]{:S(2)}, u32[]{:S(2)}) collective-permute-start(bf16[8,32,384]{2,1,0:T(8,128)(2,1)S(1)} %collective-permute-done.3), channel_id=1, source_target_pairs={{0,56},{8,0},{16,8},{24,16},{32,24},{40,32},{48,40},{56,48},{1,57}... | collective-permute-start | bytes 589832 | tf_op jit(solution)/shard_map/ppermute | solution.py:397
  60.2 7.3 %collective-permute-start.8 = (bf16[4,8,32,384]{3,2,1,0:T(8,128)(2,1)S(1)}, bf16[4,8,32,384]{3,2,1,0:T(8,128)(2,1)}, u32[]{:S(2)}, u32[]{:S(2)}) collective-permute-start(bf16[4,8,32,384]{3,2,1,0:T(8,128)(2,1)S(1)} %pad_maximum_fusion.refs_1_), channel_id=1, source_target_pairs={{0,4},{4,0},{1,5},{5,1},{2,6},{6,2},{3,7},{7,3},{8,12},{12,8},{9,1... | collective-permute-start | bytes 2359304 | tf_op jit(solution)/shard_map/ppermute | solution.py:404
  71.4 3.1 %collective-permute-start.6 = (bf16[8,32,384]{2,1,0:T(8,128)(2,1)}, bf16[8,32,384]{2,1,0:T(8,128)(2,1)S(1)}, u32[]{:S(2)}, u32[]{:S(2)}) collective-permute-start(bf16[8,32,384]{2,1,0:T(8,128)(2,1)} %copy-done.18), channel_id=1, source_target_pairs={{0,8},{8,16},{16,24},{24,32},{32,40},{40,48},{48,56},{56,0},{1,9},... | collective-permute-start | bytes 589832 | tf_op jit(solution)/shard_map/ppermute | solution.py:394
  74.5 11.2 %collective-permute-done.6 = bf16[8,32,384]{2,1,0:T(8,128)(2,1)S(1)} collective-permute-done((bf16[8,32,384]{2,1,0:T(8,128)(2,1)}, bf16[8,32,384]{2,1,0:T(8,128)(2,1)S(1)}, u32[]{:S(2)}, u32[]{:S(2)}) %collective-permute-start.6) | collective-permute-done | bytes 196640 | tf_op jit(solution)/shard_map/ppermute | solution.py:394
  85.7 2.7 %collective-permute-start.9 = (bf16[1,8,32,384]{3,2,1,0:T(8,128)(2,1)S(1)}, bf16[1,8,32,384]{3,2,1,0:T(8,128)(2,1)S(1)}, u32[]{:S(2)}, u32[]{:S(2)}) collective-permute-start(bf16[1,8,32,384]{3,2,1,0:T(8,128)(2,1)S(1)} %bitcast.36), channel_id=1, source_target_pairs={{0,4},{4,0},{1,5},{5,1},{2,6},{6,2},{3,7},{7,3},{8,12},{12,8},{9,1... | collective-permute-start | bytes 589832 | tf_op jit(solution)/shard_map/ppermute | solution.py:404
  89.5 3.2 %shard_map.147 = (bf16[16,48,128]{2,1,0:T(8,128)(2,1)S(1)}, bf16[256,128]{1,0:T(8,128)(2,1)S(1)}, bf16[256,256]{1,0:T(8,128)(2,1)S(1)}) custom-call(s32[2]{0:T(128)S(1)} %pad_add_fusion.place_ref, bf16[256,4096]{1,0:T(8,128)(2,1)S(1)} %fusion.2.normed_ref, f32[256,8]{1,0:T(8,128)S(1)} %get-tuple-element.32.update_ref.column_ref, ...), custom_call_target="tpu_custom_call" | custom-call | tf_op jit(solution)/shard_map/pallas_call | solution.py:334
  94.1 6.7 %all-to-all-start.1 = ((bf16[16,48,128]{2,1,0:T(8,128)(2,1)}), bf16[16,48,128]{2,1,0:T(8,128)(2,1)S(1)}, u32[]{:S(2)}, u32[]{:S(2)}) async-start(bf16[16,48,128]{2,1,0:T(8,128)(2,1)} %copy-done.3), calls=%async_computation.1 | async-start | bytes 393216 | tf_op jit(solution)/shard_map/all_to_all | solution.py:27
  100.9 3.5 %collective-permute-start.10 = (bf16[1,4096]{1,0:T(2,128)(2,1)S(1)}, bf16[1,4096]{1,0:T(2,128)(2,1)S(1)}, u32[]{:S(2)}, u32[]{:S(2)}) collective-permute-start(bf16[1,4096]{1,0:T(2,128)(2,1)S(1)} %get-tuple-element.38), channel_id=1, source_target_pairs={{0,4},{4,8},{8,12},{12,16},{16,20},{20,24},{24,28},{28,32},{32,36}... | collective-permute-start | bytes 24584 | tf_op jit(solution)/shard_map/ppermute | solution.py:33
  106.4 6.7 %all-to-all-done.1.state_ref = bf16[16,48,128]{2,1,0:T(8,128)(2,1)S(1)} async-done(((bf16[16,48,128]{2,1,0:T(8,128)(2,1)}), bf16[16,48,128]{2,1,0:T(8,128)(2,1)S(1)}, u32[]{:S(2)}, u32[]{:S(2)}) %all-to-all-start.1) | async-done | bytes 196640 | tf_op jit(solution)/shard_map/all_to_all | solution.py:27
  113.9 4.5 %all-to-all-start.2 = ((bf16[8,48,128]{2,1,0:T(8,128)(2,1)}), bf16[8,48,128]{2,1,0:T(8,128)(2,1)S(1)}, u32[]{:S(2)}, u32[]{:S(2)}) async-start(bf16[8,48,128]{2,1,0:T(8,128)(2,1)} %get-tuple-element.36), calls=%async_computation.2 | async-start | bytes 196608 | tf_op jit(solution)/shard_map/all_to_all | solution.py:27
  119.2 7.2 %shard_map.149 = (bf16[256,128]{1,0:T(8,128)(2,1)}, bf16[256,256]{1,0:T(8,128)(2,1)}) custom-call(bf16[256,4096]{1,0:T(8,128)(2,1)} %copy-done, bf16[16,4096]{1,0:T(8,128)(2,1)} %maximum_maximum_fusion.edge_ref, bf16[3,256]{1,0:T(4,128)(2,1)} %tap_ref.1, bf16[4096,1408]{1,0:T(8,128)(2,1)} %all-gather.2.cloned.1.call-done.whole_ref), custom_call_target="tpu_custom_call" | custom-call | tf_op jit(solution)/shard_map/pallas_call | solution.py:334
  127.4 4.7 %all-to-all-start.3 = ((bf16[16,48,128]{2,1,0:T(8,128)(2,1)}), bf16[16,48,128]{2,1,0:T(8,128)(2,1)S(1)}, u32[]{:S(2)}, u32[]{:S(2)}) async-start(bf16[16,48,128]{2,1,0:T(8,128)(2,1)} %shard_map.150), calls=%async_computation.3 | async-start | bytes 393216 | tf_op jit(solution)/shard_map/all_to_all | solution.py:27
  132.0 3.0 %collective-permute-start.12 = (bf16[256,256]{1,0:T(8,128)(2,1)}, bf16[256,256]{1,0:T(8,128)(2,1)S(1)}, u32[]{:S(2)}, u32[]{:S(2)}) collective-permute-start(bf16[256,256]{1,0:T(8,128)(2,1)} %get-tuple-element.51.refs_0_), channel_id=1, source_target_pairs={{0,1},{1,2},{2,3},{3,0},{4,5},{5,6},{6,7},{7,4},{8,9},{9,10},{10,1... | collective-permute-start | bytes 393224 | tf_op jit(solution)/shard_map/ppermute | solution.py:471
  135.1 3.4 %collective-permute-start.13 = (bf16[256,256]{1,0:T(8,128)(2,1)}, bf16[256,256]{1,0:T(8,128)(2,1)S(1)}, u32[]{:S(2)}, u32[]{:S(2)}) collective-permute-start(bf16[256,256]{1,0:T(8,128)(2,1)} %get-tuple-element.51.refs_0_), channel_id=1, source_target_pairs={{0,3},{1,0},{2,1},{3,2},{4,7},{5,4},{6,5},{7,6},{8,11},{9,8},{10,9... | collective-permute-start | bytes 393224 | tf_op jit(solution)/shard_map/ppermute | solution.py:471
  138.5 3.3 %collective-permute-start.14 = (bf16[256,256]{1,0:T(8,128)(2,1)}, bf16[256,256]{1,0:T(8,128)(2,1)S(1)}, u32[]{:S(2)}, u32[]{:S(2)}) collective-permute-start(bf16[256,256]{1,0:T(8,128)(2,1)} %get-tuple-element.51.refs_0_), channel_id=1, source_target_pairs={{0,2},{1,3},{2,0},{3,1},{4,6},{5,7},{6,4},{7,5},{8,10},{9,11},{10,... | collective-permute-start | bytes 393224 | tf_op jit(solution)/shard_map/ppermute | solution.py:471
  141.9 4.5 %collective-permute-done.14.refs_3_ = bf16[256,256]{1,0:T(8,128)(2,1)S(1)} collective-permute-done((bf16[256,256]{1,0:T(8,128)(2,1)}, bf16[256,256]{1,0:T(8,128)(2,1)S(1)}, u32[]{:S(2)}, u32[]{:S(2)}) %collective-permute-start.14) | collective-permute-done | bytes 131104 | tf_op jit(solution)/shard_map/ppermute | solution.py:471
  149.0 3.5 %all-to-all-start.4 = ((bf16[4,256,256]{2,1,0:T(8,128)(2,1)}), bf16[4,256,256]{2,1,0:T(8,128)(2,1)S(1)}, u32[]{:S(2)}, u32[]{:S(2)}) async-start(bf16[4,256,256]{2,1,0:T(8,128)(2,1)} %shard_map.151), calls=%async_computation.4 | async-start | bytes 1048576 | tf_op jit(solution)/shard_map/all_to_all | solution.py:27
  152.5 7.6 %all-to-all-done.4.lstm_ref = bf16[4,256,256]{2,1,0:T(8,128)(2,1)S(1)} async-done(((bf16[4,256,256]{2,1,0:T(8,128)(2,1)}), bf16[4,256,256]{2,1,0:T(8,128)(2,1)S(1)}, u32[]{:S(2)}, u32[]{:S(2)}) %all-to-all-start.4) | async-done | bytes 524320 | tf_op jit(solution)/shard_map/all_to_all | solution.py:27
  160.9 5.2 %shard_map.152 = bf16[256,1024]{1,0:T(8,128)(2,1)} custom-call(s32[1]{0:T(128)} %bitcast.place_ref, bf16[4,256,256]{2,1,0:T(8,128)(2,1)} %copy-done.16, bf16[256,256]{1,0:T(8,128)(2,1)} %get-tuple-element.51.refs_0_, bf16[256,256]{1,0:T(8,128)(2,1)} %copy-done.21, bf16[256,256]{1,0:T(8,128)(2,1)} %copy-done.22, bf16[256,256]{1,0:T(8,128)(2,1)} %copy-done.23, ...), custom_call_target="tpu_custom_call" | custom-call | tf_op jit(solution)/shard_map/pallas_call | solution.py:334
  (100 shorter events, 33.8 us)
Async XLA Ops:
  6.5 112.7 %all-gather.2.cloned.1.call-start = ((), (), s32[]{:S(2)}) async-start(), calls=%async_computation.5 | async-start | bytes 11624448 | tf_op jit(solution)/shard_map/all_gather | solution.py:385
  12.3 19.9 %all-to-all-start = ((bf16[8,32,384]{2,1,0:T(8,128)(2,1)}), bf16[8,32,384]{2,1,0:T(8,128)(2,1)S(1)}, u32[]{:S(2)}, u32[]{:S(2)}) async-start(bf16[8,32,384]{2,1,0:T(8,128)(2,1)} %get-tuple-element.30), calls=%async_computation | async-start | bytes 393216 | tf_op jit(solution)/shard_map/all_to_all | solution.py:27
  25.4 30.3 %copy-start.24 = (bf16[4096,2,2,1]{0,2,3,1:T(2,128)(2,1)S(1)}, bf16[4096,2,2,1]{0,2,3,1:T(2,128)(2,1)}, u32[]{:S(2)}) copy-start(bf16[4096,2,2,1]{0,2,3,1:T(2,128)(2,1)} %param.20) | copy-start | bytes 98308
  26.1 74.7 %copy-start = (bf16[256,4096]{1,0:T(8,128)(2,1)}, bf16[256,4096]{1,0:T(8,128)(2,1)S(1)}, u32[]{:S(2)}) copy-start(bf16[256,4096]{1,0:T(8,128)(2,1)S(1)} %fusion.2.normed_ref) | copy-start | bytes 6291460
  32.2 35.4 %copy-start.17 = (bf16[8,32,384]{2,1,0:T(8,128)(2,1)}, bf16[8,32,384]{2,1,0:T(8,128)(2,1)S(1)}, u32[]{:S(2)}) copy-start(bf16[8,32,384]{2,1,0:T(8,128)(2,1)S(1)} %all-to-all-done) | copy-start | bytes 589828
  32.2 8.3 %collective-permute-start = (bf16[8,32,384]{2,1,0:T(8,128)(2,1)S(1)}, bf16[8,32,384]{2,1,0:T(8,128)(2,1)}, u32[]{:S(2)}, u32[]{:S(2)}) collective-permute-start(bf16[8,32,384]{2,1,0:T(8,128)(2,1)S(1)} %all-to-all-done), channel_id=1, source_target_pairs={{0,8},{8,16},{16,24},{24,32},{32,40},{40,48},{48,56},{56,0},{1,9},... | collective-permute-start | bytes 589832 | tf_op jit(solution)/shard_map/ppermute | solution.py:394
  35.4 7.1 %collective-permute-start.1 = (bf16[8,32,384]{2,1,0:T(8,128)(2,1)S(1)}, bf16[8,32,384]{2,1,0:T(8,128)(2,1)}, u32[]{:S(2)}, u32[]{:S(2)}) collective-permute-start(bf16[8,32,384]{2,1,0:T(8,128)(2,1)S(1)} %all-to-all-done), channel_id=1, source_target_pairs={{0,56},{8,0},{16,8},{24,16},{32,24},{40,32},{48,40},{56,48},{1,57}... | collective-permute-start | bytes 589832 | tf_op jit(solution)/shard_map/ppermute | solution.py:397
  40.5 8.2 %collective-permute-start.2 = (bf16[8,32,384]{2,1,0:T(8,128)(2,1)}, bf16[8,32,384]{2,1,0:T(8,128)(2,1)S(1)}, u32[]{:S(2)}, u32[]{:S(2)}) collective-permute-start(bf16[8,32,384]{2,1,0:T(8,128)(2,1)} %collective-permute-done), channel_id=1, source_target_pairs={{0,8},{8,16},{16,24},{24,32},{32,40},{40,48},{48,56},{56,0},{1,9},... | collective-permute-start | bytes 589832 | tf_op jit(solution)/shard_map/ppermute | solution.py:394
  42.4 8.4 %collective-permute-start.3 = (bf16[8,32,384]{2,1,0:T(8,128)(2,1)}, bf16[8,32,384]{2,1,0:T(8,128)(2,1)S(1)}, u32[]{:S(2)}, u32[]{:S(2)}) collective-permute-start(bf16[8,32,384]{2,1,0:T(8,128)(2,1)} %collective-permute-done.1), channel_id=1, source_target_pairs={{0,56},{8,0},{16,8},{24,16},{32,24},{40,32},{48,40},{56,48},{1,57}... | collective-permute-start | bytes 589832 | tf_op jit(solution)/shard_map/ppermute | solution.py:397
  48.7 7.9 %collective-permute-start.4 = (bf16[8,32,384]{2,1,0:T(8,128)(2,1)S(1)}, bf16[8,32,384]{2,1,0:T(8,128)(2,1)S(1)}, u32[]{:S(2)}, u32[]{:S(2)}) collective-permute-start(bf16[8,32,384]{2,1,0:T(8,128)(2,1)S(1)} %collective-permute-done.2), channel_id=1, source_target_pairs={{0,8},{8,16},{16,24},{24,32},{32,40},{40,48},{48,56},{56,0},{1,9},... | collective-permute-start | bytes 589832 | tf_op jit(solution)/shard_map/ppermute | solution.py:394
  50.9 7.5 %collective-permute-start.5 = (bf16[8,32,384]{2,1,0:T(8,128)(2,1)S(1)}, bf16[8,32,384]{2,1,0:T(8,128)(2,1)S(1)}, u32[]{:S(2)}, u32[]{:S(2)}) collective-permute-start(bf16[8,32,384]{2,1,0:T(8,128)(2,1)S(1)} %collective-permute-done.3), channel_id=1, source_target_pairs={{0,56},{8,0},{16,8},{24,16},{32,24},{40,32},{48,40},{56,48},{1,57}... | collective-permute-start | bytes 589832 | tf_op jit(solution)/shard_map/ppermute | solution.py:397
  60.2 29.3 %collective-permute-start.8 = (bf16[4,8,32,384]{3,2,1,0:T(8,128)(2,1)S(1)}, bf16[4,8,32,384]{3,2,1,0:T(8,128)(2,1)}, u32[]{:S(2)}, u32[]{:S(2)}) collective-permute-start(bf16[4,8,32,384]{3,2,1,0:T(8,128)(2,1)S(1)} %pad_maximum_fusion.refs_1_), channel_id=1, source_target_pairs={{0,4},{4,0},{1,5},{5,1},{2,6},{6,2},{3,7},{7,3},{8,12},{12,8},{9,1... | collective-permute-start | bytes 2359304 | tf_op jit(solution)/shard_map/ppermute | solution.py:404
  68.8 20.6 %collective-permute-start.7 = (bf16[3,8,32,384]{3,2,1,0:T(8,128)(2,1)S(1)}, bf16[3,8,32,384]{3,2,1,0:T(8,128)(2,1)}, u32[]{:S(2)}, u32[]{:S(2)}) collective-permute-start(bf16[3,8,32,384]{3,2,1,0:T(8,128)(2,1)S(1)} %pad_maximum_fusion.1.refs_0_), channel_id=1, source_target_pairs={{0,4},{4,0},{1,5},{5,1},{2,6},{6,2},{3,7},{7,3},{8,12},{12,8},{9,1... | collective-permute-start | bytes 1769480 | tf_op jit(solution)/shard_map/ppermute | solution.py:404
  71.4 14.3 %collective-permute-start.6 = (bf16[8,32,384]{2,1,0:T(8,128)(2,1)}, bf16[8,32,384]{2,1,0:T(8,128)(2,1)S(1)}, u32[]{:S(2)}, u32[]{:S(2)}) collective-permute-start(bf16[8,32,384]{2,1,0:T(8,128)(2,1)} %copy-done.18), channel_id=1, source_target_pairs={{0,8},{8,16},{16,24},{24,32},{32,40},{40,48},{48,56},{56,0},{1,9},... | collective-permute-start | bytes 589832 | tf_op jit(solution)/shard_map/ppermute | solution.py:394
  85.7 3.8 %collective-permute-start.9 = (bf16[1,8,32,384]{3,2,1,0:T(8,128)(2,1)S(1)}, bf16[1,8,32,384]{3,2,1,0:T(8,128)(2,1)S(1)}, u32[]{:S(2)}, u32[]{:S(2)}) collective-permute-start(bf16[1,8,32,384]{3,2,1,0:T(8,128)(2,1)S(1)} %bitcast.36), channel_id=1, source_target_pairs={{0,4},{4,0},{1,5},{5,1},{2,6},{6,2},{3,7},{7,3},{8,12},{12,8},{9,1... | collective-permute-start | bytes 589832 | tf_op jit(solution)/shard_map/ppermute | solution.py:404
  94.1 19.0 %all-to-all-start.1 = ((bf16[16,48,128]{2,1,0:T(8,128)(2,1)}), bf16[16,48,128]{2,1,0:T(8,128)(2,1)S(1)}, u32[]{:S(2)}, u32[]{:S(2)}) async-start(bf16[16,48,128]{2,1,0:T(8,128)(2,1)} %copy-done.3), calls=%async_computation.1 | async-start | bytes 393216 | tf_op jit(solution)/shard_map/all_to_all | solution.py:27
  100.9 17.6 %collective-permute-start.10 = (bf16[1,4096]{1,0:T(2,128)(2,1)S(1)}, bf16[1,4096]{1,0:T(2,128)(2,1)S(1)}, u32[]{:S(2)}, u32[]{:S(2)}) collective-permute-start(bf16[1,4096]{1,0:T(2,128)(2,1)S(1)} %get-tuple-element.38), channel_id=1, source_target_pairs={{0,4},{4,8},{8,12},{12,16},{16,20},{20,24},{24,28},{28,32},{32,36}... | collective-permute-start | bytes 24584 | tf_op jit(solution)/shard_map/ppermute | solution.py:33
  104.4 14.0 %collective-permute-start.11 = (bf16[1,4096]{1,0:T(2,128)(2,1)S(1)}, bf16[1,4096]{1,0:T(2,128)(2,1)S(1)}, u32[]{:S(2)}, u32[]{:S(2)}) collective-permute-start(bf16[1,4096]{1,0:T(2,128)(2,1)S(1)} %get-tuple-element.39), channel_id=1, source_target_pairs={{4,0},{8,4},{12,8},{16,12},{20,16},{24,20},{28,24},{32,28},{36,32}... | collective-permute-start | bytes 24584 | tf_op jit(solution)/shard_map/ppermute | solution.py:34
  113.9 12.5 %all-to-all-start.2 = ((bf16[8,48,128]{2,1,0:T(8,128)(2,1)}), bf16[8,48,128]{2,1,0:T(8,128)(2,1)S(1)}, u32[]{:S(2)}, u32[]{:S(2)}) async-start(bf16[8,48,128]{2,1,0:T(8,128)(2,1)} %get-tuple-element.36), calls=%async_computation.2 | async-start | bytes 196608 | tf_op jit(solution)/shard_map/all_to_all | solution.py:27
  127.4 19.0 %all-to-all-start.3 = ((bf16[16,48,128]{2,1,0:T(8,128)(2,1)}), bf16[16,48,128]{2,1,0:T(8,128)(2,1)S(1)}, u32[]{:S(2)}, u32[]{:S(2)}) async-start(bf16[16,48,128]{2,1,0:T(8,128)(2,1)} %shard_map.150), calls=%async_computation.3 | async-start | bytes 393216 | tf_op jit(solution)/shard_map/all_to_all | solution.py:27
  132.0 9.8 %collective-permute-start.12 = (bf16[256,256]{1,0:T(8,128)(2,1)}, bf16[256,256]{1,0:T(8,128)(2,1)S(1)}, u32[]{:S(2)}, u32[]{:S(2)}) collective-permute-start(bf16[256,256]{1,0:T(8,128)(2,1)} %get-tuple-element.51.refs_0_), channel_id=1, source_target_pairs={{0,1},{1,2},{2,3},{3,0},{4,5},{5,6},{6,7},{7,4},{8,9},{9,10},{10,1... | collective-permute-start | bytes 393224 | tf_op jit(solution)/shard_map/ppermute | solution.py:471
  135.1 6.8 %collective-permute-start.13 = (bf16[256,256]{1,0:T(8,128)(2,1)}, bf16[256,256]{1,0:T(8,128)(2,1)S(1)}, u32[]{:S(2)}, u32[]{:S(2)}) collective-permute-start(bf16[256,256]{1,0:T(8,128)(2,1)} %get-tuple-element.51.refs_0_), channel_id=1, source_target_pairs={{0,3},{1,0},{2,1},{3,2},{4,7},{5,4},{6,5},{7,6},{8,11},{9,8},{10,9... | collective-permute-start | bytes 393224 | tf_op jit(solution)/shard_map/ppermute | solution.py:471
  138.5 7.9 %collective-permute-start.14 = (bf16[256,256]{1,0:T(8,128)(2,1)}, bf16[256,256]{1,0:T(8,128)(2,1)S(1)}, u32[]{:S(2)}, u32[]{:S(2)}) collective-permute-start(bf16[256,256]{1,0:T(8,128)(2,1)} %get-tuple-element.51.refs_0_), channel_id=1, source_target_pairs={{0,2},{1,3},{2,0},{3,1},{4,6},{5,7},{6,4},{7,5},{8,10},{9,11},{10,... | collective-permute-start | bytes 393224 | tf_op jit(solution)/shard_map/ppermute | solution.py:471
  149.0 11.1 %all-to-all-start.4 = ((bf16[4,256,256]{2,1,0:T(8,128)(2,1)}), bf16[4,256,256]{2,1,0:T(8,128)(2,1)S(1)}, u32[]{:S(2)}, u32[]{:S(2)}) async-start(bf16[4,256,256]{2,1,0:T(8,128)(2,1)} %shard_map.151), calls=%async_computation.4 | async-start | bytes 1048576 | tf_op jit(solution)/shard_map/all_to_all | solution.py:27
  (26 other events, 266.7 us)
Sparse Core Ops, SparseCore 0:
  12.4 101.6 all-gather.1
where the time goes:
time: 175 us; the launch traced here: 173 us
  starting transfers between devices  81.3 us (46%)
  waiting for transfers between devices  41.5 us (24%)
  Pallas kernels  20.6 us (12%)
  between operations  13.9 us (8%)
  local copies, waits for them, and re-layouts  8.93 us (5%)
  other arithmetic  6.16 us (4%)
    all_to_all x5, starting transfers between devices, swapped(): return lax.all_to_all(value, axes, split_axis=0, concat_axis=0, tiled=True)  30.3 us
    pallas_call x8, Pallas kernels, on_core(): pl.pallas_call(kernel, out_shape=out, in_specs=[smem] * scalars + [vmem]...  20.6 us
    all_to_all x5, waiting for transfers between devices, swapped(): return lax.all_to_all(value, axes, split_axis=0, concat_axis=0, tiled=True)  20.3 us
    ppermute x4, waiting for transfers between devices, body(): up = lax.ppermute(up, 'sp_1', ring(8, 1))  14.4 us
    ppermute x3, starting transfers between devices, body(): down = lax.ppermute(down, 'sp_1', ring(8, -1))  13.7 us
    ppermute x3, starting transfers between devices, body(): groups.append(lax.ppermute(group, 'sp_2', ring(2, 1)))  12 us
    ppermute x4, starting transfers between devices, body(): up = lax.ppermute(up, 'sp_1', ring(8, 1))  10.1 us
    ppermute x3, starting transfers between devices, body(): lax.ppermute(conv_out, 'tp', ring(4, n))  9.82 us
  transfers between devices with their start and end apart: 21, of which 11 were waited for; matrix products, arithmetic and copies ran while one was open for 4% of the time, Pallas kernels for 7%

commit v1 on v0

--- a/solution.py
+++ b/solution.py
@@ -65,19 +65,25 @@
 GROUPS = (3, 4, 1)
 
 
-def pack_kernel(query_ref, key_ref, value_ref, outer_ref, inner_ref, given_ref, out_ref, whole_ref, block_ref):
+def pack_kernel(query_ref, key_ref, value_ref, outer_ref, inner_ref, given_ref, out_ref, whole_ref, block_ref, sems):
+    moves = []
+    for z in range(block_ref.shape[0]):
+        moves.append((key_ref, block_ref.at[z, :, pl.ds(0, DQK)]))
+        moves.append((value_ref, block_ref.at[z, :, pl.ds(DQK, DV)]))
     at = 0
     for ref in (query_ref, inner_ref, given_ref, outer_ref):
-        whole_ref[:, at : at + ref.shape[1]] = ref[...]
+        moves.append((ref, whole_ref.at[:, pl.ds(at, ref.shape[1])]))
         at += ref.shape[1]
     depth, columns = out_ref.shape
+    half = columns // 2
     for side in range(2):
-        whole_ref[side * depth : (side + 1) * depth, at:] = out_ref[
-            :, side * columns // 2 : (side + 1) * columns // 2
-        ]
-    for z in range(block_ref.shape[0]):
-        block_ref[z, :, :DQK] = key_ref[...]
-        block_ref[z, :, DQK:] = value_ref[...]
+        target = whole_ref.at[pl.ds(side * depth, depth), pl.ds(at, half)]
+        moves.append((out_ref.at[:, pl.ds(side * half, half)], target))
+    moves = moves[::-1]
+    for n, (source, target) in enumerate(moves):
+        pltpu.make_async_copy(source, target, sems.at[n]).start()
+    for n, (source, target) in enumerate(moves):
+        pltpu.make_async_copy(source, target, sems.at[n]).wait()
 
 
 def gate_kernel(forget_ref, gate_ref, row_ref, column_ref, number_ref):
@@ -257,6 +263,7 @@
 
 WIDE = DQK + 3 * DV
 CHUNKS = 8
+AHEAD = 2
 
 
 def project_kernel(
@@ -270,10 +277,12 @@
             whole_ref.at[pl.ds(k * depth, depth), pl.ds(0, WIDE)], weight_ref.at[k], sems.at[k]
         )
 
-    for k in range(CHUNKS):
+    for k in range(AHEAD):
         fetch(k).start()
     for k in range(CHUNKS):
         fetch(k).wait()
+        if k + AHEAD < CHUNKS:
+            fetch(k + AHEAD).start()
         at = slice(k * depth, (k + 1) * depth)
         rows = jnp.concatenate([normed_ref[:, at], edge_ref[:, at]], axis=0)
         product = jnp.dot(rows, weight_ref[k], preferred_element_type=F32)
@@ -297,47 +306,73 @@
     conv_ref[...] = (outer * filtered).astype(BF16)
 
 
-def output_kernel(place_ref, lstm_ref, *refs):
+def fetch_rows(whole_ref, weight_ref, sems, device, slot):
+    return [
+        pltpu.make_async_copy(
+            whole_ref.at[pl.ds(device, 16), side, :, pl.ds(WIDE, 512)],
+            weight_ref.at[slot, side],
+            sems.at[slot, side],
+        )
+        for side in range(2)
+    ]
+
+
+def convolved_kernel(place_ref, *refs):
     parts, (whole_ref, out_ref, weight_ref, sems) = refs[:4], refs[4:]
     place = place_ref[0]
-    sources = [(k * 32, lstm_ref.at[k]) for k in range(4)]
-    for part_ref, offset in zip(parts, (0, -1, 1, 2)):
-        sources.append(((place + offset + 4) % 4 * 32 + 16, part_ref))
-
-    def fetch(n, side):
-        return pltpu.make_async_copy(
-            whole_ref.at[pl.ds(sources[n][0], 16), side, :, pl.ds(WIDE, 512)],
-            weight_ref.at[n, side],
-            sems.at[n, side],
-        )
-
+    now = []
+    for n, offset in enumerate((0, -1, 1, 2)):
+        now.append(fetch_rows(whole_ref, weight_ref, sems, (place + offset + 4) % 4 * 32 + 16, n))
+    for pair in now:
+        for copy in pair:
+            copy.start()
+    for n, part_ref in enumerate(parts):
+        for side in range(2):
+            now[n][side].wait()
+            weight = weight_ref[n, side].reshape(DV, 512)
+            product = jnp.dot(part_ref[...], weight, preferred_element_type=F32)
+            at = slice(side * 512, (side + 1) * 512)
+            if n:
+                out_ref[:, at] += product
+            else:
+                out_ref[:, at] = product
+
+
+def output_kernel(joined_ref, whole_ref, earlier_ref, out_ref, weight_ref, total_ref, sems, sem):
+    parts = [fetch_rows(whole_ref, weight_ref, sems, k * 32, k) for k in range(4)]
     for side in range(2):
-        for n in range(8):
-            fetch(n, side).start()
+        for k in range(4):
+            parts[k][side].start()
+    fetch = pltpu.make_async_copy(earlier_ref, total_ref, sem)
+    fetch.start()
     for side in range(2):
+        at = slice(side * 512, (side + 1) * 512)
         total = None
-        for n in range(8):
-            fetch(n, side).wait()
-            weight = weight_ref[n, side].reshape(DV, 512)
-            product = jnp.dot(sources[n][1][...], weight, preferred_element_type=F32)
+        for k in range(4):
+            parts[k][side].wait()
+            weight = weight_ref[k, side].reshape(DV, 512)
+            product = jnp.dot(joined_ref[k], weight, preferred_element_type=F32)
             total = product if total is None else total + product
-        out_ref[:, side * 512 : (side + 1) * 512] = total.astype(BF16)
+        if not side:
+            fetch.wait()
+        out_ref[:, at] = (total + total_ref[:, at]).astype(BF16)
 
 
 def ring(size, step):
     return [(i, (i + step) % size) for i in range(size)]
 
 
-def on_core(kernel, out, *operands, scalars=0, remote=0, scratch=(), limit=20):
+def on_core(kernel, out, *operands, scalars=0, remote=0, scratch=(), limit=20, outside=False):
     vmem = pl.BlockSpec(memory_space=pltpu.VMEM)
     smem = pl.BlockSpec(memory_space=pltpu.SMEM)
+    hbm = pl.BlockSpec(memory_space=pltpu.HBM)
     return pl.pallas_call(
         kernel,
         out_shape=out,
         in_specs=[smem] * scalars
         + [vmem] * (len(operands) - scalars - remote)
-        + [pl.BlockSpec(memory_space=pltpu.HBM)] * remote,
-        out_specs=jax.tree.map(lambda _: vmem, out),
+        + [hbm] * remote,
+        out_specs=jax.tree.map(lambda _: hbm if outside else vmem, out),
         scratch_shapes=scratch,
         compiler_params=pltpu.CompilerParams(vmem_limit_bytes=limit * 2**20),
     )(*operands)
@@ -380,6 +415,10 @@
         w_conv_c,
         w_conv_in,
         w_out,
+        remote=7,
+        scratch=[pltpu.SemaphoreType.DMA((6 + 2 * planes,))],
+        outside=True,
+        limit=63,
     )
     block = swapped(block, "sp_0")
     whole = lax.all_gather(packed, SP, axis=0, tiled=True)
@@ -465,11 +504,10 @@
         ],
         limit=54,
     )
-    far, queries, conv_out = lax.optimization_barrier((far, queries, conv_out))
     start = on_core(far_kernel, block, plane[None], near, far, scalars=1)
     start = swapped(start, PLANE)
     parts = [conv_out] + [lax.ppermute(conv_out, "tp", ring(4, n)) for n in (1, -1, 2)]
-    start, *parts = lax.optimization_barrier((start, *parts))
+    start, *parts[:3] = lax.optimization_barrier((start, *parts[:3]))
     lstm_out = on_core(
         read_kernel,
         jax.ShapeDtypeStruct((4, length, DV), BF16),
@@ -483,20 +521,34 @@
     )
     lstm_all = swapped(lstm_out, "tp")
     whole = whole.reshape(size, 2, depth, -1)
-    return on_core(
-        output_kernel,
-        jax.ShapeDtypeStruct((length, 2 * half), BF16),
+    done = on_core(
+        convolved_kernel,
+        jax.ShapeDtypeStruct((length, 2 * half), F32),
         lax.axis_index("tp")[None],
-        lstm_all,
         *parts,
         whole,
         scalars=1,
         remote=1,
         scratch=[
-            pltpu.VMEM((8, 2, 16, depth, half), BF16),
-            pltpu.SemaphoreType.DMA((8, 2)),
+            pltpu.VMEM((4, 2, 16, depth, half), BF16),
+            pltpu.SemaphoreType.DMA((4, 2)),
         ],
-        limit=58,
+        limit=54,
+    )
+    return on_core(
+        output_kernel,
+        jax.ShapeDtypeStruct((length, 2 * half), BF16),
+        lstm_all,
+        whole,
+        done,
+        remote=2,
+        scratch=[
+            pltpu.VMEM((4, 2, 16, depth, half), BF16),
+            pltpu.VMEM(done.shape, F32),
+            pltpu.SemaphoreType.DMA((4, 2)),
+            pltpu.SemaphoreType.DMA,
+        ],
+        limit=53,
     )
 
 

time: 175 us -> 188 us (1.074)
  blocking collectives: 0 us -> 18.9 us
  Pallas kernels: 20.6 us -> 33.3 us
  waiting for transfers between devices: 41.5 us -> 34.9 us
  local copies, waits for them, and re-layouts: 8.93 us -> 2.43 us
  starting transfers between devices: 81.3 us -> 75.9 us
    all_to_all x0 -> x1, blocking collectives: none -> 18.9 us  [swapped(): return lax.all_to_all(value, axes, split_axis=0, concat_axis=0, tiled=True)]
    pallas_call x8 -> x9, Pallas kernels: 20.6 us -> 33.3 us  [on_core(): pl.pallas_call(kernel, out_shape=out, in_specs=[smem] * scalars + [vmem]...]
    all_to_all x5 -> x4, waiting for transfers between devices: 20.3 us -> 9.19 us  [swapped(): return lax.all_to_all(value, axes, split_axis=0, concat_axis=0, tiled=True)]
    unnamed x58 -> x42, local copies, waits for them, and re-layouts: 8.78 us -> 2.28 us
    all_to_all x5 -> x4, starting transfers between devices: 30.3 us -> 24.4 us  [swapped(): return lax.all_to_all(value, axes, split_axis=0, concat_axis=0, tiled=True)]
    ppermute x3, waiting for transfers between devices: 4.49 us -> 9.09 us  [body(): lax.ppermute(conv_out, 'tp', ring(4, n))]
  transfers between devices with their start and end apart: 21 -> 20, of which waited for: 11 -> 12; matrix products, arithmetic and copies ran while one was open for 4% -> 4% of each run, Pallas kernels for 7% -> 10%
where the time goes in v1:
time: 188 us; the launch traced here: 186 us
  starting transfers between devices  75.9 us (40%)
  waiting for transfers between devices  34.9 us (19%)
  Pallas kernels  33.3 us (18%)
  blocking collectives  18.9 us (10%)
  between operations  13.8 us (7%)
  other arithmetic  6.17 us (3%)
  local copies, waits for them, and re-layouts  2.43 us (1%)
    pallas_call x9, Pallas kernels, on_core(): pl.pallas_call(kernel, out_shape=out, in_specs=[smem] * scalars + [vmem]...  33.3 us
    all_to_all x4, starting transfers between devices, swapped(): return lax.all_to_all(value, axes, split_axis=0, concat_axis=0, tiled=True)  24.4 us
    all_to_all x1, blocking collectives, swapped(): return lax.all_to_all(value, axes, split_axis=0, concat_axis=0, tiled=True)  18.9 us
    ppermute x4, waiting for transfers between devices, body(): up = lax.ppermute(up, 'sp_1', ring(8, 1))  14.4 us
    ppermute x3, starting transfers between devices, body(): down = lax.ppermute(down, 'sp_1', ring(8, -1))  13.7 us
    ppermute x3, starting transfers between devices, body(): groups.append(lax.ppermute(group, 'sp_2', ring(2, 1)))  12 us
    ppermute x3, starting transfers between devices, body(): lax.ppermute(conv_out, 'tp', ring(4, n))  11.4 us
    ppermute x4, starting transfers between devices, body(): up = lax.ppermute(up, 'sp_1', ring(8, 1))  10.1 us
  transfers between devices with their start and end apart: 20, of which 12 were waited for; matrix products, arithmetic and copies ran while one was open for 4% of the time, Pallas kernels for 10%

profile of v1, /device:TPU:1, one launch (start us, length us, event | category | flops | bytes accessed | tf_op | source)
XLA Modules:
  0.0 186.1 jit_solution(14296859611681611996)
XLA Ops:
  6.5 10.0 %shard_map.145 = (bf16[32,1408]{1,0:T(8,128)(2,1)}, bf16[8,32,384]{2,1,0:T(8,128)(2,1)}) custom-call(bf16[32,128]{1,0:T(8,128)(2,1)} %query_ref.1, bf16[32,128]{1,0:T(8,128)(2,1)} %key_ref.1, bf16[32,256]{1,0:T(8,128)(2,1)} %value_ref.1, bf16[32,256]{1,0:T(8,128)(2,1)} %outer_ref.1, bf16[32,256]{1,0:T(8,128)(2,1)} %inner_ref.1, bf16[32,256]{1,0:T(8,128)(2,1)} %given_ref.1, ...), custom_call_target="tpu_custom_call" | custom-call | tf_op jit(solution)/shard_map/pallas_call | solution.py:369
  16.6 10.9 %all-to-all-start = ((bf16[8,32,384]{2,1,0:T(8,128)(2,1)}), bf16[8,32,384]{2,1,0:T(8,128)(2,1)S(1)}, u32[]{:S(2)}, u32[]{:S(2)}) async-start(bf16[8,32,384]{2,1,0:T(8,128)(2,1)} %get-tuple-element.26), calls=%async_computation | async-start | bytes 393216 | tf_op jit(solution)/shard_map/all_to_all | solution.py:27
  30.4 6.1 %all-to-all-done = bf16[8,32,384]{2,1,0:T(8,128)(2,1)S(1)} async-done(((bf16[8,32,384]{2,1,0:T(8,128)(2,1)}), bf16[8,32,384]{2,1,0:T(8,128)(2,1)S(1)}, u32[]{:S(2)}, u32[]{:S(2)}) %all-to-all-start) | async-done | bytes 196640 | tf_op jit(solution)/shard_map/all_to_all | solution.py:27
  36.4 3.2 %collective-permute-start = (bf16[8,32,384]{2,1,0:T(8,128)(2,1)S(1)}, bf16[8,32,384]{2,1,0:T(8,128)(2,1)}, u32[]{:S(2)}, u32[]{:S(2)}) collective-permute-start(bf16[8,32,384]{2,1,0:T(8,128)(2,1)S(1)} %all-to-all-done), channel_id=1, source_target_pairs={{0,8},{8,16},{16,24},{24,32},{32,40},{40,48},{48,56},{56,0},{1,9},... | collective-permute-start | bytes 589832 | tf_op jit(solution)/shard_map/ppermute | solution.py:433
  39.6 3.8 %collective-permute-start.1 = (bf16[8,32,384]{2,1,0:T(8,128)(2,1)S(1)}, bf16[8,32,384]{2,1,0:T(8,128)(2,1)}, u32[]{:S(2)}, u32[]{:S(2)}) collective-permute-start(bf16[8,32,384]{2,1,0:T(8,128)(2,1)S(1)} %all-to-all-done), channel_id=1, source_target_pairs={{0,56},{8,0},{16,8},{24,16},{32,24},{40,32},{48,40},{56,48},{1,57}... | collective-permute-start | bytes 589832 | tf_op jit(solution)/shard_map/ppermute | solution.py:436
  46.7 5.0 %collective-permute-start.3 = (bf16[8,32,384]{2,1,0:T(8,128)(2,1)}, bf16[8,32,384]{2,1,0:T(8,128)(2,1)S(1)}, u32[]{:S(2)}, u32[]{:S(2)}) collective-permute-start(bf16[8,32,384]{2,1,0:T(8,128)(2,1)} %collective-permute-done.1), channel_id=1, source_target_pairs={{0,56},{8,0},{16,8},{24,16},{32,24},{40,32},{48,40},{56,48},{1,57}... | collective-permute-start | bytes 589832 | tf_op jit(solution)/shard_map/ppermute | solution.py:436
  55.1 4.9 %collective-permute-start.5 = (bf16[8,32,384]{2,1,0:T(8,128)(2,1)S(1)}, bf16[8,32,384]{2,1,0:T(8,128)(2,1)S(1)}, u32[]{:S(2)}, u32[]{:S(2)}) collective-permute-start(bf16[8,32,384]{2,1,0:T(8,128)(2,1)S(1)} %collective-permute-done.3), channel_id=1, source_target_pairs={{0,56},{8,0},{16,8},{24,16},{32,24},{40,32},{48,40},{56,48},{1,57}... | collective-permute-start | bytes 589832 | tf_op jit(solution)/shard_map/ppermute | solution.py:436
  64.5 7.3 %collective-permute-start.8 = (bf16[4,8,32,384]{3,2,1,0:T(8,128)(2,1)S(1)}, bf16[4,8,32,384]{3,2,1,0:T(8,128)(2,1)}, u32[]{:S(2)}, u32[]{:S(2)}) collective-permute-start(bf16[4,8,32,384]{3,2,1,0:T(8,128)(2,1)S(1)} %pad_maximum_fusion.refs_1_), channel_id=1, source_target_pairs={{0,4},{4,0},{1,5},{5,1},{2,6},{6,2},{3,7},{7,3},{8,12},{12,8},{9,1... | collective-permute-start | bytes 2359304 | tf_op jit(solution)/shard_map/ppermute | solution.py:443
  75.6 3.1 %collective-permute-start.6 = (bf16[8,32,384]{2,1,0:T(8,128)(2,1)}, bf16[8,32,384]{2,1,0:T(8,128)(2,1)S(1)}, u32[]{:S(2)}, u32[]{:S(2)}) collective-permute-start(bf16[8,32,384]{2,1,0:T(8,128)(2,1)} %copy-done.9), channel_id=1, source_target_pairs={{0,8},{8,16},{16,24},{24,32},{32,40},{40,48},{48,56},{56,0},{1,9},... | collective-permute-start | bytes 589832 | tf_op jit(solution)/shard_map/ppermute | solution.py:433
  78.7 11.2 %collective-permute-done.6 = bf16[8,32,384]{2,1,0:T(8,128)(2,1)S(1)} collective-permute-done((bf16[8,32,384]{2,1,0:T(8,128)(2,1)}, bf16[8,32,384]{2,1,0:T(8,128)(2,1)S(1)}, u32[]{:S(2)}, u32[]{:S(2)}) %collective-permute-start.6) | collective-permute-done | bytes 196640 | tf_op jit(solution)/shard_map/ppermute | solution.py:433
  90.0 2.7 %collective-permute-start.9 = (bf16[1,8,32,384]{3,2,1,0:T(8,128)(2,1)S(1)}, bf16[1,8,32,384]{3,2,1,0:T(8,128)(2,1)S(1)}, u32[]{:S(2)}, u32[]{:S(2)}) collective-permute-start(bf16[1,8,32,384]{3,2,1,0:T(8,128)(2,1)S(1)} %bitcast.36), channel_id=1, source_target_pairs={{0,4},{4,0},{1,5},{5,1},{2,6},{6,2},{3,7},{7,3},{8,12},{12,8},{9,1... | collective-permute-start | bytes 589832 | tf_op jit(solution)/shard_map/ppermute | solution.py:443
  93.7 3.2 %shard_map.147 = (bf16[16,48,128]{2,1,0:T(8,128)(2,1)S(1)}, bf16[256,128]{1,0:T(8,128)(2,1)S(1)}, bf16[256,256]{1,0:T(8,128)(2,1)S(1)}) custom-call(s32[2]{0:T(128)S(1)} %pad_add_fusion.place_ref, bf16[256,4096]{1,0:T(8,128)(2,1)S(1)} %fusion.2.normed_ref, f32[256,8]{1,0:T(8,128)S(1)} %get-tuple-element.28.update_ref.column_ref, ...), custom_call_target="tpu_custom_call" | custom-call | tf_op jit(solution)/shard_map/pallas_call | solution.py:369
  97.0 18.9 %all_to_all.25.state_ref = bf16[16,48,128]{2,1,0:T(8,128)(2,1)S(1)} all-to-all(bf16[16,48,128]{2,1,0:T(8,128)(2,1)S(1)} %get-tuple-element.39), channel_id=1, replica_groups=mesh['sp_0'=8,'sp_1'=8,'sp_2'=2,'tp'=4] {'sp_1','sp_2'}, dimensions={0} | all-to-all | bytes 393216 | tf_op jit(solution)/shard_map/all_to_all | solution.py:27
  116.7 4.5 %all-to-all-start.2 = ((bf16[8,48,128]{2,1,0:T(8,128)(2,1)}), bf16[8,48,128]{2,1,0:T(8,128)(2,1)S(1)}, u32[]{:S(2)}, u32[]{:S(2)}) async-start(bf16[8,48,128]{2,1,0:T(8,128)(2,1)} %get-tuple-element.41), calls=%async_computation.2 | async-start | bytes 196608 | tf_op jit(solution)/shard_map/all_to_all | solution.py:27
  125.7 3.1 %all-to-all-done.2.planes_ref = bf16[8,48,128]{2,1,0:T(8,128)(2,1)S(1)} async-done(((bf16[8,48,128]{2,1,0:T(8,128)(2,1)}), bf16[8,48,128]{2,1,0:T(8,128)(2,1)S(1)}, u32[]{:S(2)}, u32[]{:S(2)}) %all-to-all-start.2) | async-done | bytes 98336 | tf_op jit(solution)/shard_map/all_to_all | solution.py:27
  129.7 5.0 %all-to-all-start.3 = ((bf16[16,48,128]{2,1,0:T(8,128)(2,1)}), bf16[16,48,128]{2,1,0:T(8,128)(2,1)S(1)}, u32[]{:S(2)}, u32[]{:S(2)}) async-start(bf16[16,48,128]{2,1,0:T(8,128)(2,1)} %shard_map.150), calls=%async_computation.3 | async-start | bytes 393216 | tf_op jit(solution)/shard_map/all_to_all | solution.py:27
  135.6 8.3 %shard_map.148 = (bf16[256,128]{1,0:T(8,128)(2,1)}, bf16[256,256]{1,0:T(8,128)(2,1)}) custom-call(bf16[256,4096]{1,0:T(8,128)(2,1)} %copy-done, bf16[16,4096]{1,0:T(8,128)(2,1)} %maximum_maximum_fusion.edge_ref, bf16[3,256]{1,0:T(4,128)(2,1)} %tap_ref.1, bf16[4096,1408]{1,0:T(8,128)(2,1)} %all-gather.2.cloned.1.call-done.whole_ref), custom_call_target="tpu_custom_call" | custom-call | tf_op jit(solution)/shard_map/pallas_call | solution.py:369
  143.8 3.1 %collective-permute-start.12 = (bf16[256,256]{1,0:T(8,128)(2,1)}, bf16[256,256]{1,0:T(8,128)(2,1)S(1)}, u32[]{:S(2)}, u32[]{:S(2)}) collective-permute-start(bf16[256,256]{1,0:T(8,128)(2,1)} %get-tuple-element.44.refs_0_), channel_id=1, source_target_pairs={{0,1},{1,2},{2,3},{3,0},{4,5},{5,6},{6,7},{7,4},{8,9},{9,10},{10,1... | collective-permute-start | bytes 393224 | tf_op jit(solution)/shard_map/ppermute | solution.py:509
  146.9 3.4 %collective-permute-start.13 = (bf16[256,256]{1,0:T(8,128)(2,1)}, bf16[256,256]{1,0:T(8,128)(2,1)S(1)}, u32[]{:S(2)}, u32[]{:S(2)}) collective-permute-start(bf16[256,256]{1,0:T(8,128)(2,1)} %get-tuple-element.44.refs_0_), channel_id=1, source_target_pairs={{0,3},{1,0},{2,1},{3,2},{4,7},{5,4},{6,5},{7,6},{8,11},{9,8},{10,9... | collective-permute-start | bytes 393224 | tf_op jit(solution)/shard_map/ppermute | solution.py:509
  156.2 4.0 %all-to-all-start.4 = ((bf16[4,256,256]{2,1,0:T(8,128)(2,1)}), bf16[4,256,256]{2,1,0:T(8,128)(2,1)S(1)}, u32[]{:S(2)}, u32[]{:S(2)}) async-start(bf16[4,256,256]{2,1,0:T(8,128)(2,1)} %shard_map.151), calls=%async_computation.4 | async-start | bytes 1048576 | tf_op jit(solution)/shard_map/all_to_all | solution.py:27
  160.2 4.9 %collective-permute-start.14 = (bf16[256,256]{1,0:T(8,128)(2,1)S(1)}, bf16[256,256]{1,0:T(8,128)(2,1)S(1)}, u32[]{:S(2)}, u32[]{:S(2)}) collective-permute-start(bf16[256,256]{1,0:T(8,128)(2,1)S(1)} %copy-done.12), channel_id=1, source_target_pairs={{0,2},{1,3},{2,0},{3,1},{4,6},{5,7},{6,4},{7,5},{8,10},{9,11},{10,... | collective-permute-start | bytes 393224 | tf_op jit(solution)/shard_map/ppermute | solution.py:509
  165.1 5.9 %collective-permute-done.14.refs_3_ = bf16[256,256]{1,0:T(8,128)(2,1)S(1)} collective-permute-done((bf16[256,256]{1,0:T(8,128)(2,1)S(1)}, bf16[256,256]{1,0:T(8,128)(2,1)S(1)}, u32[]{:S(2)}, u32[]{:S(2)}) %collective-permute-start.14) | collective-permute-done | bytes 131104 | tf_op jit(solution)/shard_map/ppermute | solution.py:509
  171.6 4.3 %shard_map.152.earlier_ref = f32[256,1024]{1,0:T(8,128)} custom-call(s32[1]{0:T(128)} %bitcast.18.place_ref, bf16[256,256]{1,0:T(8,128)(2,1)} %get-tuple-element.44.refs_0_, bf16[256,256]{1,0:T(8,128)(2,1)} %copy-done.13, bf16[256,256]{1,0:T(8,128)(2,1)} %copy-done.14, bf16[256,256]{1,0:T(8,128)(2,1)} %copy-done.15, bf16[128,2,16,1408]{3,2,1,0:T(8,128)(2,1)} %bitcast.39), custom_call_target="tpu_custom_call" | custom-call | tf_op jit(solution)/shard_map/pallas_call | solution.py:369
  175.9 3.4 %shard_map.153 = bf16[256,1024]{1,0:T(8,128)(2,1)} custom-call(bf16[4,256,256]{2,1,0:T(8,128)(2,1)S(1)} %all-to-all-done.4.joined_ref, bf16[128,2,16,1408]{3,2,1,0:T(8,128)(2,1)} %bitcast.40, f32[256,1024]{1,0:T(8,128)} %shard_map.152.earlier_ref), custom_call_target="tpu_custom_call" | custom-call | tf_op jit(solution)/shard_map/pallas_call | solution.py:369
  (84 shorter events, 32.2 us)
Async XLA Ops:
  6.5 129.0 %all-gather.2.cloned.1.call-start = ((), (), s32[]{:S(2)}) async-start(), calls=%async_computation.5 | async-start | bytes 11624448 | tf_op jit(solution)/shard_map/all_gather | solution.py:424
  16.6 19.9 %all-to-all-start = ((bf16[8,32,384]{2,1,0:T(8,128)(2,1)}), bf16[8,32,384]{2,1,0:T(8,128)(2,1)S(1)}, u32[]{:S(2)}, u32[]{:S(2)}) async-start(bf16[8,32,384]{2,1,0:T(8,128)(2,1)} %get-tuple-element.26), calls=%async_computation | async-start | bytes 393216 | tf_op jit(solution)/shard_map/all_to_all | solution.py:27
  29.7 30.3 %copy-start.16 = (bf16[4096,2,2,1]{0,2,3,1:T(2,128)(2,1)S(1)}, bf16[4096,2,2,1]{0,2,3,1:T(2,128)(2,1)}, u32[]{:S(2)}) copy-start(bf16[4096,2,2,1]{0,2,3,1:T(2,128)(2,1)} %param.20) | copy-start | bytes 98308
  30.3 90.9 %copy-start = (bf16[256,4096]{1,0:T(8,128)(2,1)}, bf16[256,4096]{1,0:T(8,128)(2,1)S(1)}, u32[]{:S(2)}) copy-start(bf16[256,4096]{1,0:T(8,128)(2,1)S(1)} %fusion.2.normed_ref) | copy-start | bytes 6291460
  36.4 35.4 %copy-start.8 = (bf16[8,32,384]{2,1,0:T(8,128)(2,1)}, bf16[8,32,384]{2,1,0:T(8,128)(2,1)S(1)}, u32[]{:S(2)}) copy-start(bf16[8,32,384]{2,1,0:T(8,128)(2,1)S(1)} %all-to-all-done) | copy-start | bytes 589828
  36.4 8.3 %collective-permute-start = (bf16[8,32,384]{2,1,0:T(8,128)(2,1)S(1)}, bf16[8,32,384]{2,1,0:T(8,128)(2,1)}, u32[]{:S(2)}, u32[]{:S(2)}) collective-permute-start(bf16[8,32,384]{2,1,0:T(8,128)(2,1)S(1)} %all-to-all-done), channel_id=1, source_target_pairs={{0,8},{8,16},{16,24},{24,32},{32,40},{40,48},{48,56},{56,0},{1,9},... | collective-permute-start | bytes 589832 | tf_op jit(solution)/shard_map/ppermute | solution.py:433
  39.6 7.1 %collective-permute-start.1 = (bf16[8,32,384]{2,1,0:T(8,128)(2,1)S(1)}, bf16[8,32,384]{2,1,0:T(8,128)(2,1)}, u32[]{:S(2)}, u32[]{:S(2)}) collective-permute-start(bf16[8,32,384]{2,1,0:T(8,128)(2,1)S(1)} %all-to-all-done), channel_id=1, source_target_pairs={{0,56},{8,0},{16,8},{24,16},{32,24},{40,32},{48,40},{56,48},{1,57}... | collective-permute-start | bytes 589832 | tf_op jit(solution)/shard_map/ppermute | solution.py:436
  44.7 8.2 %collective-permute-start.2 = (bf16[8,32,384]{2,1,0:T(8,128)(2,1)}, bf16[8,32,384]{2,1,0:T(8,128)(2,1)S(1)}, u32[]{:S(2)}, u32[]{:S(2)}) collective-permute-start(bf16[8,32,384]{2,1,0:T(8,128)(2,1)} %collective-permute-done), channel_id=1, source_target_pairs={{0,8},{8,16},{16,24},{24,32},{32,40},{40,48},{48,56},{56,0},{1,9},... | collective-permute-start | bytes 589832 | tf_op jit(solution)/shard_map/ppermute | solution.py:433
  46.7 8.4 %collective-permute-start.3 = (bf16[8,32,384]{2,1,0:T(8,128)(2,1)}, bf16[8,32,384]{2,1,0:T(8,128)(2,1)S(1)}, u32[]{:S(2)}, u32[]{:S(2)}) collective-permute-start(bf16[8,32,384]{2,1,0:T(8,128)(2,1)} %collective-permute-done.1), channel_id=1, source_target_pairs={{0,56},{8,0},{16,8},{24,16},{32,24},{40,32},{48,40},{56,48},{1,57}... | collective-permute-start | bytes 589832 | tf_op jit(solution)/shard_map/ppermute | solution.py:436
  52.9 7.9 %collective-permute-start.4 = (bf16[8,32,384]{2,1,0:T(8,128)(2,1)S(1)}, bf16[8,32,384]{2,1,0:T(8,128)(2,1)S(1)}, u32[]{:S(2)}, u32[]{:S(2)}) collective-permute-start(bf16[8,32,384]{2,1,0:T(8,128)(2,1)S(1)} %collective-permute-done.2), channel_id=1, source_target_pairs={{0,8},{8,16},{16,24},{24,32},{32,40},{40,48},{48,56},{56,0},{1,9},... | collective-permute-start | bytes 589832 | tf_op jit(solution)/shard_map/ppermute | solution.py:433
  55.1 7.5 %collective-permute-start.5 = (bf16[8,32,384]{2,1,0:T(8,128)(2,1)S(1)}, bf16[8,32,384]{2,1,0:T(8,128)(2,1)S(1)}, u32[]{:S(2)}, u32[]{:S(2)}) collective-permute-start(bf16[8,32,384]{2,1,0:T(8,128)(2,1)S(1)} %collective-permute-done.3), channel_id=1, source_target_pairs={{0,56},{8,0},{16,8},{24,16},{32,24},{40,32},{48,40},{56,48},{1,57}... | collective-permute-start | bytes 589832 | tf_op jit(solution)/shard_map/ppermute | solution.py:436
  63.3 29.4 %copy-start.20 = (f32[2,1]{0,1:T(1,128)S(1)}, f32[2,1]{0,1:T(1,128)}, u32[]{:S(2)}) copy-start(f32[2,1]{0,1:T(1,128)} %param.21) | copy-start | bytes 28
  64.5 29.3 %collective-permute-start.8 = (bf16[4,8,32,384]{3,2,1,0:T(8,128)(2,1)S(1)}, bf16[4,8,32,384]{3,2,1,0:T(8,128)(2,1)}, u32[]{:S(2)}, u32[]{:S(2)}) collective-permute-start(bf16[4,8,32,384]{3,2,1,0:T(8,128)(2,1)S(1)} %pad_maximum_fusion.refs_1_), channel_id=1, source_target_pairs={{0,4},{4,0},{1,5},{5,1},{2,6},{6,2},{3,7},{7,3},{8,12},{12,8},{9,1... | collective-permute-start | bytes 2359304 | tf_op jit(solution)/shard_map/ppermute | solution.py:443
  73.0 20.6 %collective-permute-start.7 = (bf16[3,8,32,384]{3,2,1,0:T(8,128)(2,1)S(1)}, bf16[3,8,32,384]{3,2,1,0:T(8,128)(2,1)}, u32[]{:S(2)}, u32[]{:S(2)}) collective-permute-start(bf16[3,8,32,384]{3,2,1,0:T(8,128)(2,1)S(1)} %pad_maximum_fusion.1.refs_0_), channel_id=1, source_target_pairs={{0,4},{4,0},{1,5},{5,1},{2,6},{6,2},{3,7},{7,3},{8,12},{12,8},{9,1... | collective-permute-start | bytes 1769480 | tf_op jit(solution)/shard_map/ppermute | solution.py:443
  75.6 14.3 %collective-permute-start.6 = (bf16[8,32,384]{2,1,0:T(8,128)(2,1)}, bf16[8,32,384]{2,1,0:T(8,128)(2,1)S(1)}, u32[]{:S(2)}, u32[]{:S(2)}) collective-permute-start(bf16[8,32,384]{2,1,0:T(8,128)(2,1)} %copy-done.9), channel_id=1, source_target_pairs={{0,8},{8,16},{16,24},{24,32},{32,40},{40,48},{48,56},{56,0},{1,9},... | collective-permute-start | bytes 589832 | tf_op jit(solution)/shard_map/ppermute | solution.py:433
  90.0 3.8 %collective-permute-start.9 = (bf16[1,8,32,384]{3,2,1,0:T(8,128)(2,1)S(1)}, bf16[1,8,32,384]{3,2,1,0:T(8,128)(2,1)S(1)}, u32[]{:S(2)}, u32[]{:S(2)}) collective-permute-start(bf16[1,8,32,384]{3,2,1,0:T(8,128)(2,1)S(1)} %bitcast.36), channel_id=1, source_target_pairs={{0,4},{4,0},{1,5},{5,1},{2,6},{6,2},{3,7},{7,3},{8,12},{12,8},{9,1... | collective-permute-start | bytes 589832 | tf_op jit(solution)/shard_map/ppermute | solution.py:443
  116.7 12.1 %all-to-all-start.2 = ((bf16[8,48,128]{2,1,0:T(8,128)(2,1)}), bf16[8,48,128]{2,1,0:T(8,128)(2,1)S(1)}, u32[]{:S(2)}, u32[]{:S(2)}) async-start(bf16[8,48,128]{2,1,0:T(8,128)(2,1)} %get-tuple-element.41), calls=%async_computation.2 | async-start | bytes 196608 | tf_op jit(solution)/shard_map/all_to_all | solution.py:27
  121.3 13.5 %collective-permute-start.10 = (bf16[1,4096]{1,0:T(2,128)(2,1)S(1)}, bf16[1,4096]{1,0:T(2,128)(2,1)S(1)}, u32[]{:S(2)}, u32[]{:S(2)}) collective-permute-start(bf16[1,4096]{1,0:T(2,128)(2,1)S(1)} %get-tuple-element.32), channel_id=1, source_target_pairs={{0,4},{4,8},{8,12},{12,16},{16,20},{20,24},{24,28},{28,32},{32,36}... | collective-permute-start | bytes 24584 | tf_op jit(solution)/shard_map/ppermute | solution.py:33
  123.2 11.6 %collective-permute-start.11 = (bf16[1,4096]{1,0:T(2,128)(2,1)S(1)}, bf16[1,4096]{1,0:T(2,128)(2,1)S(1)}, u32[]{:S(2)}, u32[]{:S(2)}) collective-permute-start(bf16[1,4096]{1,0:T(2,128)(2,1)S(1)} %get-tuple-element.33), channel_id=1, source_target_pairs={{4,0},{8,4},{12,8},{16,12},{20,16},{24,20},{28,24},{32,28},{36,32}... | collective-permute-start | bytes 24584 | tf_op jit(solution)/shard_map/ppermute | solution.py:34
  129.7 20.6 %all-to-all-start.3 = ((bf16[16,48,128]{2,1,0:T(8,128)(2,1)}), bf16[16,48,128]{2,1,0:T(8,128)(2,1)S(1)}, u32[]{:S(2)}, u32[]{:S(2)}) async-start(bf16[16,48,128]{2,1,0:T(8,128)(2,1)} %shard_map.150), calls=%async_computation.3 | async-start | bytes 393216 | tf_op jit(solution)/shard_map/all_to_all | solution.py:27
  143.8 8.1 %collective-permute-start.12 = (bf16[256,256]{1,0:T(8,128)(2,1)}, bf16[256,256]{1,0:T(8,128)(2,1)S(1)}, u32[]{:S(2)}, u32[]{:S(2)}) collective-permute-start(bf16[256,256]{1,0:T(8,128)(2,1)} %get-tuple-element.44.refs_0_), channel_id=1, source_target_pairs={{0,1},{1,2},{2,3},{3,0},{4,5},{5,6},{6,7},{7,4},{8,9},{9,10},{10,1... | collective-permute-start | bytes 393224 | tf_op jit(solution)/shard_map/ppermute | solution.py:509
  146.9 6.7 %collective-permute-start.13 = (bf16[256,256]{1,0:T(8,128)(2,1)}, bf16[256,256]{1,0:T(8,128)(2,1)S(1)}, u32[]{:S(2)}, u32[]{:S(2)}) collective-permute-start(bf16[256,256]{1,0:T(8,128)(2,1)} %get-tuple-element.44.refs_0_), channel_id=1, source_target_pairs={{0,3},{1,0},{2,1},{3,2},{4,7},{5,4},{6,5},{7,6},{8,11},{9,8},{10,9... | collective-permute-start | bytes 393224 | tf_op jit(solution)/shard_map/ppermute | solution.py:509
  156.2 19.7 %all-to-all-start.4 = ((bf16[4,256,256]{2,1,0:T(8,128)(2,1)}), bf16[4,256,256]{2,1,0:T(8,128)(2,1)S(1)}, u32[]{:S(2)}, u32[]{:S(2)}) async-start(bf16[4,256,256]{2,1,0:T(8,128)(2,1)} %shard_map.151), calls=%async_computation.4 | async-start | bytes 1048576 | tf_op jit(solution)/shard_map/all_to_all | solution.py:27
  160.2 10.7 %collective-permute-start.14 = (bf16[256,256]{1,0:T(8,128)(2,1)S(1)}, bf16[256,256]{1,0:T(8,128)(2,1)S(1)}, u32[]{:S(2)}, u32[]{:S(2)}) collective-permute-start(bf16[256,256]{1,0:T(8,128)(2,1)S(1)} %copy-done.12), channel_id=1, source_target_pairs={{0,2},{1,3},{2,0},{3,1},{4,6},{5,7},{6,4},{7,5},{8,10},{9,11},{10,... | collective-permute-start | bytes 393224 | tf_op jit(solution)/shard_map/ppermute | solution.py:509
  (17 other events, 224.3 us)
Sparse Core Ops, SparseCore 0:
  16.7 101.8 all-gather.1

commit v2 on v0

--- a/solution.py
+++ b/solution.py
@@ -63,21 +63,6 @@
 
 ARRIVAL = (0, -1, 1, -2, 2, -3, 3, -4)
 GROUPS = (3, 4, 1)
-
-
-def pack_kernel(query_ref, key_ref, value_ref, outer_ref, inner_ref, given_ref, out_ref, whole_ref, block_ref):
-    at = 0
-    for ref in (query_ref, inner_ref, given_ref, outer_ref):
-        whole_ref[:, at : at + ref.shape[1]] = ref[...]
-        at += ref.shape[1]
-    depth, columns = out_ref.shape
-    for side in range(2):
-        whole_ref[side * depth : (side + 1) * depth, at:] = out_ref[
-            :, side * columns // 2 : (side + 1) * columns // 2
-        ]
-    for z in range(block_ref.shape[0]):
-        block_ref[z, :, :DQK] = key_ref[...]
-        block_ref[z, :, DQK:] = value_ref[...]
 
 
 def gate_kernel(forget_ref, gate_ref, row_ref, column_ref, number_ref):
@@ -213,7 +198,7 @@
         start_ref[i, NORMERS:, :] = jnp.concatenate(rows, axis=0)
 
 
-def read_kernel(query_ref, key_ref, value_ref, column_ref, row_ref, gain_ref, start_ref, out_ref):
+def read_kernel(query_ref, key_ref, value_ref, column_ref, row_ref, gain_ref, conv_ref, start_ref, out_ref):
     length = query_ref.shape[0]
     queries = query_ref[...]
     values = value_ref[...]
@@ -252,11 +237,13 @@
     inverse_rms = lax.rsqrt(jnp.mean(summed * summed, axis=-1, keepdims=True) + EPS)
     out = (summed * inverse_rms * gain_ref[...]).astype(BF16)
     for k in range(out_ref.shape[0]):
-        out_ref[k] = out
+        out_ref[k, :, :DV] = out
+        out_ref[k, :, DV:] = conv_ref[...]
 
 
 WIDE = DQK + 3 * DV
 CHUNKS = 8
+AHEAD = 4
 
 
 def project_kernel(
@@ -270,10 +257,12 @@
             whole_ref.at[pl.ds(k * depth, depth), pl.ds(0, WIDE)], weight_ref.at[k], sems.at[k]
         )
 
-    for k in range(CHUNKS):
+    for k in range(AHEAD):
         fetch(k).start()
     for k in range(CHUNKS):
         fetch(k).wait()
+        if k + AHEAD < CHUNKS:
+            fetch(k + AHEAD).start()
         at = slice(k * depth, (k + 1) * depth)
         rows = jnp.concatenate([normed_ref[:, at], edge_ref[:, at]], axis=0)
         product = jnp.dot(rows, weight_ref[k], preferred_element_type=F32)
@@ -297,29 +286,29 @@
     conv_ref[...] = (outer * filtered).astype(BF16)
 
 
-def output_kernel(place_ref, lstm_ref, *refs):
-    parts, (whole_ref, out_ref, weight_ref, sems) = refs[:4], refs[4:]
-    place = place_ref[0]
-    sources = [(k * 32, lstm_ref.at[k]) for k in range(4)]
-    for part_ref, offset in zip(parts, (0, -1, 1, 2)):
-        sources.append(((place + offset + 4) % 4 * 32 + 16, part_ref))
-
-    def fetch(n, side):
+def output_kernel(joined_ref, whole_ref, out_ref, weight_ref, sems):
+    blocks = joined_ref.shape[0]
+    share = whole_ref.shape[0] // blocks
+
+    def fetch(n):
+        side, k = divmod(n, blocks)
         return pltpu.make_async_copy(
-            whole_ref.at[pl.ds(sources[n][0], 16), side, :, pl.ds(WIDE, 512)],
-            weight_ref.at[n, side],
-            sems.at[n, side],
-        )
-
-    for side in range(2):
-        for n in range(8):
-            fetch(n, side).start()
+            whole_ref.at[pl.ds(k * share, share), side, :, pl.ds(WIDE, 512)],
+            weight_ref.at[n],
+            sems.at[n],
+        )
+
+    for n in range(3):
+        fetch(n).start()
     for side in range(2):
         total = None
-        for n in range(8):
-            fetch(n, side).wait()
-            weight = weight_ref[n, side].reshape(DV, 512)
-            product = jnp.dot(sources[n][1][...], weight, preferred_element_type=F32)
+        for k in range(blocks):
+            n = side * blocks + k
+            fetch(n).wait()
+            if n + 3 < 2 * blocks:
+                fetch(n + 3).start()
+            weight = weight_ref[n].reshape(2 * DV, 512)
+            product = jnp.dot(joined_ref[k], weight, preferred_element_type=F32)
             total = product if total is None else total + product
         out_ref[:, side * 512 : (side + 1) * 512] = total.astype(BF16)
 
@@ -331,12 +320,13 @@
 def on_core(kernel, out, *operands, scalars=0, remote=0, scratch=(), limit=20):
     vmem = pl.BlockSpec(memory_space=pltpu.VMEM)
     smem = pl.BlockSpec(memory_space=pltpu.SMEM)
+    hbm = pl.BlockSpec(memory_space=pltpu.HBM)
     return pl.pallas_call(
         kernel,
         out_shape=out,
         in_specs=[smem] * scalars
         + [vmem] * (len(operands) - scalars - remote)
-        + [pl.BlockSpec(memory_space=pltpu.HBM)] * remote,
+        + [hbm] * remote,
         out_specs=jax.tree.map(lambda _: vmem, out),
         scratch_shapes=scratch,
         compiler_params=pltpu.CompilerParams(vmem_limit_bytes=limit * 2**20),
@@ -367,20 +357,10 @@
     plane = lax.axis_index("sp_0")
     depth = w_out.shape[0]
     half = w_out.shape[1] // 2
-    packed, block = on_core(
-        pack_kernel,
-        (
-            jax.ShapeDtypeStruct((w_key.shape[0], WIDE + half), BF16),
-            jax.ShapeDtypeStruct((planes, w_key.shape[0], DQK + DV), BF16),
-        ),
-        w_query,
-        w_key,
-        w_value,
-        w_conv_b,
-        w_conv_c,
-        w_conv_in,
-        w_out,
-    )
+    out_rows = jnp.concatenate([w_out[:, :half], w_out[:, half:]], axis=0)
+    packed = jnp.concatenate([w_query, w_conv_c, w_conv_in, w_conv_b, out_rows], axis=1)
+    block = jnp.concatenate([w_key, w_value], axis=1)
+    block = jnp.broadcast_to(block, (planes, *block.shape))
     block = swapped(block, "sp_0")
     whole = lax.all_gather(packed, SP, axis=0, tiled=True)
     core = lax.axis_index("sp_2")
@@ -465,38 +445,32 @@
         ],
         limit=54,
     )
-    far, queries, conv_out = lax.optimization_barrier((far, queries, conv_out))
     start = on_core(far_kernel, block, plane[None], near, far, scalars=1)
     start = swapped(start, PLANE)
-    parts = [conv_out] + [lax.ppermute(conv_out, "tp", ring(4, n)) for n in (1, -1, 2)]
-    start, *parts = lax.optimization_barrier((start, *parts))
-    lstm_out = on_core(
+    joined = on_core(
         read_kernel,
-        jax.ShapeDtypeStruct((4, length, DV), BF16),
+        jax.ShapeDtypeStruct((4, length, 2 * DV), BF16),
         queries,
         keys,
         values,
         columns,
         rows,
         head_gain[None],
+        conv_out,
         start,
     )
-    lstm_all = swapped(lstm_out, "tp")
-    whole = whole.reshape(size, 2, depth, -1)
+    joined = swapped(joined, "tp")
     return on_core(
         output_kernel,
         jax.ShapeDtypeStruct((length, 2 * half), BF16),
-        lax.axis_index("tp")[None],
-        lstm_all,
-        *parts,
-        whole,
-        scalars=1,
+        joined,
+        whole.reshape(size, 2, depth, -1),
         remote=1,
         scratch=[
-            pltpu.VMEM((8, 2, 16, depth, half), BF16),
-            pltpu.SemaphoreType.DMA((8, 2)),
+            pltpu.VMEM((8, size // 4, depth, half), BF16),
+            pltpu.SemaphoreType.DMA((8,)),
         ],
-        limit=58,
+        limit=53,
     )
 
 

time: 175 us -> 176 us (level)
  blocking collectives: 0 us -> 39.3 us
  starting transfers between devices: 81.3 us -> 58.6 us
  waiting for transfers between devices: 41.5 us -> 28 us
    all_to_all x0 -> x2, blocking collectives: none -> 39.3 us  [swapped(): return lax.all_to_all(value, axes, split_axis=0, concat_axis=0, tiled=True)]
    all_to_all x5 -> x3, starting transfers between devices: 30.3 us -> 18.3 us  [swapped(): return lax.all_to_all(value, axes, split_axis=0, concat_axis=0, tiled=True)]
    ppermute x3 -> x0, starting transfers between devices: 9.82 us -> none  [body(): lax.ppermute(conv_out, 'tp', ring(4, n))]
    all_to_all x5 -> x3, waiting for transfers between devices: 20.3 us -> 12.8 us  [swapped(): return lax.all_to_all(value, axes, split_axis=0, concat_axis=0, tiled=True)]
    ppermute x3 -> x0, waiting for transfers between devices: 4.49 us -> none  [body(): lax.ppermute(conv_out, 'tp', ring(4, n))]
    unnamed x58 -> x38, local copies, waits for them, and re-layouts: 8.78 us -> 5.94 us
    pallas_call x8 -> x7, Pallas kernels: 20.6 us -> 19.8 us  [on_core(): pl.pallas_call(kernel, out_shape=out, in_specs=[smem] * scalars + [vmem]...]
  transfers between devices with their start and end apart: 21 -> 16, of which waited for: 11 -> 9; matrix products, arithmetic and copies ran while one was open for 4% -> 5% of each run, Pallas kernels for 7% -> 7%
where the time goes in v2:
time: 176 us; the launch traced here: 175 us
  starting transfers between devices  58.6 us (33%)
  blocking collectives  39.3 us (22%)
  waiting for transfers between devices  28 us (16%)
  Pallas kernels  19.8 us (11%)
  between operations  13.8 us (8%)
  local copies, waits for them, and re-layouts  7.54 us (4%)
  other arithmetic  6.88 us (4%)
    all_to_all x2, blocking collectives, swapped(): return lax.all_to_all(value, axes, split_axis=0, concat_axis=0, tiled=True)  39.3 us
    pallas_call x7, Pallas kernels, on_core(): pl.pallas_call(kernel, out_shape=out, in_specs=[smem] * scalars + [vmem]...  19.8 us
    all_to_all x3, starting transfers between devices, swapped(): return lax.all_to_all(value, axes, split_axis=0, concat_axis=0, tiled=True)  18.3 us
    ppermute x4, waiting for transfers between devices, body(): up = lax.ppermute(up, 'sp_1', ring(8, 1))  14.2 us
    ppermute x3, starting transfers between devices, body(): groups.append(lax.ppermute(group, 'sp_2', ring(2, 1)))  13.6 us
    ppermute x3, starting transfers between devices, body(): down = lax.ppermute(down, 'sp_1', ring(8, -1))  12.9 us
    all_to_all x3, waiting for transfers between devices, swapped(): return lax.all_to_all(value, axes, split_axis=0, concat_axis=0, tiled=True)  12.8 us
    ppermute x4, starting transfers between devices, body(): up = lax.ppermute(up, 'sp_1', ring(8, 1))  9.42 us
  transfers between devices with their start and end apart: 16, of which 9 were waited for; matrix products, arithmetic and copies ran while one was open for 5% of the time, Pallas kernels for 7%

profile of v2, /device:TPU:1, one launch (start us, length us, event | category | flops | bytes accessed | tf_op | source)
XLA Modules:
  0.0 174.5 jit_solution(7839361973476178220)
XLA Ops:
  12.2 10.9 %all-to-all-start = ((bf16[8,32,384]{2,1,0:T(8,128)(2,1)}), bf16[8,32,384]{2,1,0:T(8,128)(2,1)S(1)}, u32[]{:S(2)}, u32[]{:S(2)}) async-start(bf16[8,32,384]{2,1,0:T(8,128)(2,1)} %broadcast_in_dim.14), calls=%async_computation | async-start | bytes 393216 | tf_op jit(solution)/shard_map/all_to_all | solution.py:27
  23.1 2.2 %fusion = f32[256]{0:T(256)S(1)} fusion(bf16[256,4096]{1,0:T(8,128)(2,1)} %param.15), kind=kLoop, calls=%fused_computation.2 | loop fusion | flops 3145472 | bytes 2098176 | tf_op jit(solution)/shard_map/reduce_sum | solution.py:22
  26.0 6.1 %all-to-all-done = bf16[8,32,384]{2,1,0:T(8,128)(2,1)S(1)} async-done(((bf16[8,32,384]{2,1,0:T(8,128)(2,1)}), bf16[8,32,384]{2,1,0:T(8,128)(2,1)S(1)}, u32[]{:S(2)}, u32[]{:S(2)}) %all-to-all-start) | async-done | bytes 196640 | tf_op jit(solution)/shard_map/all_to_all | solution.py:27
  32.1 3.2 %collective-permute-start = (bf16[8,32,384]{2,1,0:T(8,128)(2,1)S(1)}, bf16[8,32,384]{2,1,0:T(8,128)(2,1)}, u32[]{:S(2)}, u32[]{:S(2)}) collective-permute-start(bf16[8,32,384]{2,1,0:T(8,128)(2,1)S(1)} %all-to-all-done), channel_id=1, source_target_pairs={{0,8},{8,16},{16,24},{24,32},{32,40},{40,48},{48,56},{56,0},{1,9},... | collective-permute-start | bytes 589832 | tf_op jit(solution)/shard_map/ppermute | solution.py:374
  35.3 3.8 %collective-permute-start.1 = (bf16[8,32,384]{2,1,0:T(8,128)(2,1)S(1)}, bf16[8,32,384]{2,1,0:T(8,128)(2,1)}, u32[]{:S(2)}, u32[]{:S(2)}) collective-permute-start(bf16[8,32,384]{2,1,0:T(8,128)(2,1)S(1)} %all-to-all-done), channel_id=1, source_target_pairs={{0,56},{8,0},{16,8},{24,16},{32,24},{40,32},{48,40},{56,48},{1,57}... | collective-permute-start | bytes 589832 | tf_op jit(solution)/shard_map/ppermute | solution.py:377
  40.4 1.9 %collective-permute-start.2 = (bf16[8,32,384]{2,1,0:T(8,128)(2,1)}, bf16[8,32,384]{2,1,0:T(8,128)(2,1)S(1)}, u32[]{:S(2)}, u32[]{:S(2)}) collective-permute-start(bf16[8,32,384]{2,1,0:T(8,128)(2,1)} %collective-permute-done), channel_id=1, source_target_pairs={{0,8},{8,16},{16,24},{24,32},{32,40},{40,48},{48,56},{56,0},{1,9},... | collective-permute-start | bytes 589832 | tf_op jit(solution)/shard_map/ppermute | solution.py:374
  42.4 4.5 %collective-permute-start.3 = (bf16[8,32,384]{2,1,0:T(8,128)(2,1)}, bf16[8,32,384]{2,1,0:T(8,128)(2,1)S(1)}, u32[]{:S(2)}, u32[]{:S(2)}) collective-permute-start(bf16[8,32,384]{2,1,0:T(8,128)(2,1)} %collective-permute-done.1), channel_id=1, source_target_pairs={{0,56},{8,0},{16,8},{24,16},{32,24},{40,32},{48,40},{56,48},{1,57}... | collective-permute-start | bytes 589832 | tf_op jit(solution)/shard_map/ppermute | solution.py:377
  50.4 4.6 %collective-permute-start.5 = (bf16[8,32,384]{2,1,0:T(8,128)(2,1)S(1)}, bf16[8,32,384]{2,1,0:T(8,128)(2,1)S(1)}, u32[]{:S(2)}, u32[]{:S(2)}) collective-permute-start(bf16[8,32,384]{2,1,0:T(8,128)(2,1)S(1)} %collective-permute-done.3), channel_id=1, source_target_pairs={{0,56},{8,0},{16,8},{24,16},{32,24},{40,32},{48,40},{56,48},{1,57}... | collective-permute-start | bytes 589832 | tf_op jit(solution)/shard_map/ppermute | solution.py:377
  59.5 8.0 %collective-permute-start.8 = (bf16[4,8,32,384]{3,2,1,0:T(8,128)(2,1)S(1)}, bf16[4,8,32,384]{3,2,1,0:T(8,128)(2,1)}, u32[]{:S(2)}, u32[]{:S(2)}) collective-permute-start(bf16[4,8,32,384]{3,2,1,0:T(8,128)(2,1)S(1)} %pad_maximum_fusion.refs_1_), channel_id=1, source_target_pairs={{0,4},{4,0},{1,5},{5,1},{2,6},{6,2},{3,7},{7,3},{8,12},{12,8},{9,1... | collective-permute-start | bytes 2359304 | tf_op jit(solution)/shard_map/ppermute | solution.py:384
  68.7 1.9 %collective-permute-start.7 = (bf16[3,8,32,384]{3,2,1,0:T(8,128)(2,1)S(1)}, bf16[3,8,32,384]{3,2,1,0:T(8,128)(2,1)}, u32[]{:S(2)}, u32[]{:S(2)}) collective-permute-start(bf16[3,8,32,384]{3,2,1,0:T(8,128)(2,1)S(1)} %pad_maximum_fusion.1.refs_0_), channel_id=1, source_target_pairs={{0,4},{4,0},{1,5},{5,1},{2,6},{6,2},{3,7},{7,3},{8,12},{12,8},{9,1... | collective-permute-start | bytes 1769480 | tf_op jit(solution)/shard_map/ppermute | solution.py:384
  71.3 2.4 %collective-permute-start.6 = (bf16[8,32,384]{2,1,0:T(8,128)(2,1)}, bf16[8,32,384]{2,1,0:T(8,128)(2,1)S(1)}, u32[]{:S(2)}, u32[]{:S(2)}) collective-permute-start(bf16[8,32,384]{2,1,0:T(8,128)(2,1)} %collective-permute-done.4), channel_id=1, source_target_pairs={{0,8},{8,16},{16,24},{24,32},{32,40},{40,48},{48,56},{56,0},{1,9},... | collective-permute-start | bytes 589832 | tf_op jit(solution)/shard_map/ppermute | solution.py:374
  73.7 9.7 %collective-permute-done.6 = bf16[8,32,384]{2,1,0:T(8,128)(2,1)S(1)} collective-permute-done((bf16[8,32,384]{2,1,0:T(8,128)(2,1)}, bf16[8,32,384]{2,1,0:T(8,128)(2,1)S(1)}, u32[]{:S(2)}, u32[]{:S(2)}) %collective-permute-start.6) | collective-permute-done | bytes 196640 | tf_op jit(solution)/shard_map/ppermute | solution.py:374
  83.4 3.7 %collective-permute-start.9 = (bf16[1,8,32,384]{3,2,1,0:T(8,128)(2,1)S(1)}, bf16[1,8,32,384]{3,2,1,0:T(8,128)(2,1)S(1)}, u32[]{:S(2)}, u32[]{:S(2)}) collective-permute-start(bf16[1,8,32,384]{3,2,1,0:T(8,128)(2,1)S(1)} %bitcast.35), channel_id=1, source_target_pairs={{0,4},{4,0},{1,5},{5,1},{2,6},{6,2},{3,7},{7,3},{8,12},{12,8},{9,1... | collective-permute-start | bytes 589832 | tf_op jit(solution)/shard_map/ppermute | solution.py:384
  88.1 3.2 %shard_map.146 = (bf16[16,48,128]{2,1,0:T(8,128)(2,1)S(1)}, bf16[256,128]{1,0:T(8,128)(2,1)S(1)}, bf16[256,256]{1,0:T(8,128)(2,1)S(1)}) custom-call(s32[2]{0:T(128)S(1)} %pad_add_fusion.place_ref, bf16[256,4096]{1,0:T(8,128)(2,1)S(1)} %fusion.2.normed_ref, f32[256,8]{1,0:T(8,128)S(1)} %get-tuple-element.21.update_ref.column_ref, ...), custom_call_target="tpu_custom_call" | custom-call | tf_op jit(solution)/shard_map/pallas_call | solution.py:324
  91.3 20.4 %all_to_all.25.state_ref = bf16[16,48,128]{2,1,0:T(8,128)(2,1)S(1)} all-to-all(bf16[16,48,128]{2,1,0:T(8,128)(2,1)S(1)} %get-tuple-element.32), channel_id=1, replica_groups=mesh['sp_0'=8,'sp_1'=8,'sp_2'=2,'tp'=4] {'sp_1','sp_2'}, dimensions={0} | all-to-all | bytes 393216 | tf_op jit(solution)/shard_map/all_to_all | solution.py:27
  112.5 3.7 %all-to-all-start.2 = ((bf16[8,48,128]{2,1,0:T(8,128)(2,1)}), bf16[8,48,128]{2,1,0:T(8,128)(2,1)S(1)}, u32[]{:S(2)}, u32[]{:S(2)}) async-start(bf16[8,48,128]{2,1,0:T(8,128)(2,1)} %get-tuple-element.34), calls=%async_computation.2 | async-start | bytes 196608 | tf_op jit(solution)/shard_map/all_to_all | solution.py:27
  116.3 1.9 %collective-permute-start.10 = (bf16[1,4096]{1,0:T(2,128)(2,1)S(1)}, bf16[1,4096]{1,0:T(2,128)(2,1)S(1)}, u32[]{:S(2)}, u32[]{:S(2)}) collective-permute-start(bf16[1,4096]{1,0:T(2,128)(2,1)S(1)} %get-tuple-element.25), channel_id=1, source_target_pairs={{0,4},{4,8},{8,12},{12,16},{16,20},{20,24},{24,28},{28,32},{32,36}... | collective-permute-start | bytes 24584 | tf_op jit(solution)/shard_map/ppermute | solution.py:33
  118.2 2.4 %collective-permute-start.11 = (bf16[1,4096]{1,0:T(2,128)(2,1)S(1)}, bf16[1,4096]{1,0:T(2,128)(2,1)S(1)}, u32[]{:S(2)}, u32[]{:S(2)}) collective-permute-start(bf16[1,4096]{1,0:T(2,128)(2,1)S(1)} %get-tuple-element.26), channel_id=1, source_target_pairs={{4,0},{8,4},{12,8},{16,12},{20,16},{24,20},{28,24},{32,28},{36,32}... | collective-permute-start | bytes 24584 | tf_op jit(solution)/shard_map/ppermute | solution.py:34
  120.7 4.4 %all-to-all-done.2.planes_ref = bf16[8,48,128]{2,1,0:T(8,128)(2,1)S(1)} async-done(((bf16[8,48,128]{2,1,0:T(8,128)(2,1)}), bf16[8,48,128]{2,1,0:T(8,128)(2,1)S(1)}, u32[]{:S(2)}, u32[]{:S(2)}) %all-to-all-start.2) | async-done | bytes 98336 | tf_op jit(solution)/shard_map/all_to_all | solution.py:27
  126.1 3.7 %all-to-all-start.3 = ((bf16[16,48,128]{2,1,0:T(8,128)(2,1)}), bf16[16,48,128]{2,1,0:T(8,128)(2,1)S(1)}, u32[]{:S(2)}, u32[]{:S(2)}) async-start(bf16[16,48,128]{2,1,0:T(8,128)(2,1)} %shard_map.149), calls=%async_computation.3 | async-start | bytes 393216 | tf_op jit(solution)/shard_map/all_to_all | solution.py:27
  130.6 7.2 %shard_map.147 = (bf16[256,128]{1,0:T(8,128)(2,1)}, bf16[256,256]{1,0:T(8,128)(2,1)}) custom-call(bf16[256,4096]{1,0:T(8,128)(2,1)} %copy-done, bf16[16,4096]{1,0:T(8,128)(2,1)} %maximum_maximum_fusion.edge_ref, bf16[3,256]{1,0:T(4,128)(2,1)} %tap_ref.1, bf16[4096,1408]{1,0:T(8,128)(2,1)} %all-gather.2.cloned.1.call-done.whole_ref), custom_call_target="tpu_custom_call" | custom-call | tf_op jit(solution)/shard_map/pallas_call | solution.py:324
  137.8 2.3 %all-to-all-done.3.start_ref = bf16[16,48,128]{2,1,0:T(8,128)(2,1)S(1)} async-done(((bf16[16,48,128]{2,1,0:T(8,128)(2,1)}), bf16[16,48,128]{2,1,0:T(8,128)(2,1)S(1)}, u32[]{:S(2)}, u32[]{:S(2)}) %all-to-all-start.3) | async-done | bytes 196640 | tf_op jit(solution)/shard_map/all_to_all | solution.py:27
  142.8 18.9 %all_to_all.26.joined_ref = bf16[4,256,512]{2,1,0:T(8,128)(2,1)} all-to-all(bf16[4,256,512]{2,1,0:T(8,128)(2,1)S(1)} %shard_map.150), channel_id=1, replica_groups=mesh['sp_0'=8,'sp_1'=8,'sp_2'=2,'tp'=4] {'tp'}, dimensions={0} | all-to-all | bytes 2097152 | tf_op jit(solution)/shard_map/all_to_all | solution.py:27
  161.7 6.0 %shard_map.151 = bf16[256,1024]{1,0:T(8,128)(2,1)} custom-call(bf16[4,256,512]{2,1,0:T(8,128)(2,1)} %all_to_all.26.joined_ref, bf16[128,2,16,1408]{3,2,1,0:T(8,128)(2,1)} %bitcast.38), custom_call_target="tpu_custom_call" | custom-call | tf_op jit(solution)/shard_map/pallas_call | solution.py:324
  (75 shorter events, 23.7 us)
Async XLA Ops:
  6.5 18.8 %copy-start.13 = (f32[4096]{0:T(1024)S(1)}, f32[4096]{0:T(1024)}, u32[]{:S(2)}) copy-start(f32[4096]{0:T(1024)} %param.16) | copy-start | bytes 49156
  6.5 124.0 %all-gather.2.cloned.1.call-start = ((), (), s32[]{:S(2)}) async-start(), calls=%async_computation.5 | async-start | bytes 11624448 | tf_op jit(solution)/shard_map/all_gather | solution.py:365
  12.2 19.8 %all-to-all-start = ((bf16[8,32,384]{2,1,0:T(8,128)(2,1)}), bf16[8,32,384]{2,1,0:T(8,128)(2,1)S(1)}, u32[]{:S(2)}, u32[]{:S(2)}) async-start(bf16[8,32,384]{2,1,0:T(8,128)(2,1)} %broadcast_in_dim.14), calls=%async_computation | async-start | bytes 393216 | tf_op jit(solution)/shard_map/all_to_all | solution.py:27
  25.3 29.7 %copy-start.12 = (bf16[4096,2,2,1]{0,2,3,1:T(2,128)(2,1)S(1)}, bf16[4096,2,2,1]{0,2,3,1:T(2,128)(2,1)}, u32[]{:S(2)}) copy-start(bf16[4096,2,2,1]{0,2,3,1:T(2,128)(2,1)} %param.20) | copy-start | bytes 98308
  26.0 90.3 %copy-start = (bf16[256,4096]{1,0:T(8,128)(2,1)}, bf16[256,4096]{1,0:T(8,128)(2,1)S(1)}, u32[]{:S(2)}) copy-start(bf16[256,4096]{1,0:T(8,128)(2,1)S(1)} %fusion.2.normed_ref) | copy-start | bytes 6291460
  32.1 35.4 %copy-start.9 = (bf16[8,32,384]{2,1,0:T(8,128)(2,1)}, bf16[8,32,384]{2,1,0:T(8,128)(2,1)S(1)}, u32[]{:S(2)}) copy-start(bf16[8,32,384]{2,1,0:T(8,128)(2,1)S(1)} %all-to-all-done) | copy-start | bytes 589828
  32.1 8.4 %collective-permute-start = (bf16[8,32,384]{2,1,0:T(8,128)(2,1)S(1)}, bf16[8,32,384]{2,1,0:T(8,128)(2,1)}, u32[]{:S(2)}, u32[]{:S(2)}) collective-permute-start(bf16[8,32,384]{2,1,0:T(8,128)(2,1)S(1)} %all-to-all-done), channel_id=1, source_target_pairs={{0,8},{8,16},{16,24},{24,32},{32,40},{40,48},{48,56},{56,0},{1,9},... | collective-permute-start | bytes 589832 | tf_op jit(solution)/shard_map/ppermute | solution.py:374
  35.3 7.1 %collective-permute-start.1 = (bf16[8,32,384]{2,1,0:T(8,128)(2,1)S(1)}, bf16[8,32,384]{2,1,0:T(8,128)(2,1)}, u32[]{:S(2)}, u32[]{:S(2)}) collective-permute-start(bf16[8,32,384]{2,1,0:T(8,128)(2,1)S(1)} %all-to-all-done), channel_id=1, source_target_pairs={{0,56},{8,0},{16,8},{24,16},{32,24},{40,32},{48,40},{56,48},{1,57}... | collective-permute-start | bytes 589832 | tf_op jit(solution)/shard_map/ppermute | solution.py:377
  40.4 8.1 %collective-permute-start.2 = (bf16[8,32,384]{2,1,0:T(8,128)(2,1)}, bf16[8,32,384]{2,1,0:T(8,128)(2,1)S(1)}, u32[]{:S(2)}, u32[]{:S(2)}) collective-permute-start(bf16[8,32,384]{2,1,0:T(8,128)(2,1)} %collective-permute-done), channel_id=1, source_target_pairs={{0,8},{8,16},{16,24},{24,32},{32,40},{40,48},{48,56},{56,0},{1,9},... | collective-permute-start | bytes 589832 | tf_op jit(solution)/shard_map/ppermute | solution.py:374
  42.4 8.0 %collective-permute-start.3 = (bf16[8,32,384]{2,1,0:T(8,128)(2,1)}, bf16[8,32,384]{2,1,0:T(8,128)(2,1)S(1)}, u32[]{:S(2)}, u32[]{:S(2)}) collective-permute-start(bf16[8,32,384]{2,1,0:T(8,128)(2,1)} %collective-permute-done.1), channel_id=1, source_target_pairs={{0,56},{8,0},{16,8},{24,16},{32,24},{40,32},{48,40},{56,48},{1,57}... | collective-permute-start | bytes 589832 | tf_op jit(solution)/shard_map/ppermute | solution.py:377
  48.5 8.3 %collective-permute-start.4 = (bf16[8,32,384]{2,1,0:T(8,128)(2,1)S(1)}, bf16[8,32,384]{2,1,0:T(8,128)(2,1)}, u32[]{:S(2)}, u32[]{:S(2)}) collective-permute-start(bf16[8,32,384]{2,1,0:T(8,128)(2,1)S(1)} %collective-permute-done.2), channel_id=1, source_target_pairs={{0,8},{8,16},{16,24},{24,32},{32,40},{40,48},{48,56},{56,0},{1,9},... | collective-permute-start | bytes 589832 | tf_op jit(solution)/shard_map/ppermute | solution.py:374
  50.4 7.2 %collective-permute-start.5 = (bf16[8,32,384]{2,1,0:T(8,128)(2,1)S(1)}, bf16[8,32,384]{2,1,0:T(8,128)(2,1)S(1)}, u32[]{:S(2)}, u32[]{:S(2)}) collective-permute-start(bf16[8,32,384]{2,1,0:T(8,128)(2,1)S(1)} %collective-permute-done.3), channel_id=1, source_target_pairs={{0,56},{8,0},{16,8},{24,16},{32,24},{40,32},{48,40},{56,48},{1,57}... | collective-permute-start | bytes 589832 | tf_op jit(solution)/shard_map/ppermute | solution.py:377
  58.3 28.8 %copy-start.14 = (f32[2,256,1]{1,2,0:T(1,128)S(1)}, f32[2,256,1]{1,2,0:T(1,128)}, u32[]{:S(2)}) copy-start(f32[2,256,1]{1,2,0:T(1,128)} %param.23) | copy-start | bytes 6148
  58.3 28.8 %copy-start.15 = (f32[2,1]{0,1:T(1,128)S(1)}, f32[2,1]{0,1:T(1,128)}, u32[]{:S(2)}) copy-start(f32[2,1]{0,1:T(1,128)} %param.22) | copy-start | bytes 28
  58.3 28.8 %copy-start.16 = (f32[2,1]{0,1:T(1,128)S(1)}, f32[2,1]{0,1:T(1,128)}, u32[]{:S(2)}) copy-start(f32[2,1]{0,1:T(1,128)} %param.21) | copy-start | bytes 28
  59.5 28.6 %collective-permute-start.8 = (bf16[4,8,32,384]{3,2,1,0:T(8,128)(2,1)S(1)}, bf16[4,8,32,384]{3,2,1,0:T(8,128)(2,1)}, u32[]{:S(2)}, u32[]{:S(2)}) collective-permute-start(bf16[4,8,32,384]{3,2,1,0:T(8,128)(2,1)S(1)} %pad_maximum_fusion.refs_1_), channel_id=1, source_target_pairs={{0,4},{4,0},{1,5},{5,1},{2,6},{6,2},{3,7},{7,3},{8,12},{12,8},{9,1... | collective-permute-start | bytes 2359304 | tf_op jit(solution)/shard_map/ppermute | solution.py:384
  68.7 19.3 %collective-permute-start.7 = (bf16[3,8,32,384]{3,2,1,0:T(8,128)(2,1)S(1)}, bf16[3,8,32,384]{3,2,1,0:T(8,128)(2,1)}, u32[]{:S(2)}, u32[]{:S(2)}) collective-permute-start(bf16[3,8,32,384]{3,2,1,0:T(8,128)(2,1)S(1)} %pad_maximum_fusion.1.refs_0_), channel_id=1, source_target_pairs={{0,4},{4,0},{1,5},{5,1},{2,6},{6,2},{3,7},{7,3},{8,12},{12,8},{9,1... | collective-permute-start | bytes 1769480 | tf_op jit(solution)/shard_map/ppermute | solution.py:384
  71.3 12.1 %collective-permute-start.6 = (bf16[8,32,384]{2,1,0:T(8,128)(2,1)}, bf16[8,32,384]{2,1,0:T(8,128)(2,1)S(1)}, u32[]{:S(2)}, u32[]{:S(2)}) collective-permute-start(bf16[8,32,384]{2,1,0:T(8,128)(2,1)} %collective-permute-done.4), channel_id=1, source_target_pairs={{0,8},{8,16},{16,24},{24,32},{32,40},{40,48},{48,56},{56,0},{1,9},... | collective-permute-start | bytes 589832 | tf_op jit(solution)/shard_map/ppermute | solution.py:374
  83.4 4.7 %collective-permute-start.9 = (bf16[1,8,32,384]{3,2,1,0:T(8,128)(2,1)S(1)}, bf16[1,8,32,384]{3,2,1,0:T(8,128)(2,1)S(1)}, u32[]{:S(2)}, u32[]{:S(2)}) collective-permute-start(bf16[1,8,32,384]{3,2,1,0:T(8,128)(2,1)S(1)} %bitcast.35), channel_id=1, source_target_pairs={{0,4},{4,0},{1,5},{5,1},{2,6},{6,2},{3,7},{7,3},{8,12},{12,8},{9,1... | collective-permute-start | bytes 589832 | tf_op jit(solution)/shard_map/ppermute | solution.py:384
  91.3 21.3 %copy-start.3 = (bf16[256,256]{1,0:T(8,128)(2,1)}, bf16[256,256]{1,0:T(8,128)(2,1)S(1)}, u32[]{:S(2)}) copy-start(bf16[256,256]{1,0:T(8,128)(2,1)S(1)} %get-tuple-element.29.value_ref) | copy-start | bytes 393220
  112.5 12.6 %all-to-all-start.2 = ((bf16[8,48,128]{2,1,0:T(8,128)(2,1)}), bf16[8,48,128]{2,1,0:T(8,128)(2,1)S(1)}, u32[]{:S(2)}, u32[]{:S(2)}) async-start(bf16[8,48,128]{2,1,0:T(8,128)(2,1)} %get-tuple-element.34), calls=%async_computation.2 | async-start | bytes 196608 | tf_op jit(solution)/shard_map/all_to_all | solution.py:27
  116.3 13.5 %collective-permute-start.10 = (bf16[1,4096]{1,0:T(2,128)(2,1)S(1)}, bf16[1,4096]{1,0:T(2,128)(2,1)S(1)}, u32[]{:S(2)}, u32[]{:S(2)}) collective-permute-start(bf16[1,4096]{1,0:T(2,128)(2,1)S(1)} %get-tuple-element.25), channel_id=1, source_target_pairs={{0,4},{4,8},{8,12},{12,16},{16,20},{20,24},{24,28},{28,32},{32,36}... | collective-permute-start | bytes 24584 | tf_op jit(solution)/shard_map/ppermute | solution.py:33
  118.2 11.6 %collective-permute-start.11 = (bf16[1,4096]{1,0:T(2,128)(2,1)S(1)}, bf16[1,4096]{1,0:T(2,128)(2,1)S(1)}, u32[]{:S(2)}, u32[]{:S(2)}) collective-permute-start(bf16[1,4096]{1,0:T(2,128)(2,1)S(1)} %get-tuple-element.26), channel_id=1, source_target_pairs={{4,0},{8,4},{12,8},{16,12},{20,16},{24,20},{28,24},{32,28},{36,32}... | collective-permute-start | bytes 24584 | tf_op jit(solution)/shard_map/ppermute | solution.py:34
  126.1 14.0 %all-to-all-start.3 = ((bf16[16,48,128]{2,1,0:T(8,128)(2,1)}), bf16[16,48,128]{2,1,0:T(8,128)(2,1)S(1)}, u32[]{:S(2)}, u32[]{:S(2)}) async-start(bf16[16,48,128]{2,1,0:T(8,128)(2,1)} %shard_map.149), calls=%async_computation.3 | async-start | bytes 393216 | tf_op jit(solution)/shard_map/all_to_all | solution.py:27
  (9 other events, 37.2 us)
Sparse Core Ops, SparseCore 0:
  10.9 102.2 all-gather.1

commit v3 on v0

--- a/solution.py
+++ b/solution.py
@@ -213,7 +213,7 @@
         start_ref[i, NORMERS:, :] = jnp.concatenate(rows, axis=0)
 
 
-def read_kernel(query_ref, key_ref, value_ref, column_ref, row_ref, gain_ref, start_ref, out_ref):
+def read_kernel(query_ref, key_ref, value_ref, column_ref, row_ref, gain_ref, conv_ref, start_ref, out_ref):
     length = query_ref.shape[0]
     queries = query_ref[...]
     values = value_ref[...]
@@ -252,11 +252,13 @@
     inverse_rms = lax.rsqrt(jnp.mean(summed * summed, axis=-1, keepdims=True) + EPS)
     out = (summed * inverse_rms * gain_ref[...]).astype(BF16)
     for k in range(out_ref.shape[0]):
-        out_ref[k] = out
+        out_ref[k, :, :DV] = out
+        out_ref[k, :, DV:] = conv_ref[...]
 
 
 WIDE = DQK + 3 * DV
 CHUNKS = 8
+AHEAD = 4
 
 
 def project_kernel(
@@ -267,16 +269,18 @@
 
     def fetch(k):
         return pltpu.make_async_copy(
-            whole_ref.at[pl.ds(k * depth, depth), pl.ds(0, WIDE)], weight_ref.at[k], sems.at[k]
+            whole_ref.at[pl.ds(k * depth, depth)], weight_ref.at[k], sems.at[k]
         )
 
-    for k in range(CHUNKS):
+    for k in range(AHEAD):
         fetch(k).start()
     for k in range(CHUNKS):
         fetch(k).wait()
+        if k + AHEAD < CHUNKS:
+            fetch(k + AHEAD).start()
         at = slice(k * depth, (k + 1) * depth)
         rows = jnp.concatenate([normed_ref[:, at], edge_ref[:, at]], axis=0)
-        product = jnp.dot(rows, weight_ref[k], preferred_element_type=F32)
+        product = jnp.dot(rows, weight_ref[k, :, :WIDE], preferred_element_type=F32)
         if k:
             total_ref[...] += product
         else:
@@ -297,29 +301,11 @@
     conv_ref[...] = (outer * filtered).astype(BF16)
 
 
-def output_kernel(place_ref, lstm_ref, *refs):
-    parts, (whole_ref, out_ref, weight_ref, sems) = refs[:4], refs[4:]
-    place = place_ref[0]
-    sources = [(k * 32, lstm_ref.at[k]) for k in range(4)]
-    for part_ref, offset in zip(parts, (0, -1, 1, 2)):
-        sources.append(((place + offset + 4) % 4 * 32 + 16, part_ref))
-
-    def fetch(n, side):
-        return pltpu.make_async_copy(
-            whole_ref.at[pl.ds(sources[n][0], 16), side, :, pl.ds(WIDE, 512)],
-            weight_ref.at[n, side],
-            sems.at[n, side],
-        )
-
-    for side in range(2):
-        for n in range(8):
-            fetch(n, side).start()
-    for side in range(2):
+def output_kernel(joined_ref, left_ref, right_ref, out_ref):
+    for side, weight_ref in enumerate((left_ref, right_ref)):
         total = None
-        for n in range(8):
-            fetch(n, side).wait()
-            weight = weight_ref[n, side].reshape(DV, 512)
-            product = jnp.dot(sources[n][1][...], weight, preferred_element_type=F32)
+        for k in range(joined_ref.shape[0]):
+            product = jnp.dot(joined_ref[k], weight_ref[k], preferred_element_type=F32)
             total = product if total is None else total + product
         out_ref[:, side * 512 : (side + 1) * 512] = total.astype(BF16)
 
@@ -331,12 +317,13 @@
 def on_core(kernel, out, *operands, scalars=0, remote=0, scratch=(), limit=20):
     vmem = pl.BlockSpec(memory_space=pltpu.VMEM)
     smem = pl.BlockSpec(memory_space=pltpu.SMEM)
+    hbm = pl.BlockSpec(memory_space=pltpu.HBM)
     return pl.pallas_call(
         kernel,
         out_shape=out,
         in_specs=[smem] * scalars
         + [vmem] * (len(operands) - scalars - remote)
-        + [pl.BlockSpec(memory_space=pltpu.HBM)] * remote,
+        + [hbm] * remote,
         out_specs=jax.tree.map(lambda _: vmem, out),
         scratch_shapes=scratch,
         compiler_params=pltpu.CompilerParams(vmem_limit_bytes=limit * 2**20),
@@ -380,6 +367,7 @@
         w_conv_c,
         w_conv_in,
         w_out,
+        limit=63,
     )
     block = swapped(block, "sp_0")
     whole = lax.all_gather(packed, SP, axis=0, tiled=True)
@@ -459,44 +447,33 @@
         whole,
         remote=1,
         scratch=[
-            pltpu.VMEM((CHUNKS, whole.shape[0] // CHUNKS, WIDE), BF16),
+            pltpu.VMEM((CHUNKS, whole.shape[0] // CHUNKS, whole.shape[1]), BF16),
             pltpu.VMEM((length + edges.shape[0], WIDE), F32),
             pltpu.SemaphoreType.DMA((CHUNKS,)),
         ],
-        limit=54,
-    )
-    far, queries, conv_out = lax.optimization_barrier((far, queries, conv_out))
+        limit=50,
+    )
     start = on_core(far_kernel, block, plane[None], near, far, scalars=1)
     start = swapped(start, PLANE)
-    parts = [conv_out] + [lax.ppermute(conv_out, "tp", ring(4, n)) for n in (1, -1, 2)]
-    start, *parts = lax.optimization_barrier((start, *parts))
-    lstm_out = on_core(
+    joined = on_core(
         read_kernel,
-        jax.ShapeDtypeStruct((4, length, DV), BF16),
+        jax.ShapeDtypeStruct((4, length, 2 * DV), BF16),
         queries,
         keys,
         values,
         columns,
         rows,
         head_gain[None],
+        conv_out,
         start,
     )
-    lstm_all = swapped(lstm_out, "tp")
-    whole = whole.reshape(size, 2, depth, -1)
+    joined = swapped(joined, "tp")
+    sides = whole[:, WIDE:].reshape(size, 2, depth, half)
     return on_core(
         output_kernel,
         jax.ShapeDtypeStruct((length, 2 * half), BF16),
-        lax.axis_index("tp")[None],
-        lstm_all,
-        *parts,
-        whole,
-        scalars=1,
-        remote=1,
-        scratch=[
-            pltpu.VMEM((8, 2, 16, depth, half), BF16),
-            pltpu.SemaphoreType.DMA((8, 2)),
-        ],
-        limit=58,
+        joined,
+        *(sides[:, side].reshape(4, 2 * DV, half) for side in range(2)),
     )
 
 

time: 175 us -> 168 us (0.960)
  starting transfers between devices: 81.3 us -> 61.7 us
  blocking collectives: 0 us -> 19.3 us
  Pallas kernels: 20.6 us -> 16.6 us
  local copies, waits for them, and re-layouts: 8.93 us -> 6.48 us
    all_to_all x0 -> x1, blocking collectives: none -> 19.3 us  [swapped(): return lax.all_to_all(value, axes, split_axis=0, concat_axis=0, tiled=True)]
    ppermute x3 -> x0, starting transfers between devices: 9.82 us -> none  [body(): lax.ppermute(conv_out, 'tp', ring(4, n))]
    all_to_all x5 -> x4, starting transfers between devices: 30.3 us -> 21.9 us  [swapped(): return lax.all_to_all(value, axes, split_axis=0, concat_axis=0, tiled=True)]
    unnamed x58 -> x40, local copies, waits for them, and re-layouts: 8.78 us -> 2.35 us
    all_to_all x5 -> x4, waiting for transfers between devices: 20.3 us -> 26.4 us  [swapped(): return lax.all_to_all(value, axes, split_axis=0, concat_axis=0, tiled=True)]
    ppermute x3 -> x0, waiting for transfers between devices: 4.49 us -> none  [body(): lax.ppermute(conv_out, 'tp', ring(4, n))]
    pallas_call x8, Pallas kernels: 20.6 us -> 16.6 us  [on_core(): pl.pallas_call(kernel, out_shape=out, in_specs=[smem] * scalars + [vmem]...]
    slice x0 -> x3, local copies, waits for them, and re-layouts: none -> 3.98 us  [the longest x2 2.19 us: body(): sides = whole[:, WIDE:].reshape(size, 2, depth, half)]
  transfers between devices with their start and end apart: 21 -> 17, of which waited for: 11 -> 10; matrix products, arithmetic and copies ran while one was open for 4% -> 5% of each run, Pallas kernels for 7% -> 7%
where the time goes in v3:
time: 168 us; the launch traced here: 167 us
  starting transfers between devices  61.7 us (37%)
  waiting for transfers between devices  43.2 us (26%)
  blocking collectives  19.3 us (11%)
  Pallas kernels  16.6 us (10%)
  between operations  13.8 us (8%)
  local copies, waits for them, and re-layouts  6.48 us (4%)
  other arithmetic  5.7 us (3%)
    all_to_all x4, waiting for transfers between devices, swapped(): return lax.all_to_all(value, axes, split_axis=0, concat_axis=0, tiled=True)  26.4 us
    all_to_all x4, starting transfers between devices, swapped(): return lax.all_to_all(value, axes, split_axis=0, concat_axis=0, tiled=True)  21.9 us
    all_to_all x1, blocking collectives, swapped(): return lax.all_to_all(value, axes, split_axis=0, concat_axis=0, tiled=True)  19.3 us
    pallas_call x8, Pallas kernels, on_core(): pl.pallas_call(kernel, out_shape=out, in_specs=[smem] * scalars + [vmem]...  16.6 us
    ppermute x4, waiting for transfers between devices, body(): up = lax.ppermute(up, 'sp_1', ring(8, 1))  15.7 us
    ppermute x3, starting transfers between devices, body(): down = lax.ppermute(down, 'sp_1', ring(8, -1))  13 us
    ppermute x3, starting transfers between devices, body(): groups.append(lax.ppermute(group, 'sp_2', ring(2, 1)))  12.6 us
    ppermute x4, starting transfers between devices, body(): up = lax.ppermute(up, 'sp_1', ring(8, 1))  9.9 us
  transfers between devices with their start and end apart: 17, of which 10 were waited for; matrix products, arithmetic and copies ran while one was open for 5% of the time, Pallas kernels for 7%

profile of v3, /device:TPU:1, one launch (start us, length us, event | category | flops | bytes accessed | tf_op | source)
XLA Modules:
  0.0 167.3 jit_solution(10901068947144101510)
XLA Ops:
  8.1 10.9 %all-to-all-start = ((bf16[8,32,384]{2,1,0:T(8,128)(2,1)}), bf16[8,32,384]{2,1,0:T(8,128)(2,1)S(1)}, u32[]{:S(2)}, u32[]{:S(2)}) async-start(bf16[8,32,384]{2,1,0:T(8,128)(2,1)} %get-tuple-element.22), calls=%async_computation | async-start | bytes 393216 | tf_op jit(solution)/shard_map/all_to_all | solution.py:27
  19.0 2.2 %fusion = f32[256]{0:T(256)S(1)} fusion(bf16[256,4096]{1,0:T(8,128)(2,1)} %param.15), kind=kLoop, calls=%fused_computation.2 | loop fusion | flops 3145472 | bytes 2098176 | tf_op jit(solution)/shard_map/reduce_sum | solution.py:22
  21.9 6.1 %all-to-all-done = bf16[8,32,384]{2,1,0:T(8,128)(2,1)S(1)} async-done(((bf16[8,32,384]{2,1,0:T(8,128)(2,1)}), bf16[8,32,384]{2,1,0:T(8,128)(2,1)S(1)}, u32[]{:S(2)}, u32[]{:S(2)}) %all-to-all-start) | async-done | bytes 196640 | tf_op jit(solution)/shard_map/all_to_all | solution.py:27
  28.0 3.2 %collective-permute-start = (bf16[8,32,384]{2,1,0:T(8,128)(2,1)S(1)}, bf16[8,32,384]{2,1,0:T(8,128)(2,1)S(1)}, u32[]{:S(2)}, u32[]{:S(2)}) collective-permute-start(bf16[8,32,384]{2,1,0:T(8,128)(2,1)S(1)} %all-to-all-done), channel_id=1, source_target_pairs={{0,8},{8,16},{16,24},{24,32},{32,40},{40,48},{48,56},{56,0},{1,9},... | collective-permute-start | bytes 589832 | tf_op jit(solution)/shard_map/ppermute | solution.py:382
  31.2 3.8 %collective-permute-start.1 = (bf16[8,32,384]{2,1,0:T(8,128)(2,1)S(1)}, bf16[8,32,384]{2,1,0:T(8,128)(2,1)S(1)}, u32[]{:S(2)}, u32[]{:S(2)}) collective-permute-start(bf16[8,32,384]{2,1,0:T(8,128)(2,1)S(1)} %all-to-all-done), channel_id=1, source_target_pairs={{0,56},{8,0},{16,8},{24,16},{32,24},{40,32},{48,40},{56,48},{1,57}... | collective-permute-start | bytes 589832 | tf_op jit(solution)/shard_map/ppermute | solution.py:385
  38.6 4.6 %collective-permute-start.3 = (bf16[8,32,384]{2,1,0:T(8,128)(2,1)S(1)}, bf16[8,32,384]{2,1,0:T(8,128)(2,1)S(1)}, u32[]{:S(2)}, u32[]{:S(2)}) collective-permute-start(bf16[8,32,384]{2,1,0:T(8,128)(2,1)S(1)} %collective-permute-done.1), channel_id=1, source_target_pairs={{0,56},{8,0},{16,8},{24,16},{32,24},{40,32},{48,40},{56,48},{1,57}... | collective-permute-start | bytes 589832 | tf_op jit(solution)/shard_map/ppermute | solution.py:385
  46.5 4.6 %collective-permute-start.5 = (bf16[8,32,384]{2,1,0:T(8,128)(2,1)S(1)}, bf16[8,32,384]{2,1,0:T(8,128)(2,1)S(1)}, u32[]{:S(2)}, u32[]{:S(2)}) collective-permute-start(bf16[8,32,384]{2,1,0:T(8,128)(2,1)S(1)} %collective-permute-done.3), channel_id=1, source_target_pairs={{0,56},{8,0},{16,8},{24,16},{32,24},{40,32},{48,40},{56,48},{1,57}... | collective-permute-start | bytes 589832 | tf_op jit(solution)/shard_map/ppermute | solution.py:385
  55.9 7.1 %collective-permute-start.8 = (bf16[4,8,32,384]{3,2,1,0:T(8,128)(2,1)S(1)}, bf16[4,8,32,384]{3,2,1,0:T(8,128)(2,1)}, u32[]{:S(2)}, u32[]{:S(2)}) collective-permute-start(bf16[4,8,32,384]{3,2,1,0:T(8,128)(2,1)S(1)} %pad_maximum_fusion.refs_1_), channel_id=1, source_target_pairs={{0,4},{4,0},{1,5},{5,1},{2,6},{6,2},{3,7},{7,3},{8,12},{12,8},{9,1... | collective-permute-start | bytes 2359304 | tf_op jit(solution)/shard_map/ppermute | solution.py:392
  66.8 2.9 %collective-permute-start.6 = (bf16[8,32,384]{2,1,0:T(8,128)(2,1)}, bf16[8,32,384]{2,1,0:T(8,128)(2,1)S(1)}, u32[]{:S(2)}, u32[]{:S(2)}) collective-permute-start(bf16[8,32,384]{2,1,0:T(8,128)(2,1)} %copy-done.11), channel_id=1, source_target_pairs={{0,8},{8,16},{16,24},{24,32},{32,40},{40,48},{48,56},{56,0},{1,9},... | collective-permute-start | bytes 589832 | tf_op jit(solution)/shard_map/ppermute | solution.py:382
  69.7 10.9 %collective-permute-done.6 = bf16[8,32,384]{2,1,0:T(8,128)(2,1)S(1)} collective-permute-done((bf16[8,32,384]{2,1,0:T(8,128)(2,1)}, bf16[8,32,384]{2,1,0:T(8,128)(2,1)S(1)}, u32[]{:S(2)}, u32[]{:S(2)}) %collective-permute-start.6) | collective-permute-done | bytes 196640 | tf_op jit(solution)/shard_map/ppermute | solution.py:382
  80.7 3.6 %collective-permute-start.9 = (bf16[1,8,32,384]{3,2,1,0:T(8,128)(2,1)S(1)}, bf16[1,8,32,384]{3,2,1,0:T(8,128)(2,1)S(1)}, u32[]{:S(2)}, u32[]{:S(2)}) collective-permute-start(bf16[1,8,32,384]{3,2,1,0:T(8,128)(2,1)S(1)} %bitcast.43), channel_id=1, source_target_pairs={{0,4},{4,0},{1,5},{5,1},{2,6},{6,2},{3,7},{7,3},{8,12},{12,8},{9,1... | collective-permute-start | bytes 589832 | tf_op jit(solution)/shard_map/ppermute | solution.py:392
  85.3 3.2 %shard_map.147 = (bf16[16,48,128]{2,1,0:T(8,128)(2,1)S(1)}, bf16[256,128]{1,0:T(8,128)(2,1)S(1)}, bf16[256,256]{1,0:T(8,128)(2,1)S(1)}) custom-call(s32[2]{0:T(128)S(1)} %pad_add_fusion.place_ref, bf16[256,4096]{1,0:T(8,128)(2,1)S(1)} %fusion.2.normed_ref, f32[256,8]{1,0:T(8,128)S(1)} %get-tuple-element.24.update_ref.column_ref, ...), custom_call_target="tpu_custom_call" | custom-call | tf_op jit(solution)/shard_map/pallas_call | solution.py:321
  88.6 19.3 %all_to_all.25.state_ref = bf16[16,48,128]{2,1,0:T(8,128)(2,1)S(1)} all-to-all(bf16[16,48,128]{2,1,0:T(8,128)(2,1)S(1)} %get-tuple-element.36), channel_id=1, replica_groups=mesh['sp_0'=8,'sp_1'=8,'sp_2'=2,'tp'=4] {'sp_1','sp_2'}, dimensions={0} | all-to-all | bytes 393216 | tf_op jit(solution)/shard_map/all_to_all | solution.py:27
  108.6 3.4 %all-to-all-start.2 = ((bf16[8,48,128]{2,1,0:T(8,128)(2,1)}), bf16[8,48,128]{2,1,0:T(8,128)(2,1)S(1)}, u32[]{:S(2)}, u32[]{:S(2)}) async-start(bf16[8,48,128]{2,1,0:T(8,128)(2,1)} %get-tuple-element.38), calls=%async_computation.2 | async-start | bytes 196608 | tf_op jit(solution)/shard_map/all_to_all | solution.py:27
  114.0 2.4 %collective-permute-start.11 = (bf16[1,4096]{1,0:T(2,128)(2,1)S(1)}, bf16[1,4096]{1,0:T(2,128)(2,1)S(1)}, u32[]{:S(2)}, u32[]{:S(2)}) collective-permute-start(bf16[1,4096]{1,0:T(2,128)(2,1)S(1)} %get-tuple-element.29), channel_id=1, source_target_pairs={{4,0},{8,4},{12,8},{16,12},{20,16},{24,20},{28,24},{32,28},{36,32}... | collective-permute-start | bytes 24584 | tf_op jit(solution)/shard_map/ppermute | solution.py:34
  116.5 4.3 %all-to-all-done.2.planes_ref = bf16[8,48,128]{2,1,0:T(8,128)(2,1)S(1)} async-done(((bf16[8,48,128]{2,1,0:T(8,128)(2,1)}), bf16[8,48,128]{2,1,0:T(8,128)(2,1)S(1)}, u32[]{:S(2)}, u32[]{:S(2)}) %all-to-all-start.2) | async-done | bytes 98336 | tf_op jit(solution)/shard_map/all_to_all | solution.py:27
  121.7 3.7 %all-to-all-start.3 = ((bf16[16,48,128]{2,1,0:T(8,128)(2,1)}), bf16[16,48,128]{2,1,0:T(8,128)(2,1)S(1)}, u32[]{:S(2)}, u32[]{:S(2)}) async-start(bf16[16,48,128]{2,1,0:T(8,128)(2,1)} %shard_map.150), calls=%async_computation.3 | async-start | bytes 393216 | tf_op jit(solution)/shard_map/all_to_all | solution.py:27
  125.6 5.3 %shard_map.148 = (bf16[256,128]{1,0:T(8,128)(2,1)S(1)}, bf16[256,256]{1,0:T(8,128)(2,1)S(1)}) custom-call(bf16[256,4096]{1,0:T(8,128)(2,1)S(1)} %fusion.2.normed_ref, bf16[16,4096]{1,0:T(8,128)(2,1)S(1)} %maximum_maximum_fusion.edge_ref, bf16[3,256]{1,0:T(4,128)(2,1)S(1)} %copy-done.5, bf16[4096,1408]{1,0:T(8,128)(2,1)} %all-gather.2.cloned.1.call-done.whole_ref), custom_call_target="tpu_custom_call" | custom-call | tf_op jit(solution)/shard_map/pallas_call | solution.py:321
  130.9 4.8 %all-to-all-done.3.start_ref = bf16[16,48,128]{2,1,0:T(8,128)(2,1)S(1)} async-done(((bf16[16,48,128]{2,1,0:T(8,128)(2,1)}), bf16[16,48,128]{2,1,0:T(8,128)(2,1)S(1)}, u32[]{:S(2)}, u32[]{:S(2)}) %all-to-all-start.3) | async-done | bytes 196640 | tf_op jit(solution)/shard_map/all_to_all | solution.py:27
  135.7 2.0 %shard_map.151 = bf16[4,256,512]{2,1,0:T(8,128)(2,1)} custom-call(bf16[256,128]{1,0:T(8,128)(2,1)S(1)} %get-tuple-element.31.query_ref, bf16[256,128]{1,0:T(8,128)(2,1)S(1)} %get-tuple-element.32.key_ref, bf16[256,256]{1,0:T(8,128)(2,1)S(1)} %copy-done.4, f32[256,8]{1,0:T(8,128)S(1)} %copy-done.2, f32[4,256]{1,0:T(4,128)S(1)} %get-tuple-element.34.row_ref, ...), custom_call_target="tpu_custom_call" | custom-call | tf_op jit(solution)/shard_map/pallas_call | solution.py:321
  137.7 3.9 %all-to-all-start.4 = ((bf16[4,256,512]{2,1,0:T(8,128)(2,1)}), bf16[4,256,512]{2,1,0:T(8,128)(2,1)S(1)}, u32[]{:S(2)}, u32[]{:S(2)}) async-start(bf16[4,256,512]{2,1,0:T(8,128)(2,1)} %shard_map.151), calls=%async_computation.4 | async-start | bytes 2097152 | tf_op jit(solution)/shard_map/all_to_all | solution.py:27
  141.7 2.2 %slice-done = bf16[4096,512]{1,0:T(8,128)(2,1)S(1)} async-done(((bf16[4096,1408]{1,0:T(8,128)(2,1)}), bf16[4096,512]{1,0:T(8,128)(2,1)S(1)}, s32[]{:S(2)}) %slice-start) | async-done | bytes 4194328 | tf_op jit(solution)/shard_map/slice | solution.py:471
  145.7 11.2 %all-to-all-done.4.joined_ref = bf16[4,256,512]{2,1,0:T(8,128)(2,1)S(1)} async-done(((bf16[4,256,512]{2,1,0:T(8,128)(2,1)}), bf16[4,256,512]{2,1,0:T(8,128)(2,1)S(1)}, u32[]{:S(2)}, u32[]{:S(2)}) %all-to-all-start.4) | async-done | bytes 1048608 | tf_op jit(solution)/shard_map/all_to_all | solution.py:27
  158.5 2.0 %shard_map.152 = bf16[256,1024]{1,0:T(8,128)(2,1)} custom-call(bf16[4,256,512]{2,1,0:T(8,128)(2,1)S(1)} %all-to-all-done.4.joined_ref, bf16[4,512,512]{2,1,0:T(8,128)(2,1)S(1)} %bitcast.42, bf16[4,512,512]{2,1,0:T(8,128)(2,1)S(1)} %bitcast.41), custom_call_target="tpu_custom_call" | custom-call | tf_op jit(solution)/shard_map/pallas_call | solution.py:321
  (78 shorter events, 26.0 us)
Async XLA Ops:
  6.5 119.1 %all-gather.2.cloned.1.call-start = ((), (), s32[]{:S(2)}) async-start(), calls=%async_computation.5 | async-start | bytes 11624448 | tf_op jit(solution)/shard_map/all_gather | solution.py:373
  8.1 19.9 %all-to-all-start = ((bf16[8,32,384]{2,1,0:T(8,128)(2,1)}), bf16[8,32,384]{2,1,0:T(8,128)(2,1)S(1)}, u32[]{:S(2)}, u32[]{:S(2)}) async-start(bf16[8,32,384]{2,1,0:T(8,128)(2,1)} %get-tuple-element.22), calls=%async_computation | async-start | bytes 393216 | tf_op jit(solution)/shard_map/all_to_all | solution.py:27
  21.3 29.8 %copy-start.15 = (bf16[4096,2,2,1]{0,2,3,1:T(2,128)(2,1)S(1)}, bf16[4096,2,2,1]{0,2,3,1:T(2,128)(2,1)}, u32[]{:S(2)}) copy-start(bf16[4096,2,2,1]{0,2,3,1:T(2,128)(2,1)} %param.20) | copy-start | bytes 98308
  28.0 35.0 %copy-start.8 = (bf16[8,32,384]{2,1,0:T(8,128)(2,1)}, bf16[8,32,384]{2,1,0:T(8,128)(2,1)S(1)}, u32[]{:S(2)}) copy-start(bf16[8,32,384]{2,1,0:T(8,128)(2,1)S(1)} %all-to-all-done) | copy-start | bytes 589828
  28.0 8.6 %collective-permute-start = (bf16[8,32,384]{2,1,0:T(8,128)(2,1)S(1)}, bf16[8,32,384]{2,1,0:T(8,128)(2,1)S(1)}, u32[]{:S(2)}, u32[]{:S(2)}) collective-permute-start(bf16[8,32,384]{2,1,0:T(8,128)(2,1)S(1)} %all-to-all-done), channel_id=1, source_target_pairs={{0,8},{8,16},{16,24},{24,32},{32,40},{40,48},{48,56},{56,0},{1,9},... | collective-permute-start | bytes 589832 | tf_op jit(solution)/shard_map/ppermute | solution.py:382
  31.2 7.3 %collective-permute-start.1 = (bf16[8,32,384]{2,1,0:T(8,128)(2,1)S(1)}, bf16[8,32,384]{2,1,0:T(8,128)(2,1)S(1)}, u32[]{:S(2)}, u32[]{:S(2)}) collective-permute-start(bf16[8,32,384]{2,1,0:T(8,128)(2,1)S(1)} %all-to-all-done), channel_id=1, source_target_pairs={{0,56},{8,0},{16,8},{24,16},{32,24},{40,32},{48,40},{56,48},{1,57}... | collective-permute-start | bytes 589832 | tf_op jit(solution)/shard_map/ppermute | solution.py:385
  36.6 26.4 %copy-start.9 = (bf16[8,32,384]{2,1,0:T(8,128)(2,1)}, bf16[8,32,384]{2,1,0:T(8,128)(2,1)S(1)}, u32[]{:S(2)}) copy-start(bf16[8,32,384]{2,1,0:T(8,128)(2,1)S(1)} %collective-permute-done) | copy-start | bytes 589828
  36.6 7.9 %collective-permute-start.2 = (bf16[8,32,384]{2,1,0:T(8,128)(2,1)S(1)}, bf16[8,32,384]{2,1,0:T(8,128)(2,1)S(1)}, u32[]{:S(2)}, u32[]{:S(2)}) collective-permute-start(bf16[8,32,384]{2,1,0:T(8,128)(2,1)S(1)} %collective-permute-done), channel_id=1, source_target_pairs={{0,8},{8,16},{16,24},{24,32},{32,40},{40,48},{48,56},{56,0},{1,9},... | collective-permute-start | bytes 589832 | tf_op jit(solution)/shard_map/ppermute | solution.py:382
  38.6 7.9 %collective-permute-start.3 = (bf16[8,32,384]{2,1,0:T(8,128)(2,1)S(1)}, bf16[8,32,384]{2,1,0:T(8,128)(2,1)S(1)}, u32[]{:S(2)}, u32[]{:S(2)}) collective-permute-start(bf16[8,32,384]{2,1,0:T(8,128)(2,1)S(1)} %collective-permute-done.1), channel_id=1, source_target_pairs={{0,56},{8,0},{16,8},{24,16},{32,24},{40,32},{48,40},{56,48},{1,57}... | collective-permute-start | bytes 589832 | tf_op jit(solution)/shard_map/ppermute | solution.py:385
  44.5 8.4 %collective-permute-start.4 = (bf16[8,32,384]{2,1,0:T(8,128)(2,1)S(1)}, bf16[8,32,384]{2,1,0:T(8,128)(2,1)S(1)}, u32[]{:S(2)}, u32[]{:S(2)}) collective-permute-start(bf16[8,32,384]{2,1,0:T(8,128)(2,1)S(1)} %collective-permute-done.2), channel_id=1, source_target_pairs={{0,8},{8,16},{16,24},{24,32},{32,40},{40,48},{48,56},{56,0},{1,9},... | collective-permute-start | bytes 589832 | tf_op jit(solution)/shard_map/ppermute | solution.py:382
  46.5 7.4 %collective-permute-start.5 = (bf16[8,32,384]{2,1,0:T(8,128)(2,1)S(1)}, bf16[8,32,384]{2,1,0:T(8,128)(2,1)S(1)}, u32[]{:S(2)}, u32[]{:S(2)}) collective-permute-start(bf16[8,32,384]{2,1,0:T(8,128)(2,1)S(1)} %collective-permute-done.3), channel_id=1, source_target_pairs={{0,56},{8,0},{16,8},{24,16},{32,24},{40,32},{48,40},{56,48},{1,57}... | collective-permute-start | bytes 589832 | tf_op jit(solution)/shard_map/ppermute | solution.py:385
  54.5 29.7 %copy-start.17 = (f32[2,256,1]{1,2,0:T(1,128)S(1)}, f32[2,256,1]{1,2,0:T(1,128)}, u32[]{:S(2)}) copy-start(f32[2,256,1]{1,2,0:T(1,128)} %param.23) | copy-start | bytes 6148
  54.5 29.7 %copy-start.18 = (f32[2,1]{0,1:T(1,128)S(1)}, f32[2,1]{0,1:T(1,128)}, u32[]{:S(2)}) copy-start(f32[2,1]{0,1:T(1,128)} %param.22) | copy-start | bytes 28
  54.5 29.7 %copy-start.19 = (f32[2,1]{0,1:T(1,128)S(1)}, f32[2,1]{0,1:T(1,128)}, u32[]{:S(2)}) copy-start(f32[2,1]{0,1:T(1,128)} %param.21) | copy-start | bytes 28
  55.9 29.4 %collective-permute-start.8 = (bf16[4,8,32,384]{3,2,1,0:T(8,128)(2,1)S(1)}, bf16[4,8,32,384]{3,2,1,0:T(8,128)(2,1)}, u32[]{:S(2)}, u32[]{:S(2)}) collective-permute-start(bf16[4,8,32,384]{3,2,1,0:T(8,128)(2,1)S(1)} %pad_maximum_fusion.refs_1_), channel_id=1, source_target_pairs={{0,4},{4,0},{1,5},{5,1},{2,6},{6,2},{3,7},{7,3},{8,12},{12,8},{9,1... | collective-permute-start | bytes 2359304 | tf_op jit(solution)/shard_map/ppermute | solution.py:392
  64.2 21.0 %collective-permute-start.7 = (bf16[3,8,32,384]{3,2,1,0:T(8,128)(2,1)S(1)}, bf16[3,8,32,384]{3,2,1,0:T(8,128)(2,1)}, u32[]{:S(2)}, u32[]{:S(2)}) collective-permute-start(bf16[3,8,32,384]{3,2,1,0:T(8,128)(2,1)S(1)} %pad_maximum_fusion.1.refs_0_), channel_id=1, source_target_pairs={{0,4},{4,0},{1,5},{5,1},{2,6},{6,2},{3,7},{7,3},{8,12},{12,8},{9,1... | collective-permute-start | bytes 1769480 | tf_op jit(solution)/shard_map/ppermute | solution.py:392
  66.8 13.8 %collective-permute-start.6 = (bf16[8,32,384]{2,1,0:T(8,128)(2,1)}, bf16[8,32,384]{2,1,0:T(8,128)(2,1)S(1)}, u32[]{:S(2)}, u32[]{:S(2)}) collective-permute-start(bf16[8,32,384]{2,1,0:T(8,128)(2,1)} %copy-done.11), channel_id=1, source_target_pairs={{0,8},{8,16},{16,24},{24,32},{32,40},{40,48},{48,56},{56,0},{1,9},... | collective-permute-start | bytes 589832 | tf_op jit(solution)/shard_map/ppermute | solution.py:382
  80.7 4.6 %collective-permute-start.9 = (bf16[1,8,32,384]{3,2,1,0:T(8,128)(2,1)S(1)}, bf16[1,8,32,384]{3,2,1,0:T(8,128)(2,1)S(1)}, u32[]{:S(2)}, u32[]{:S(2)}) collective-permute-start(bf16[1,8,32,384]{3,2,1,0:T(8,128)(2,1)S(1)} %bitcast.43), channel_id=1, source_target_pairs={{0,4},{4,0},{1,5},{5,1},{2,6},{6,2},{3,7},{7,3},{8,12},{12,8},{9,1... | collective-permute-start | bytes 589832 | tf_op jit(solution)/shard_map/ppermute | solution.py:392
  88.5 37.1 %copy-start.5 = (bf16[3,256]{1,0:T(4,128)(2,1)S(1)}, bf16[3,256]{1,0:T(4,128)(2,1)}, u32[]{:S(2)}) copy-start(bf16[3,256]{1,0:T(4,128)(2,1)} %tap_ref.1) | copy-start | bytes 4612
  108.6 12.2 %all-to-all-start.2 = ((bf16[8,48,128]{2,1,0:T(8,128)(2,1)}), bf16[8,48,128]{2,1,0:T(8,128)(2,1)S(1)}, u32[]{:S(2)}, u32[]{:S(2)}) async-start(bf16[8,48,128]{2,1,0:T(8,128)(2,1)} %get-tuple-element.38), calls=%async_computation.2 | async-start | bytes 196608 | tf_op jit(solution)/shard_map/all_to_all | solution.py:27
  112.0 13.4 %collective-permute-start.10 = (bf16[1,4096]{1,0:T(2,128)(2,1)S(1)}, bf16[1,4096]{1,0:T(2,128)(2,1)S(1)}, u32[]{:S(2)}, u32[]{:S(2)}) collective-permute-start(bf16[1,4096]{1,0:T(2,128)(2,1)S(1)} %get-tuple-element.28), channel_id=1, source_target_pairs={{0,4},{4,8},{8,12},{12,16},{16,20},{20,24},{24,28},{28,32},{32,36}... | collective-permute-start | bytes 24584 | tf_op jit(solution)/shard_map/ppermute | solution.py:33
  114.0 11.5 %collective-permute-start.11 = (bf16[1,4096]{1,0:T(2,128)(2,1)S(1)}, bf16[1,4096]{1,0:T(2,128)(2,1)S(1)}, u32[]{:S(2)}, u32[]{:S(2)}) collective-permute-start(bf16[1,4096]{1,0:T(2,128)(2,1)S(1)} %get-tuple-element.29), channel_id=1, source_target_pairs={{4,0},{8,4},{12,8},{16,12},{20,16},{24,20},{28,24},{32,28},{36,32}... | collective-permute-start | bytes 24584 | tf_op jit(solution)/shard_map/ppermute | solution.py:34
  121.7 14.0 %all-to-all-start.3 = ((bf16[16,48,128]{2,1,0:T(8,128)(2,1)}), bf16[16,48,128]{2,1,0:T(8,128)(2,1)S(1)}, u32[]{:S(2)}, u32[]{:S(2)}) async-start(bf16[16,48,128]{2,1,0:T(8,128)(2,1)} %shard_map.150), calls=%async_computation.3 | async-start | bytes 393216 | tf_op jit(solution)/shard_map/all_to_all | solution.py:27
  137.7 19.1 %all-to-all-start.4 = ((bf16[4,256,512]{2,1,0:T(8,128)(2,1)}), bf16[4,256,512]{2,1,0:T(8,128)(2,1)S(1)}, u32[]{:S(2)}, u32[]{:S(2)}) async-start(bf16[4,256,512]{2,1,0:T(8,128)(2,1)} %shard_map.151), calls=%async_computation.4 | async-start | bytes 2097152 | tf_op jit(solution)/shard_map/all_to_all | solution.py:27
  (14 other events, 117.4 us)
Sparse Core Ops, SparseCore 0:
  10.5 101.1 all-gather.1

commit v4 on v3

--- a/solution.py
+++ b/solution.py
@@ -59,10 +59,6 @@
             rows += in_terms(number)
     rows.append(jnp.zeros((ROWS - NORMERS - len(rows), 128), BF16))
     return jnp.concatenate(rows, axis=0)
-
-
-ARRIVAL = (0, -1, 1, -2, 2, -3, 3, -4)
-GROUPS = (3, 4, 1)
 
 
 def pack_kernel(query_ref, key_ref, value_ref, outer_ref, inner_ref, given_ref, out_ref, whole_ref, block_ref):
@@ -105,19 +101,16 @@
 
 
 def state_kernel(place_ref, normed_ref, update_ref, number_ref, *refs):
-    groups = len(GROUPS)
-    state_ref, key_ref, value_ref, weight_ref = refs[2 * groups :]
-    core, row = place_ref[0], place_ref[1]
-    for side in range(2):
-        cell = 1 - core if side else core
-        arrivals = iter(ARRIVAL)
-        for group_ref in refs[side * groups : (side + 1) * groups]:
-            _, planes, depth, _ = group_ref.shape
-            for k in range(group_ref.shape[0]):
-                y = (row + next(arrivals) + 8) % 8
-                for z in range(planes):
-                    start = ((z * 8 + y) * 2 + cell) * depth
-                    weight_ref[pl.ds(pl.multiple_of(start, depth), depth), :] = group_ref[k, z]
+    blocks = refs[:8]
+    state_ref, key_ref, value_ref, weight_ref = refs[8:]
+    way, row = place_ref[0], place_ref[1]
+    for n, block_ref in enumerate(blocks):
+        offset = (n if n < 4 else 3 - n) if n < 7 else 4
+        y = (row + way * offset + 8) % 8
+        planes, depth, _ = block_ref.shape
+        for z in range(planes):
+            start = (z * 8 + y) * depth
+            weight_ref[pl.ds(pl.multiple_of(start, depth), depth), :] = block_ref[z]
     both = jnp.dot(normed_ref[...], weight_ref[...], preferred_element_type=F32)
     both = both.astype(BF16)
     keys, values = both[:, :DQK], both[:, DQK:]
@@ -301,13 +294,16 @@
     conv_ref[...] = (outer * filtered).astype(BF16)
 
 
-def output_kernel(joined_ref, left_ref, right_ref, out_ref):
-    for side, weight_ref in enumerate((left_ref, right_ref)):
-        total = None
-        for k in range(joined_ref.shape[0]):
-            product = jnp.dot(joined_ref[k], weight_ref[k], preferred_element_type=F32)
-            total = product if total is None else total + product
-        out_ref[:, side * 512 : (side + 1) * 512] = total.astype(BF16)
+def output_kernel(joined_ref, weight_ref, *refs):
+    total = None
+    for k in range(joined_ref.shape[0]):
+        product = jnp.dot(joined_ref[k], weight_ref[k], preferred_element_type=F32)
+        total = product if total is None else total + product
+    if len(refs) == 1:
+        refs[0][...] = total.astype(BF16)
+    else:
+        refs[1][:, : total.shape[1]] = refs[0][...]
+        refs[1][:, total.shape[1] :] = total.astype(BF16)
 
 
 def ring(size, step):
@@ -358,7 +354,7 @@
         pack_kernel,
         (
             jax.ShapeDtypeStruct((w_key.shape[0], WIDE + half), BF16),
-            jax.ShapeDtypeStruct((planes, w_key.shape[0], DQK + DV), BF16),
+            jax.ShapeDtypeStruct((2 * planes, w_key.shape[0], DQK + DV), BF16),
         ),
         w_query,
         w_key,
@@ -369,27 +365,20 @@
         w_out,
         limit=63,
     )
-    block = swapped(block, "sp_0")
+    block = swapped(block, ("sp_0", "sp_2")).reshape(planes, -1, DQK + DV)
     whole = lax.all_gather(packed, SP, axis=0, tiled=True)
     core = lax.axis_index("sp_2")
     row = lax.axis_index("sp_1")
     normed = row_norm(tokens, norm_gain)
 
     block, normed = lax.optimization_barrier((block, normed))
-    up = down = block
-    pieces = [block]
+    apart = [(2 * y + c, (y + 1 - 2 * c) % 8 * 2 + c) for y in range(8) for c in range(2)]
+    pieces, swaps = [block], []
     for k in range(4):
-        up = lax.ppermute(up, "sp_1", ring(8, 1))
-        pieces.append(up)
+        pieces.append(lax.ppermute(pieces[-1], PLANE, apart))
         if k < 3:
-            down = lax.ppermute(down, "sp_1", ring(8, -1))
-            pieces.append(down)
-    groups, at = [], 0
-    for count in GROUPS:
-        groups.append(jnp.stack(pieces[at : at + count]))
-        at += count
-    for count, group in zip(GROUPS, tuple(groups)):
-        groups.append(lax.ppermute(group, "sp_2", ring(2, 1)))
+            swaps.append(lax.ppermute(pieces[-1], "sp_2", ring(2, 1)))
+    pieces = pieces[:4] + swaps + pieces[4:]
 
     gates = lax.dot_general(
         w_gates.reshape(-1, 4), normed, (((0,), (1,)), ((), ())), preferred_element_type=F32
@@ -414,11 +403,11 @@
             jax.ShapeDtypeStruct((length, DQK), BF16),
             jax.ShapeDtypeStruct((length, DV), BF16),
         ),
-        jnp.stack([core, row]),
+        jnp.stack([2 * core - 1, row]),
         normed,
         columns,
         numbers,
-        *groups,
+        *pieces,
         scalars=1,
         scratch=[pltpu.VMEM((normed.shape[1], DQK + DV), BF16)],
     )
@@ -469,11 +458,14 @@
     )
     joined = swapped(joined, "tp")
     sides = whole[:, WIDE:].reshape(size, 2, depth, half)
+    left, right = (sides[:, side].reshape(4, 2 * DV, half) for side in range(2))
+    first = on_core(output_kernel, jax.ShapeDtypeStruct((length, half), BF16), joined, left)
     return on_core(
         output_kernel,
         jax.ShapeDtypeStruct((length, 2 * half), BF16),
         joined,
-        *(sides[:, side].reshape(4, 2 * DV, half) for side in range(2)),
+        right,
+        first,
     )
 
 

time: 168 us -> 172 us (1.024)
  waiting for transfers between devices: 43.2 us -> 53.5 us
  starting transfers between devices: 61.7 us -> 57.2 us
  other arithmetic: 5.7 us -> 3.13 us
  blocking collectives: 19.3 us -> 21.1 us
    ppermute x10 -> x7, starting transfers between devices: 35.4 us -> 26.1 us  [the longest x4 17 us: body(): pieces.append(lax.ppermute(pieces[-1], PLANE, apart))]
    ppermute x10 -> x7, waiting for transfers between devices: 16.7 us -> 22.2 us  [the longest x4 22.2 us: body(): pieces.append(lax.ppermute(pieces[-1], PLANE, apart))]
    all_to_all x4, starting transfers between devices: 21.9 us -> 26.8 us  [swapped(): return lax.all_to_all(value, axes, split_axis=0, concat_axis=0, tiled=True)]
    all_to_all x4, waiting for transfers between devices: 26.4 us -> 31.3 us  [swapped(): return lax.all_to_all(value, axes, split_axis=0, concat_axis=0, tiled=True)]
    another operation x3 -> x1, other arithmetic: 2.65 us -> 0.08 us  [body(): jnp.stack([2 * core - 1, row])]
    all_to_all x1, blocking collectives: 19.3 us -> 21.1 us  [swapped(): return lax.all_to_all(value, axes, split_axis=0, concat_axis=0, tiled=True)]
    pallas_call x8 -> x9, Pallas kernels: 16.6 us -> 16.3 us  [on_core(): pl.pallas_call(kernel, out_shape=out, in_specs=[smem] * scalars + [vmem]...]
  transfers between devices with their start and end apart: 17 -> 14, of which waited for: 10 -> 7; matrix products, arithmetic and copies ran while one was open for 5% -> 3% of each run, Pallas kernels for 7% -> 6%
where the time goes in v4:
time: 172 us; the launch traced here: 171 us
  starting transfers between devices  57.2 us (33%)
  waiting for transfers between devices  53.5 us (31%)
  blocking collectives  21.1 us (12%)
  Pallas kernels  16.3 us (9%)
  between operations  13.7 us (8%)
  local copies, waits for them, and re-layouts  5.8 us (3%)
  other arithmetic  3.13 us (2%)
    all_to_all x4, waiting for transfers between devices, swapped(): return lax.all_to_all(value, axes, split_axis=0, concat_axis=0, tiled=True)  31.3 us
    all_to_all x4, starting transfers between devices, swapped(): return lax.all_to_all(value, axes, split_axis=0, concat_axis=0, tiled=True)  26.8 us
    ppermute x4, waiting for transfers between devices, body(): pieces.append(lax.ppermute(pieces[-1], PLANE, apart))  22.2 us
    all_to_all x1, blocking collectives, swapped(): return lax.all_to_all(value, axes, split_axis=0, concat_axis=0, tiled=True)  21.1 us
    ppermute x4, starting transfers between devices, body(): pieces.append(lax.ppermute(pieces[-1], PLANE, apart))  17 us
    pallas_call x9, Pallas kernels, on_core(): pl.pallas_call(kernel, out_shape=out, in_specs=[smem] * scalars + [vmem]...  16.3 us
    ppermute x3, starting transfers between devices, body(): swaps.append(lax.ppermute(pieces[-1], 'sp_2', ring(2, 1)))  9.1 us
  transfers between devices with their start and end apart: 14, of which 7 were waited for; matrix products, arithmetic and copies ran while one was open for 3% of the time, Pallas kernels for 6%

profile of v4, /device:TPU:1, one launch (start us, length us, event | category | flops | bytes accessed | tf_op | source)
XLA Modules:
  0.0 171.5 jit_solution(7139478748434486399)
XLA Ops:
  8.2 11.8 %all-to-all-start = ((bf16[16,32,384]{2,1,0:T(8,128)(2,1)}), bf16[16,32,384]{2,1,0:T(8,128)(2,1)S(1)}, u32[]{:S(2)}, u32[]{:S(2)}) async-start(bf16[16,32,384]{2,1,0:T(8,128)(2,1)} %get-tuple-element.22), calls=%async_computation | async-start | bytes 786432 | tf_op jit(solution)/shard_map/all_to_all | solution.py:27
  20.1 2.2 %fusion = f32[256]{0:T(256)S(1)} fusion(bf16[256,4096]{1,0:T(8,128)(2,1)} %param.15), kind=kLoop, calls=%fused_computation.2 | loop fusion | flops 3145472 | bytes 2098176 | tf_op jit(solution)/shard_map/reduce_sum | solution.py:22
  23.0 11.5 %all-to-all-done = bf16[16,32,384]{2,1,0:T(8,128)(2,1)S(1)} async-done(((bf16[16,32,384]{2,1,0:T(8,128)(2,1)}), bf16[16,32,384]{2,1,0:T(8,128)(2,1)S(1)}, u32[]{:S(2)}, u32[]{:S(2)}) %all-to-all-start) | async-done | bytes 393248 | tf_op jit(solution)/shard_map/all_to_all | solution.py:27
  34.5 5.1 %collective-permute-start = (bf16[8,64,384]{2,1,0:T(8,128)(2,1)S(1)}, bf16[8,64,384]{2,1,0:T(8,128)(2,1)S(1)}, u32[]{:S(2)}, u32[]{:S(2)}) collective-permute-start(bf16[8,64,384]{2,1,0:T(8,128)(2,1)S(1)} %bitcast.36), channel_id=1, source_target_pairs={{0,8},{4,60},{8,16},{12,4},{16,24},{20,12},{24,32},{28,20},{32,40}... | collective-permute-start | bytes 1179656 | tf_op jit(solution)/shard_map/ppermute | solution.py:378
  39.6 5.5 %collective-permute-done.refs_1_ = bf16[8,64,384]{2,1,0:T(8,128)(2,1)S(1)} collective-permute-done((bf16[8,64,384]{2,1,0:T(8,128)(2,1)S(1)}, bf16[8,64,384]{2,1,0:T(8,128)(2,1)S(1)}, u32[]{:S(2)}, u32[]{:S(2)}) %collective-permute-start) | collective-permute-done | bytes 393248 | tf_op jit(solution)/shard_map/ppermute | solution.py:378
  45.1 5.0 %collective-permute-start.1 = (bf16[8,64,384]{2,1,0:T(8,128)(2,1)S(1)}, bf16[8,64,384]{2,1,0:T(8,128)(2,1)S(1)}, u32[]{:S(2)}, u32[]{:S(2)}) collective-permute-start(bf16[8,64,384]{2,1,0:T(8,128)(2,1)S(1)} %collective-permute-done.refs_1_), channel_id=1, source_target_pairs={{0,8},{4,60},{8,16},{12,4},{16,24},{20,12},{24,32},{28,20},{32,40}... | collective-permute-start | bytes 1179656 | tf_op jit(solution)/shard_map/ppermute | solution.py:378
  50.1 5.2 %collective-permute-done.1.refs_2_ = bf16[8,64,384]{2,1,0:T(8,128)(2,1)S(1)} collective-permute-done((bf16[8,64,384]{2,1,0:T(8,128)(2,1)S(1)}, bf16[8,64,384]{2,1,0:T(8,128)(2,1)S(1)}, u32[]{:S(2)}, u32[]{:S(2)}) %collective-permute-start.1) | collective-permute-done | bytes 393248 | tf_op jit(solution)/shard_map/ppermute | solution.py:378
  55.3 5.0 %collective-permute-start.2 = (bf16[8,64,384]{2,1,0:T(8,128)(2,1)S(1)}, bf16[8,64,384]{2,1,0:T(8,128)(2,1)}, u32[]{:S(2)}, u32[]{:S(2)}) collective-permute-start(bf16[8,64,384]{2,1,0:T(8,128)(2,1)S(1)} %collective-permute-done.1.refs_2_), channel_id=1, source_target_pairs={{0,8},{4,60},{8,16},{12,4},{16,24},{20,12},{24,32},{28,20},{32,40}... | collective-permute-start | bytes 1179656 | tf_op jit(solution)/shard_map/ppermute | solution.py:378
  61.1 1.9 %collective-permute-start.3 = (bf16[8,64,384]{2,1,0:T(8,128)(2,1)S(1)}, bf16[8,64,384]{2,1,0:T(8,128)(2,1)S(1)}, u32[]{:S(2)}, u32[]{:S(2)}) collective-permute-start(bf16[8,64,384]{2,1,0:T(8,128)(2,1)S(1)} %collective-permute-done.refs_1_), channel_id=1, source_target_pairs={{0,4},{4,0},{1,5},{5,1},{2,6},{6,2},{3,7},{7,3},{8,12},{12,8},{9,1... | collective-permute-start | bytes 1179656 | tf_op jit(solution)/shard_map/ppermute | solution.py:380
  63.1 2.4 %collective-permute-start.4 = (bf16[8,64,384]{2,1,0:T(8,128)(2,1)S(1)}, bf16[8,64,384]{2,1,0:T(8,128)(2,1)S(1)}, u32[]{:S(2)}, u32[]{:S(2)}) collective-permute-start(bf16[8,64,384]{2,1,0:T(8,128)(2,1)S(1)} %collective-permute-done.1.refs_2_), channel_id=1, source_target_pairs={{0,4},{4,0},{1,5},{5,1},{2,6},{6,2},{3,7},{7,3},{8,12},{12,8},{9,1... | collective-permute-start | bytes 1179656 | tf_op jit(solution)/shard_map/ppermute | solution.py:380
  65.5 4.8 %collective-permute-start.5 = (bf16[8,64,384]{2,1,0:T(8,128)(2,1)}, bf16[8,64,384]{2,1,0:T(8,128)(2,1)S(1)}, u32[]{:S(2)}, u32[]{:S(2)}) collective-permute-start(bf16[8,64,384]{2,1,0:T(8,128)(2,1)} %collective-permute-done.2.refs_3_), channel_id=1, source_target_pairs={{0,4},{4,0},{1,5},{5,1},{2,6},{6,2},{3,7},{7,3},{8,12},{12,8},{9,1... | collective-permute-start | bytes 1179656 | tf_op jit(solution)/shard_map/ppermute | solution.py:380
  73.1 11.6 %collective-permute-done.6.refs_7_ = bf16[8,64,384]{2,1,0:T(8,128)(2,1)S(1)} collective-permute-done((bf16[8,64,384]{2,1,0:T(8,128)(2,1)}, bf16[8,64,384]{2,1,0:T(8,128)(2,1)S(1)}, u32[]{:S(2)}, u32[]{:S(2)}) %collective-permute-start.6) | collective-permute-done | bytes 393248 | tf_op jit(solution)/shard_map/ppermute | solution.py:378
  84.7 2.8 %shard_map.147 = (bf16[16,48,128]{2,1,0:T(8,128)(2,1)S(1)}, bf16[256,128]{1,0:T(8,128)(2,1)S(1)}, bf16[256,256]{1,0:T(8,128)(2,1)S(1)}) custom-call(s32[2]{0:T(128)S(1)} %pad_add_fusion.place_ref, bf16[256,4096]{1,0:T(8,128)(2,1)S(1)} %fusion.2.normed_ref, f32[256,8]{1,0:T(8,128)S(1)} %get-tuple-element.24.update_ref.column_ref, ...), custom_call_target="tpu_custom_call" | custom-call | tf_op jit(solution)/shard_map/pallas_call | solution.py:317
  87.5 21.1 %all_to_all.25.state_ref = bf16[16,48,128]{2,1,0:T(8,128)(2,1)S(1)} all-to-all(bf16[16,48,128]{2,1,0:T(8,128)(2,1)S(1)} %get-tuple-element.36), channel_id=1, replica_groups=mesh['sp_0'=8,'sp_1'=8,'sp_2'=2,'tp'=4] {'sp_1','sp_2'}, dimensions={0} | all-to-all | bytes 393216 | tf_op jit(solution)/shard_map/all_to_all | solution.py:27
  109.4 6.5 %all-to-all-start.2 = ((bf16[8,48,128]{2,1,0:T(8,128)(2,1)}), bf16[8,48,128]{2,1,0:T(8,128)(2,1)S(1)}, u32[]{:S(2)}, u32[]{:S(2)}) async-start(bf16[8,48,128]{2,1,0:T(8,128)(2,1)} %get-tuple-element.38), calls=%async_computation.2 | async-start | bytes 196608 | tf_op jit(solution)/shard_map/all_to_all | solution.py:27
  117.9 2.4 %collective-permute-start.8 = (bf16[1,4096]{1,0:T(2,128)(2,1)S(1)}, bf16[1,4096]{1,0:T(2,128)(2,1)S(1)}, u32[]{:S(2)}, u32[]{:S(2)}) collective-permute-start(bf16[1,4096]{1,0:T(2,128)(2,1)S(1)} %get-tuple-element.29), channel_id=1, source_target_pairs={{4,0},{8,4},{12,8},{16,12},{20,16},{24,20},{28,24},{32,28},{36,32}... | collective-permute-start | bytes 24584 | tf_op jit(solution)/shard_map/ppermute | solution.py:34
  120.4 3.7 %all-to-all-done.2.planes_ref = bf16[8,48,128]{2,1,0:T(8,128)(2,1)S(1)} async-done(((bf16[8,48,128]{2,1,0:T(8,128)(2,1)}), bf16[8,48,128]{2,1,0:T(8,128)(2,1)S(1)}, u32[]{:S(2)}, u32[]{:S(2)}) %all-to-all-start.2) | async-done | bytes 98336 | tf_op jit(solution)/shard_map/all_to_all | solution.py:27
  125.0 4.5 %all-to-all-start.3 = ((bf16[16,48,128]{2,1,0:T(8,128)(2,1)}), bf16[16,48,128]{2,1,0:T(8,128)(2,1)S(1)}, u32[]{:S(2)}, u32[]{:S(2)}) async-start(bf16[16,48,128]{2,1,0:T(8,128)(2,1)} %shard_map.150), calls=%async_computation.3 | async-start | bytes 393216 | tf_op jit(solution)/shard_map/all_to_all | solution.py:27
  129.6 5.2 %shard_map.148 = (bf16[256,128]{1,0:T(8,128)(2,1)S(1)}, bf16[256,256]{1,0:T(8,128)(2,1)S(1)}) custom-call(bf16[256,4096]{1,0:T(8,128)(2,1)S(1)} %fusion.2.normed_ref, bf16[16,4096]{1,0:T(8,128)(2,1)S(1)} %maximum_maximum_fusion.edge_ref, bf16[3,256]{1,0:T(4,128)(2,1)S(1)} %copy-done.3, bf16[4096,1408]{1,0:T(8,128)(2,1)} %all-gather.2.cloned.1.call-done.whole_ref), custom_call_target="tpu_custom_call" | custom-call | tf_op jit(solution)/shard_map/pallas_call | solution.py:317
  134.8 4.9 %all-to-all-done.3.start_ref = bf16[16,48,128]{2,1,0:T(8,128)(2,1)S(1)} async-done(((bf16[16,48,128]{2,1,0:T(8,128)(2,1)}), bf16[16,48,128]{2,1,0:T(8,128)(2,1)S(1)}, u32[]{:S(2)}, u32[]{:S(2)}) %all-to-all-start.3) | async-done | bytes 196640 | tf_op jit(solution)/shard_map/all_to_all | solution.py:27
  139.7 2.0 %shard_map.151 = bf16[4,256,512]{2,1,0:T(8,128)(2,1)} custom-call(bf16[256,128]{1,0:T(8,128)(2,1)S(1)} %get-tuple-element.31.query_ref, bf16[256,128]{1,0:T(8,128)(2,1)S(1)} %copy-done.2, bf16[256,256]{1,0:T(8,128)(2,1)S(1)} %get-tuple-element.33.value_ref, f32[256,8]{1,0:T(8,128)S(1)} %get-tuple-element.24.update_ref.column_ref, ...), custom_call_target="tpu_custom_call" | custom-call | tf_op jit(solution)/shard_map/pallas_call | solution.py:317
  141.7 3.9 %all-to-all-start.4 = ((bf16[4,256,512]{2,1,0:T(8,128)(2,1)}), bf16[4,256,512]{2,1,0:T(8,128)(2,1)S(1)}, u32[]{:S(2)}, u32[]{:S(2)}) async-start(bf16[4,256,512]{2,1,0:T(8,128)(2,1)} %shard_map.151), calls=%async_computation.4 | async-start | bytes 2097152 | tf_op jit(solution)/shard_map/all_to_all | solution.py:27
  145.6 2.2 %slice-done = bf16[4096,512]{1,0:T(8,128)(2,1)S(1)} async-done(((bf16[4096,1408]{1,0:T(8,128)(2,1)}), bf16[4096,512]{1,0:T(8,128)(2,1)S(1)}, s32[]{:S(2)}) %slice-start) | async-done | bytes 4194328 | tf_op jit(solution)/shard_map/slice | solution.py:460
  149.6 11.2 %all-to-all-done.4.joined_ref = bf16[4,256,512]{2,1,0:T(8,128)(2,1)S(1)} async-done(((bf16[4,256,512]{2,1,0:T(8,128)(2,1)}), bf16[4,256,512]{2,1,0:T(8,128)(2,1)S(1)}, u32[]{:S(2)}, u32[]{:S(2)}) %all-to-all-start.4) | async-done | bytes 1048608 | tf_op jit(solution)/shard_map/all_to_all | solution.py:27
  (53 shorter events, 15.4 us)
Async XLA Ops:
  6.5 15.8 %copy-start.7 = (f32[4096]{0:T(1024)S(1)}, f32[4096]{0:T(1024)}, u32[]{:S(2)}) copy-start(f32[4096]{0:T(1024)} %param.16) | copy-start | bytes 49156
  6.5 123.1 %all-gather.2.cloned.1.call-start = ((), (), s32[]{:S(2)}) async-start(), calls=%async_computation.5 | async-start | bytes 11624448 | tf_op jit(solution)/shard_map/all_gather | solution.py:369
  8.2 26.3 %all-to-all-start = ((bf16[16,32,384]{2,1,0:T(8,128)(2,1)}), bf16[16,32,384]{2,1,0:T(8,128)(2,1)S(1)}, u32[]{:S(2)}, u32[]{:S(2)}) async-start(bf16[16,32,384]{2,1,0:T(8,128)(2,1)} %get-tuple-element.22), calls=%async_computation | async-start | bytes 786432 | tf_op jit(solution)/shard_map/all_to_all | solution.py:27
  20.1 2.3 %copy-start.5 = (bf16[256,4096]{1,0:T(8,128)(2,1)S(1)}, bf16[256,4096]{1,0:T(8,128)(2,1)}, u32[]{:S(2)}) copy-start(bf16[256,4096]{1,0:T(8,128)(2,1)} %param.15) | copy-start | bytes 6291460
  22.3 38.0 %copy-start.6 = (bf16[4096,2,2,1]{0,2,3,1:T(2,128)(2,1)S(1)}, bf16[4096,2,2,1]{0,2,3,1:T(2,128)(2,1)}, u32[]{:S(2)}) copy-start(bf16[4096,2,2,1]{0,2,3,1:T(2,128)(2,1)} %param.20) | copy-start | bytes 98308
  23.0 49.2 %copy-start.8 = (f32[2,256,1]{1,2,0:T(1,128)S(1)}, f32[2,256,1]{1,2,0:T(1,128)}, u32[]{:S(2)}) copy-start(f32[2,256,1]{1,2,0:T(1,128)} %param.23) | copy-start | bytes 6148
  23.0 49.2 %copy-start.9 = (f32[2,1]{0,1:T(1,128)S(1)}, f32[2,1]{0,1:T(1,128)}, u32[]{:S(2)}) copy-start(f32[2,1]{0,1:T(1,128)} %param.22) | copy-start | bytes 28
  23.0 49.2 %copy-start.10 = (f32[2,1]{0,1:T(1,128)S(1)}, f32[2,1]{0,1:T(1,128)}, u32[]{:S(2)}) copy-start(f32[2,1]{0,1:T(1,128)} %param.21) | copy-start | bytes 28
  34.5 10.6 %collective-permute-start = (bf16[8,64,384]{2,1,0:T(8,128)(2,1)S(1)}, bf16[8,64,384]{2,1,0:T(8,128)(2,1)S(1)}, u32[]{:S(2)}, u32[]{:S(2)}) collective-permute-start(bf16[8,64,384]{2,1,0:T(8,128)(2,1)S(1)} %bitcast.36), channel_id=1, source_target_pairs={{0,8},{4,60},{8,16},{12,4},{16,24},{20,12},{24,32},{28,20},{32,40}... | collective-permute-start | bytes 1179656 | tf_op jit(solution)/shard_map/ppermute | solution.py:378
  45.1 10.2 %collective-permute-start.1 = (bf16[8,64,384]{2,1,0:T(8,128)(2,1)S(1)}, bf16[8,64,384]{2,1,0:T(8,128)(2,1)S(1)}, u32[]{:S(2)}, u32[]{:S(2)}) collective-permute-start(bf16[8,64,384]{2,1,0:T(8,128)(2,1)S(1)} %collective-permute-done.refs_1_), channel_id=1, source_target_pairs={{0,8},{4,60},{8,16},{12,4},{16,24},{20,12},{24,32},{28,20},{32,40}... | collective-permute-start | bytes 1179656 | tf_op jit(solution)/shard_map/ppermute | solution.py:378
  55.3 10.2 %collective-permute-start.2 = (bf16[8,64,384]{2,1,0:T(8,128)(2,1)S(1)}, bf16[8,64,384]{2,1,0:T(8,128)(2,1)}, u32[]{:S(2)}, u32[]{:S(2)}) collective-permute-start(bf16[8,64,384]{2,1,0:T(8,128)(2,1)S(1)} %collective-permute-done.1.refs_2_), channel_id=1, source_target_pairs={{0,8},{4,60},{8,16},{12,4},{16,24},{20,12},{24,32},{28,20},{32,40}... | collective-permute-start | bytes 1179656 | tf_op jit(solution)/shard_map/ppermute | solution.py:378
  61.1 12.0 %collective-permute-start.3 = (bf16[8,64,384]{2,1,0:T(8,128)(2,1)S(1)}, bf16[8,64,384]{2,1,0:T(8,128)(2,1)S(1)}, u32[]{:S(2)}, u32[]{:S(2)}) collective-permute-start(bf16[8,64,384]{2,1,0:T(8,128)(2,1)S(1)} %collective-permute-done.refs_1_), channel_id=1, source_target_pairs={{0,4},{4,0},{1,5},{5,1},{2,6},{6,2},{3,7},{7,3},{8,12},{12,8},{9,1... | collective-permute-start | bytes 1179656 | tf_op jit(solution)/shard_map/ppermute | solution.py:380
  63.1 10.1 %collective-permute-start.4 = (bf16[8,64,384]{2,1,0:T(8,128)(2,1)S(1)}, bf16[8,64,384]{2,1,0:T(8,128)(2,1)S(1)}, u32[]{:S(2)}, u32[]{:S(2)}) collective-permute-start(bf16[8,64,384]{2,1,0:T(8,128)(2,1)S(1)} %collective-permute-done.1.refs_2_), channel_id=1, source_target_pairs={{0,4},{4,0},{1,5},{5,1},{2,6},{6,2},{3,7},{7,3},{8,12},{12,8},{9,1... | collective-permute-start | bytes 1179656 | tf_op jit(solution)/shard_map/ppermute | solution.py:380
  65.5 7.7 %collective-permute-start.5 = (bf16[8,64,384]{2,1,0:T(8,128)(2,1)}, bf16[8,64,384]{2,1,0:T(8,128)(2,1)S(1)}, u32[]{:S(2)}, u32[]{:S(2)}) collective-permute-start(bf16[8,64,384]{2,1,0:T(8,128)(2,1)} %collective-permute-done.2.refs_3_), channel_id=1, source_target_pairs={{0,4},{4,0},{1,5},{5,1},{2,6},{6,2},{3,7},{7,3},{8,12},{12,8},{9,1... | collective-permute-start | bytes 1179656 | tf_op jit(solution)/shard_map/ppermute | solution.py:380
  70.3 14.4 %collective-permute-start.6 = (bf16[8,64,384]{2,1,0:T(8,128)(2,1)}, bf16[8,64,384]{2,1,0:T(8,128)(2,1)S(1)}, u32[]{:S(2)}, u32[]{:S(2)}) collective-permute-start(bf16[8,64,384]{2,1,0:T(8,128)(2,1)} %collective-permute-done.2.refs_3_), channel_id=1, source_target_pairs={{0,8},{4,60},{8,16},{12,4},{16,24},{20,12},{24,32},{28,20},{32,40}... | collective-permute-start | bytes 1179656 | tf_op jit(solution)/shard_map/ppermute | solution.py:378
  87.5 21.9 %copy-start.1 = (bf16[256,128]{1,0:T(8,128)(2,1)}, bf16[256,128]{1,0:T(8,128)(2,1)S(1)}, u32[]{:S(2)}) copy-start(bf16[256,128]{1,0:T(8,128)(2,1)S(1)} %get-tuple-element.32.key_ref) | copy-start | bytes 196612
  87.5 42.1 %copy-start.3 = (bf16[3,256]{1,0:T(4,128)(2,1)S(1)}, bf16[3,256]{1,0:T(4,128)(2,1)}, u32[]{:S(2)}) copy-start(bf16[3,256]{1,0:T(4,128)(2,1)} %tap_ref.1) | copy-start | bytes 4612
  109.4 14.6 %all-to-all-start.2 = ((bf16[8,48,128]{2,1,0:T(8,128)(2,1)}), bf16[8,48,128]{2,1,0:T(8,128)(2,1)S(1)}, u32[]{:S(2)}, u32[]{:S(2)}) async-start(bf16[8,48,128]{2,1,0:T(8,128)(2,1)} %get-tuple-element.38), calls=%async_computation.2 | async-start | bytes 196608 | tf_op jit(solution)/shard_map/all_to_all | solution.py:27
  115.9 13.5 %collective-permute-start.7 = (bf16[1,4096]{1,0:T(2,128)(2,1)S(1)}, bf16[1,4096]{1,0:T(2,128)(2,1)S(1)}, u32[]{:S(2)}, u32[]{:S(2)}) collective-permute-start(bf16[1,4096]{1,0:T(2,128)(2,1)S(1)} %get-tuple-element.28), channel_id=1, source_target_pairs={{0,4},{4,8},{8,12},{12,16},{16,20},{20,24},{24,28},{28,32},{32,36}... | collective-permute-start | bytes 24584 | tf_op jit(solution)/shard_map/ppermute | solution.py:33
  117.9 11.6 %collective-permute-start.8 = (bf16[1,4096]{1,0:T(2,128)(2,1)S(1)}, bf16[1,4096]{1,0:T(2,128)(2,1)S(1)}, u32[]{:S(2)}, u32[]{:S(2)}) collective-permute-start(bf16[1,4096]{1,0:T(2,128)(2,1)S(1)} %get-tuple-element.29), channel_id=1, source_target_pairs={{4,0},{8,4},{12,8},{16,12},{20,16},{24,20},{28,24},{32,28},{36,32}... | collective-permute-start | bytes 24584 | tf_op jit(solution)/shard_map/ppermute | solution.py:34
  125.0 14.8 %all-to-all-start.3 = ((bf16[16,48,128]{2,1,0:T(8,128)(2,1)}), bf16[16,48,128]{2,1,0:T(8,128)(2,1)S(1)}, u32[]{:S(2)}, u32[]{:S(2)}) async-start(bf16[16,48,128]{2,1,0:T(8,128)(2,1)} %shard_map.150), calls=%async_computation.3 | async-start | bytes 393216 | tf_op jit(solution)/shard_map/all_to_all | solution.py:27
  129.6 10.2 %copy-start.2 = (bf16[256,128]{1,0:T(8,128)(2,1)S(1)}, bf16[256,128]{1,0:T(8,128)(2,1)}, u32[]{:S(2)}) copy-start(bf16[256,128]{1,0:T(8,128)(2,1)} %copy-done.1) | copy-start | bytes 196612
  129.6 10.2 %copy-start.4 = (f32[256]{0:T(256)S(1)}, f32[256]{0:T(256)}, u32[]{:S(2)}) copy-start(f32[256]{0:T(256)} %param.24) | copy-start | bytes 3076
  141.7 19.1 %all-to-all-start.4 = ((bf16[4,256,512]{2,1,0:T(8,128)(2,1)}), bf16[4,256,512]{2,1,0:T(8,128)(2,1)S(1)}, u32[]{:S(2)}, u32[]{:S(2)}) async-start(bf16[4,256,512]{2,1,0:T(8,128)(2,1)} %shard_map.151), calls=%async_computation.4 | async-start | bytes 2097152 | tf_op jit(solution)/shard_map/all_to_all | solution.py:27
  (2 other events, 3.8 us)
Sparse Core Ops, SparseCore 0:
  10.5 102.0 all-gather.1

commit v5 on v3

--- a/solution.py
+++ b/solution.py
@@ -62,7 +62,7 @@
 
 
 ARRIVAL = (0, -1, 1, -2, 2, -3, 3, -4)
-GROUPS = (3, 4, 1)
+GROUPS = (7, 1)
 
 
 def pack_kernel(query_ref, key_ref, value_ref, outer_ref, inner_ref, given_ref, out_ref, whole_ref, block_ref):
@@ -375,7 +375,24 @@
     row = lax.axis_index("sp_1")
     normed = row_norm(tokens, norm_gain)
 
-    block, normed = lax.optimization_barrier((block, normed))
+    gates = lax.dot_general(
+        w_gates.reshape(-1, 4), normed, (((0,), (1,)), ((), ())), preferred_element_type=F32
+    ).reshape(2, 2, length)
+    in_gate = gates[:, 0] + input_bias
+    log_forget = jax.nn.log_sigmoid(gates[:, 1] + forget_bias) + decay_shift[:, :, 0]
+    rows, columns, numbers = on_core(
+        gate_kernel,
+        (
+            jax.ShapeDtypeStruct((4, length), F32),
+            jax.ShapeDtypeStruct((length, 8), F32),
+            jax.ShapeDtypeStruct((4, 128), F32),
+        ),
+        log_forget,
+        in_gate,
+    )
+    block, normed, rows, columns, numbers = lax.optimization_barrier(
+        (block, normed, rows, columns, numbers)
+    )
     up = down = block
     pieces = [block]
     for k in range(4):
@@ -391,21 +408,6 @@
     for count, group in zip(GROUPS, tuple(groups)):
         groups.append(lax.ppermute(group, "sp_2", ring(2, 1)))
 
-    gates = lax.dot_general(
-        w_gates.reshape(-1, 4), normed, (((0,), (1,)), ((), ())), preferred_element_type=F32
-    ).reshape(2, 2, length)
-    in_gate = gates[:, 0] + input_bias
-    log_forget = jax.nn.log_sigmoid(gates[:, 1] + forget_bias) + decay_shift[:, :, 0]
-    rows, columns, numbers = on_core(
-        gate_kernel,
-        (
-            jax.ShapeDtypeStruct((4, length), F32),
-            jax.ShapeDtypeStruct((length, 8), F32),
-            jax.ShapeDtypeStruct((4, 128), F32),
-        ),
-        log_forget,
-        in_gate,
-    )
     block = jax.ShapeDtypeStruct((members, ROWS, 128), BF16)
     state, keys, values = on_core(
         state_kernel,

time: 168 us -> 162 us (0.964)
  waiting for transfers between devices: 43.2 us -> 35.9 us
  local copies, waits for them, and re-layouts: 6.48 us -> 9.26 us
  other arithmetic: 5.7 us -> 3.13 us
  blocking collectives: 19.3 us -> 21.7 us
    all_to_all x4, waiting for transfers between devices: 26.4 us -> 20.9 us  [swapped(): return lax.all_to_all(value, axes, split_axis=0, concat_axis=0, tiled=True)]
    ppermute x3 -> x2, starting transfers between devices: 12.6 us -> 8.39 us  [body(): groups.append(lax.ppermute(group, 'sp_2', ring(2, 1)))]
    ppermute x4, waiting for transfers between devices: 15.7 us -> 12.3 us  [body(): up = lax.ppermute(up, 'sp_1', ring(8, 1))]
    another operation x2 -> x0, other arithmetic: 2.57 us -> none  [body(): groups.append(jnp.stack(pieces[at:at + count]))]
    all_to_all x1, blocking collectives: 19.3 us -> 21.7 us  [swapped(): return lax.all_to_all(value, axes, split_axis=0, concat_axis=0, tiled=True)]
    unnamed x40 -> x32, local copies, waits for them, and re-layouts: 2.35 us -> 4.32 us
  transfers between devices with their start and end apart: 17 -> 16, of which waited for: 10 -> 10; matrix products, arithmetic and copies ran while one was open for 5% -> 5% of each run, Pallas kernels for 7% -> 7%
where the time goes in v5:
time: 162 us; the launch traced here: 161 us
  starting transfers between devices  60.4 us (37%)
  waiting for transfers between devices  35.9 us (22%)
  blocking collectives  21.7 us (13%)
  Pallas kernels  16.7 us (10%)
  between operations  13.8 us (9%)
  local copies, waits for them, and re-layouts  9.26 us (6%)
  other arithmetic  3.13 us (2%)
    all_to_all x4, starting transfers between devices, swapped(): return lax.all_to_all(value, axes, split_axis=0, concat_axis=0, tiled=True)  23.5 us
    all_to_all x1, blocking collectives, swapped(): return lax.all_to_all(value, axes, split_axis=0, concat_axis=0, tiled=True)  21.7 us
    all_to_all x4, waiting for transfers between devices, swapped(): return lax.all_to_all(value, axes, split_axis=0, concat_axis=0, tiled=True)  20.9 us
    pallas_call x8, Pallas kernels, on_core(): pl.pallas_call(kernel, out_shape=out, in_specs=[smem] * scalars + [vmem]...  16.7 us
    ppermute x3, starting transfers between devices, body(): down = lax.ppermute(down, 'sp_1', ring(8, -1))  13 us
    ppermute x4, waiting for transfers between devices, body(): up = lax.ppermute(up, 'sp_1', ring(8, 1))  12.3 us
    ppermute x4, starting transfers between devices, body(): up = lax.ppermute(up, 'sp_1', ring(8, 1))  9.94 us
    ppermute x2, starting transfers between devices, body(): groups.append(lax.ppermute(group, 'sp_2', ring(2, 1)))  8.39 us
  transfers between devices with their start and end apart: 16, of which 10 were waited for; matrix products, arithmetic and copies ran while one was open for 5% of the time, Pallas kernels for 7%

profile of v5, /device:TPU:1, one launch (start us, length us, event | category | flops | bytes accessed | tf_op | source)
XLA Modules:
  0.0 161.4 jit_solution(4215532522116198234)
XLA Ops:
  8.1 10.9 %all-to-all-start = ((bf16[8,32,384]{2,1,0:T(8,128)(2,1)}), bf16[8,32,384]{2,1,0:T(8,128)(2,1)}, u32[]{:S(2)}, u32[]{:S(2)}) async-start(bf16[8,32,384]{2,1,0:T(8,128)(2,1)} %get-tuple-element.25), calls=%async_computation | async-start | bytes 393216 | tf_op jit(solution)/shard_map/all_to_all | solution.py:27
  19.8 2.2 %fusion = f32[256]{0:T(256)S(1)} fusion(bf16[256,4096]{1,0:T(8,128)(2,1)} %param.15), kind=kLoop, calls=%fused_computation.2 | loop fusion | flops 3145472 | bytes 2098176 | tf_op jit(solution)/shard_map/reduce_sum | solution.py:22
  25.0 3.1 %all-to-all-done = bf16[8,32,384]{2,1,0:T(8,128)(2,1)} async-done(((bf16[8,32,384]{2,1,0:T(8,128)(2,1)}), bf16[8,32,384]{2,1,0:T(8,128)(2,1)}, u32[]{:S(2)}, u32[]{:S(2)}) %all-to-all-start) | async-done | bytes 196640 | tf_op jit(solution)/shard_map/all_to_all | solution.py:27
  28.1 3.2 %collective-permute-start = (bf16[8,32,384]{2,1,0:T(8,128)(2,1)}, bf16[8,32,384]{2,1,0:T(8,128)(2,1)S(1)}, u32[]{:S(2)}, u32[]{:S(2)}) collective-permute-start(bf16[8,32,384]{2,1,0:T(8,128)(2,1)} %all-to-all-done), channel_id=1, source_target_pairs={{0,8},{8,16},{16,24},{24,32},{32,40},{40,48},{48,56},{56,0},{1,9},... | collective-permute-start | bytes 589832 | tf_op jit(solution)/shard_map/ppermute | solution.py:399
  31.3 3.8 %collective-permute-start.1 = (bf16[8,32,384]{2,1,0:T(8,128)(2,1)}, bf16[8,32,384]{2,1,0:T(8,128)(2,1)S(1)}, u32[]{:S(2)}, u32[]{:S(2)}) collective-permute-start(bf16[8,32,384]{2,1,0:T(8,128)(2,1)} %all-to-all-done), channel_id=1, source_target_pairs={{0,56},{8,0},{16,8},{24,16},{32,24},{40,32},{48,40},{56,48},{1,57}... | collective-permute-start | bytes 589832 | tf_op jit(solution)/shard_map/ppermute | solution.py:402
  39.3 4.6 %collective-permute-start.3 = (bf16[8,32,384]{2,1,0:T(8,128)(2,1)S(1)}, bf16[8,32,384]{2,1,0:T(8,128)(2,1)S(1)}, u32[]{:S(2)}, u32[]{:S(2)}) collective-permute-start(bf16[8,32,384]{2,1,0:T(8,128)(2,1)S(1)} %collective-permute-done.1), channel_id=1, source_target_pairs={{0,56},{8,0},{16,8},{24,16},{32,24},{40,32},{48,40},{56,48},{1,57}... | collective-permute-start | bytes 589832 | tf_op jit(solution)/shard_map/ppermute | solution.py:402
  47.7 4.6 %collective-permute-start.5 = (bf16[8,32,384]{2,1,0:T(8,128)(2,1)S(1)}, bf16[8,32,384]{2,1,0:T(8,128)(2,1)S(1)}, u32[]{:S(2)}, u32[]{:S(2)}) collective-permute-start(bf16[8,32,384]{2,1,0:T(8,128)(2,1)S(1)} %collective-permute-done.3), channel_id=1, source_target_pairs={{0,56},{8,0},{16,8},{24,16},{32,24},{40,32},{48,40},{56,48},{1,57}... | collective-permute-start | bytes 589832 | tf_op jit(solution)/shard_map/ppermute | solution.py:402
  55.2 5.9 %collective-permute-start.7 = (bf16[7,8,32,384]{3,2,1,0:T(8,128)(2,1)S(1)}, bf16[7,8,32,384]{3,2,1,0:T(8,128)(2,1)}, u32[]{:S(2)}, u32[]{:S(2)}) collective-permute-start(bf16[7,8,32,384]{3,2,1,0:T(8,128)(2,1)S(1)} %bitcast_dynamic-update-slice_fusion.refs_0_), channel_id=1, source_target_pairs={{0,4},{4,0},{1,5},{5,1},{2,6},{6,2},{3,7},{7,3},{8,12},{12,8},{9,1... | collective-permute-start | bytes 4128776 | tf_op jit(solution)/shard_map/ppermute | solution.py:409
  61.2 2.9 %collective-permute-start.6 = (bf16[8,32,384]{2,1,0:T(8,128)(2,1)S(1)}, bf16[8,32,384]{2,1,0:T(8,128)(2,1)}, u32[]{:S(2)}, u32[]{:S(2)}) collective-permute-start(bf16[8,32,384]{2,1,0:T(8,128)(2,1)S(1)} %collective-permute-done.4), channel_id=1, source_target_pairs={{0,8},{8,16},{16,24},{24,32},{32,40},{40,48},{48,56},{56,0},{1,9},... | collective-permute-start | bytes 589832 | tf_op jit(solution)/shard_map/ppermute | solution.py:399
  64.1 7.7 %collective-permute-done.6 = bf16[8,32,384]{2,1,0:T(8,128)(2,1)} collective-permute-done((bf16[8,32,384]{2,1,0:T(8,128)(2,1)S(1)}, bf16[8,32,384]{2,1,0:T(8,128)(2,1)}, u32[]{:S(2)}, u32[]{:S(2)}) %collective-permute-start.6) | collective-permute-done | bytes 196640 | tf_op jit(solution)/shard_map/ppermute | solution.py:399
  71.8 2.5 %collective-permute-start.8 = (bf16[1,8,32,384]{3,2,1,0:T(8,128)(2,1)}, bf16[1,8,32,384]{3,2,1,0:T(8,128)(2,1)}, u32[]{:S(2)}, u32[]{:S(2)}) collective-permute-start(bf16[1,8,32,384]{3,2,1,0:T(8,128)(2,1)} %bitcast.14.refs_1_), channel_id=1, source_target_pairs={{0,4},{4,0},{1,5},{5,1},{2,6},{6,2},{3,7},{7,3},{8,12},{12,8},{9,1... | collective-permute-start | bytes 589832 | tf_op jit(solution)/shard_map/ppermute | solution.py:409
  76.6 3.3 %shard_map.147 = (bf16[16,48,128]{2,1,0:T(8,128)(2,1)S(1)}, bf16[256,128]{1,0:T(8,128)(2,1)S(1)}, bf16[256,256]{1,0:T(8,128)(2,1)S(1)}) custom-call(s32[2]{0:T(128)S(1)} %pad_add_fusion.place_ref, bf16[256,4096]{1,0:T(8,128)(2,1)S(1)} %fusion.2.normed_ref, f32[256,8]{1,0:T(8,128)S(1)} %copy-done.2, f32[4,128]{1,0:T(4,128)S(1)} %get-tuple-element.31.number_ref, ...), custom_call_target="tpu_custom_call" | custom-call | tf_op jit(solution)/shard_map/pallas_call | solution.py:321
  80.0 21.7 %all_to_all.25.state_ref = bf16[16,48,128]{2,1,0:T(8,128)(2,1)S(1)} all-to-all(bf16[16,48,128]{2,1,0:T(8,128)(2,1)S(1)} %get-tuple-element.42), channel_id=1, replica_groups=mesh['sp_0'=8,'sp_1'=8,'sp_2'=2,'tp'=4] {'sp_1','sp_2'}, dimensions={0} | all-to-all | bytes 393216 | tf_op jit(solution)/shard_map/all_to_all | solution.py:27
  102.5 3.4 %all-to-all-start.2 = ((bf16[8,48,128]{2,1,0:T(8,128)(2,1)}), bf16[8,48,128]{2,1,0:T(8,128)(2,1)S(1)}, u32[]{:S(2)}, u32[]{:S(2)}) async-start(bf16[8,48,128]{2,1,0:T(8,128)(2,1)} %get-tuple-element.44), calls=%async_computation.2 | async-start | bytes 196608 | tf_op jit(solution)/shard_map/all_to_all | solution.py:27
  105.9 2.3 %collective-permute-start.10 = (bf16[1,4096]{1,0:T(2,128)(2,1)S(1)}, bf16[1,4096]{1,0:T(2,128)(2,1)S(1)}, u32[]{:S(2)}, u32[]{:S(2)}) collective-permute-start(bf16[1,4096]{1,0:T(2,128)(2,1)S(1)} %get-tuple-element.35), channel_id=1, source_target_pairs={{4,0},{8,4},{12,8},{16,12},{20,16},{24,20},{28,24},{32,28},{36,32}... | collective-permute-start | bytes 24584 | tf_op jit(solution)/shard_map/ppermute | solution.py:34
  108.2 3.3 %collective-permute-start.9 = (bf16[1,4096]{1,0:T(2,128)(2,1)S(1)}, bf16[1,4096]{1,0:T(2,128)(2,1)S(1)}, u32[]{:S(2)}, u32[]{:S(2)}) collective-permute-start(bf16[1,4096]{1,0:T(2,128)(2,1)S(1)} %get-tuple-element.34), channel_id=1, source_target_pairs={{0,4},{4,8},{8,12},{12,16},{16,20},{20,24},{24,28},{28,32},{32,36}... | collective-permute-start | bytes 24584 | tf_op jit(solution)/shard_map/ppermute | solution.py:33
  114.2 5.1 %all-to-all-start.3 = ((bf16[16,48,128]{2,1,0:T(8,128)(2,1)}), bf16[16,48,128]{2,1,0:T(8,128)(2,1)S(1)}, u32[]{:S(2)}, u32[]{:S(2)}) async-start(bf16[16,48,128]{2,1,0:T(8,128)(2,1)} %shard_map.150), calls=%async_computation.3 | async-start | bytes 393216 | tf_op jit(solution)/shard_map/all_to_all | solution.py:27
  119.5 5.3 %shard_map.148 = (bf16[256,128]{1,0:T(8,128)(2,1)S(1)}, bf16[256,256]{1,0:T(8,128)(2,1)S(1)}) custom-call(bf16[256,4096]{1,0:T(8,128)(2,1)S(1)} %fusion.2.normed_ref, bf16[16,4096]{1,0:T(8,128)(2,1)S(1)} %maximum_maximum_fusion.edge_ref, bf16[3,256]{1,0:T(4,128)(2,1)S(1)} %copy-done.6, bf16[4096,1408]{1,0:T(8,128)(2,1)} %all-gather.2.cloned.1.call-done.whole_ref), custom_call_target="tpu_custom_call" | custom-call | tf_op jit(solution)/shard_map/pallas_call | solution.py:321
  124.7 4.8 %all-to-all-done.3.start_ref = bf16[16,48,128]{2,1,0:T(8,128)(2,1)S(1)} async-done(((bf16[16,48,128]{2,1,0:T(8,128)(2,1)}), bf16[16,48,128]{2,1,0:T(8,128)(2,1)S(1)}, u32[]{:S(2)}, u32[]{:S(2)}) %all-to-all-start.3) | async-done | bytes 196640 | tf_op jit(solution)/shard_map/all_to_all | solution.py:27
  129.6 2.0 %shard_map.151 = bf16[4,256,512]{2,1,0:T(8,128)(2,1)} custom-call(bf16[256,128]{1,0:T(8,128)(2,1)S(1)} %get-tuple-element.37.query_ref, bf16[256,128]{1,0:T(8,128)(2,1)S(1)} %get-tuple-element.38.key_ref, bf16[256,256]{1,0:T(8,128)(2,1)S(1)} %copy-done.5, f32[256,8]{1,0:T(8,128)S(1)} %copy-done.3, f32[4,256]{1,0:T(4,128)S(1)} %get-tuple-element.40.row_ref, ...), custom_call_target="tpu_custom_call" | custom-call | tf_op jit(solution)/shard_map/pallas_call | solution.py:321
  131.5 4.2 %all-to-all-start.4 = ((bf16[4,256,512]{2,1,0:T(8,128)(2,1)}), bf16[4,256,512]{2,1,0:T(8,128)(2,1)S(1)}, u32[]{:S(2)}, u32[]{:S(2)}) async-start(bf16[4,256,512]{2,1,0:T(8,128)(2,1)} %shard_map.151), calls=%async_computation.4 | async-start | bytes 2097152 | tf_op jit(solution)/shard_map/all_to_all | solution.py:27
  135.7 2.2 %slice-done = bf16[4096,512]{1,0:T(8,128)(2,1)S(1)} async-done(((bf16[4096,1408]{1,0:T(8,128)(2,1)}), bf16[4096,512]{1,0:T(8,128)(2,1)S(1)}, s32[]{:S(2)}) %slice-start) | async-done | bytes 4194328 | tf_op jit(solution)/shard_map/slice | solution.py:473
  139.7 11.2 %all-to-all-done.4.joined_ref = bf16[4,256,512]{2,1,0:T(8,128)(2,1)S(1)} async-done(((bf16[4,256,512]{2,1,0:T(8,128)(2,1)}), bf16[4,256,512]{2,1,0:T(8,128)(2,1)S(1)}, u32[]{:S(2)}, u32[]{:S(2)}) %all-to-all-start.4) | async-done | bytes 1048608 | tf_op jit(solution)/shard_map/all_to_all | solution.py:27
  152.5 2.0 %shard_map.152 = bf16[256,1024]{1,0:T(8,128)(2,1)} custom-call(bf16[4,256,512]{2,1,0:T(8,128)(2,1)S(1)} %all-to-all-done.4.joined_ref, bf16[4,512,512]{2,1,0:T(8,128)(2,1)S(1)} %bitcast.49, bf16[4,512,512]{2,1,0:T(8,128)(2,1)S(1)} %bitcast.48), custom_call_target="tpu_custom_call" | custom-call | tf_op jit(solution)/shard_map/pallas_call | solution.py:321
  (67 shorter events, 25.5 us)
Async XLA Ops:
  6.5 15.5 %copy-start.9 = (f32[4096]{0:T(1024)S(1)}, f32[4096]{0:T(1024)}, u32[]{:S(2)}) copy-start(f32[4096]{0:T(1024)} %param.16) | copy-start | bytes 49156
  6.5 112.9 %all-gather.2.cloned.1.call-start = ((), (), s32[]{:S(2)}) async-start(), calls=%async_computation.5 | async-start | bytes 11624448 | tf_op jit(solution)/shard_map/all_gather | solution.py:373
  8.1 20.0 %all-to-all-start = ((bf16[8,32,384]{2,1,0:T(8,128)(2,1)}), bf16[8,32,384]{2,1,0:T(8,128)(2,1)}, u32[]{:S(2)}, u32[]{:S(2)}) async-start(bf16[8,32,384]{2,1,0:T(8,128)(2,1)} %get-tuple-element.25), calls=%async_computation | async-start | bytes 393216 | tf_op jit(solution)/shard_map/all_to_all | solution.py:27
  19.8 2.3 %copy-start.8 = (bf16[256,4096]{1,0:T(8,128)(2,1)S(1)}, bf16[256,4096]{1,0:T(8,128)(2,1)}, u32[]{:S(2)}) copy-start(bf16[256,4096]{1,0:T(8,128)(2,1)} %param.15) | copy-start | bytes 6291460
  28.1 9.2 %collective-permute-start = (bf16[8,32,384]{2,1,0:T(8,128)(2,1)}, bf16[8,32,384]{2,1,0:T(8,128)(2,1)S(1)}, u32[]{:S(2)}, u32[]{:S(2)}) collective-permute-start(bf16[8,32,384]{2,1,0:T(8,128)(2,1)} %all-to-all-done), channel_id=1, source_target_pairs={{0,8},{8,16},{16,24},{24,32},{32,40},{40,48},{48,56},{56,0},{1,9},... | collective-permute-start | bytes 589832 | tf_op jit(solution)/shard_map/ppermute | solution.py:399
  31.3 8.0 %collective-permute-start.1 = (bf16[8,32,384]{2,1,0:T(8,128)(2,1)}, bf16[8,32,384]{2,1,0:T(8,128)(2,1)S(1)}, u32[]{:S(2)}, u32[]{:S(2)}) collective-permute-start(bf16[8,32,384]{2,1,0:T(8,128)(2,1)} %all-to-all-done), channel_id=1, source_target_pairs={{0,56},{8,0},{16,8},{24,16},{32,24},{40,32},{48,40},{56,48},{1,57}... | collective-permute-start | bytes 589832 | tf_op jit(solution)/shard_map/ppermute | solution.py:402
  37.3 8.4 %collective-permute-start.2 = (bf16[8,32,384]{2,1,0:T(8,128)(2,1)S(1)}, bf16[8,32,384]{2,1,0:T(8,128)(2,1)S(1)}, u32[]{:S(2)}, u32[]{:S(2)}) collective-permute-start(bf16[8,32,384]{2,1,0:T(8,128)(2,1)S(1)} %collective-permute-done), channel_id=1, source_target_pairs={{0,8},{8,16},{16,24},{24,32},{32,40},{40,48},{48,56},{56,0},{1,9},... | collective-permute-start | bytes 589832 | tf_op jit(solution)/shard_map/ppermute | solution.py:399
  39.3 8.4 %collective-permute-start.3 = (bf16[8,32,384]{2,1,0:T(8,128)(2,1)S(1)}, bf16[8,32,384]{2,1,0:T(8,128)(2,1)S(1)}, u32[]{:S(2)}, u32[]{:S(2)}) collective-permute-start(bf16[8,32,384]{2,1,0:T(8,128)(2,1)S(1)} %collective-permute-done.1), channel_id=1, source_target_pairs={{0,56},{8,0},{16,8},{24,16},{32,24},{40,32},{48,40},{56,48},{1,57}... | collective-permute-start | bytes 589832 | tf_op jit(solution)/shard_map/ppermute | solution.py:402
  45.8 8.0 %collective-permute-start.4 = (bf16[8,32,384]{2,1,0:T(8,128)(2,1)S(1)}, bf16[8,32,384]{2,1,0:T(8,128)(2,1)S(1)}, u32[]{:S(2)}, u32[]{:S(2)}) collective-permute-start(bf16[8,32,384]{2,1,0:T(8,128)(2,1)S(1)} %collective-permute-done.2), channel_id=1, source_target_pairs={{0,8},{8,16},{16,24},{24,32},{32,40},{40,48},{48,56},{56,0},{1,9},... | collective-permute-start | bytes 589832 | tf_op jit(solution)/shard_map/ppermute | solution.py:399
  47.7 7.5 %collective-permute-start.5 = (bf16[8,32,384]{2,1,0:T(8,128)(2,1)S(1)}, bf16[8,32,384]{2,1,0:T(8,128)(2,1)S(1)}, u32[]{:S(2)}, u32[]{:S(2)}) collective-permute-start(bf16[8,32,384]{2,1,0:T(8,128)(2,1)S(1)} %collective-permute-done.3), channel_id=1, source_target_pairs={{0,56},{8,0},{16,8},{24,16},{32,24},{40,32},{48,40},{56,48},{1,57}... | collective-permute-start | bytes 589832 | tf_op jit(solution)/shard_map/ppermute | solution.py:402
  55.2 20.5 %collective-permute-start.7 = (bf16[7,8,32,384]{3,2,1,0:T(8,128)(2,1)S(1)}, bf16[7,8,32,384]{3,2,1,0:T(8,128)(2,1)}, u32[]{:S(2)}, u32[]{:S(2)}) collective-permute-start(bf16[7,8,32,384]{3,2,1,0:T(8,128)(2,1)S(1)} %bitcast_dynamic-update-slice_fusion.refs_0_), channel_id=1, source_target_pairs={{0,4},{4,0},{1,5},{5,1},{2,6},{6,2},{3,7},{7,3},{8,12},{12,8},{9,1... | collective-permute-start | bytes 4128776 | tf_op jit(solution)/shard_map/ppermute | solution.py:409
  61.2 10.7 %collective-permute-start.6 = (bf16[8,32,384]{2,1,0:T(8,128)(2,1)S(1)}, bf16[8,32,384]{2,1,0:T(8,128)(2,1)}, u32[]{:S(2)}, u32[]{:S(2)}) collective-permute-start(bf16[8,32,384]{2,1,0:T(8,128)(2,1)S(1)} %collective-permute-done.4), channel_id=1, source_target_pairs={{0,8},{8,16},{16,24},{24,32},{32,40},{40,48},{48,56},{56,0},{1,9},... | collective-permute-start | bytes 589832 | tf_op jit(solution)/shard_map/ppermute | solution.py:399
  71.8 3.9 %collective-permute-start.8 = (bf16[1,8,32,384]{3,2,1,0:T(8,128)(2,1)}, bf16[1,8,32,384]{3,2,1,0:T(8,128)(2,1)}, u32[]{:S(2)}, u32[]{:S(2)}) collective-permute-start(bf16[1,8,32,384]{3,2,1,0:T(8,128)(2,1)} %bitcast.14.refs_1_), channel_id=1, source_target_pairs={{0,4},{4,0},{1,5},{5,1},{2,6},{6,2},{3,7},{7,3},{8,12},{12,8},{9,1... | collective-permute-start | bytes 589832 | tf_op jit(solution)/shard_map/ppermute | solution.py:409
  80.0 22.5 %copy-start.4 = (bf16[256,256]{1,0:T(8,128)(2,1)}, bf16[256,256]{1,0:T(8,128)(2,1)S(1)}, u32[]{:S(2)}) copy-start(bf16[256,256]{1,0:T(8,128)(2,1)S(1)} %get-tuple-element.39.value_ref) | copy-start | bytes 393220
  80.0 39.5 %copy-start.6 = (bf16[3,256]{1,0:T(4,128)(2,1)S(1)}, bf16[3,256]{1,0:T(4,128)(2,1)}, u32[]{:S(2)}) copy-start(bf16[3,256]{1,0:T(4,128)(2,1)} %tap_ref.1) | copy-start | bytes 4612
  102.5 10.8 %all-to-all-start.2 = ((bf16[8,48,128]{2,1,0:T(8,128)(2,1)}), bf16[8,48,128]{2,1,0:T(8,128)(2,1)S(1)}, u32[]{:S(2)}, u32[]{:S(2)}) async-start(bf16[8,48,128]{2,1,0:T(8,128)(2,1)} %get-tuple-element.44), calls=%async_computation.2 | async-start | bytes 196608 | tf_op jit(solution)/shard_map/all_to_all | solution.py:27
  105.9 13.4 %collective-permute-start.10 = (bf16[1,4096]{1,0:T(2,128)(2,1)S(1)}, bf16[1,4096]{1,0:T(2,128)(2,1)S(1)}, u32[]{:S(2)}, u32[]{:S(2)}) collective-permute-start(bf16[1,4096]{1,0:T(2,128)(2,1)S(1)} %get-tuple-element.35), channel_id=1, source_target_pairs={{4,0},{8,4},{12,8},{16,12},{20,16},{24,20},{28,24},{32,28},{36,32}... | collective-permute-start | bytes 24584 | tf_op jit(solution)/shard_map/ppermute | solution.py:34
  108.2 11.1 %collective-permute-start.9 = (bf16[1,4096]{1,0:T(2,128)(2,1)S(1)}, bf16[1,4096]{1,0:T(2,128)(2,1)S(1)}, u32[]{:S(2)}, u32[]{:S(2)}) collective-permute-start(bf16[1,4096]{1,0:T(2,128)(2,1)S(1)} %get-tuple-element.34), channel_id=1, source_target_pairs={{0,4},{4,8},{8,12},{12,16},{16,20},{20,24},{24,28},{28,32},{32,36}... | collective-permute-start | bytes 24584 | tf_op jit(solution)/shard_map/ppermute | solution.py:33
  114.2 15.4 %all-to-all-start.3 = ((bf16[16,48,128]{2,1,0:T(8,128)(2,1)}), bf16[16,48,128]{2,1,0:T(8,128)(2,1)S(1)}, u32[]{:S(2)}, u32[]{:S(2)}) async-start(bf16[16,48,128]{2,1,0:T(8,128)(2,1)} %shard_map.150), calls=%async_computation.3 | async-start | bytes 393216 | tf_op jit(solution)/shard_map/all_to_all | solution.py:27
  119.4 10.2 %copy-start.3 = (f32[256,8]{1,0:T(8,128)S(1)}, f32[256,8]{1,0:T(8,128)}, u32[]{:S(2)}) copy-start(f32[256,8]{1,0:T(8,128)} %copy-done.1) | copy-start | bytes 24580
  119.4 10.2 %copy-start.5 = (bf16[256,256]{1,0:T(8,128)(2,1)S(1)}, bf16[256,256]{1,0:T(8,128)(2,1)}, u32[]{:S(2)}) copy-start(bf16[256,256]{1,0:T(8,128)(2,1)} %copy-done.4) | copy-start | bytes 393220
  119.4 10.1 %copy-start.7 = (f32[256]{0:T(256)S(1)}, f32[256]{0:T(256)}, u32[]{:S(2)}) copy-start(f32[256]{0:T(256)} %param.24) | copy-start | bytes 3076
  131.5 19.4 %all-to-all-start.4 = ((bf16[4,256,512]{2,1,0:T(8,128)(2,1)}), bf16[4,256,512]{2,1,0:T(8,128)(2,1)S(1)}, u32[]{:S(2)}, u32[]{:S(2)}) async-start(bf16[4,256,512]{2,1,0:T(8,128)(2,1)} %shard_map.151), calls=%async_computation.4 | async-start | bytes 2097152 | tf_op jit(solution)/shard_map/all_to_all | solution.py:27
  135.7 2.2 %slice-start = ((bf16[4096,1408]{1,0:T(8,128)(2,1)}), bf16[4096,512]{1,0:T(8,128)(2,1)S(1)}, s32[]{:S(2)}) async-start(bf16[4096,1408]{1,0:T(8,128)(2,1)} %all-gather.2.cloned.1.call-done.whole_ref), calls=%async_computation.6 | async-start | bytes 8388608 | tf_op jit(solution)/shard_map/slice | solution.py:473
  (6 other events, 5.3 us)
Sparse Core Ops, SparseCore 0:
  10.5 100.7 all-gather.1

commit v6 on v5

--- a/solution.py
+++ b/solution.py
@@ -62,7 +62,7 @@
 
 
 ARRIVAL = (0, -1, 1, -2, 2, -3, 3, -4)
-GROUPS = (7, 1)
+GROUPS = (3, 4, 1)
 
 
 def pack_kernel(query_ref, key_ref, value_ref, outer_ref, inner_ref, given_ref, out_ref, whole_ref, block_ref):
@@ -213,16 +213,30 @@
         start_ref[i, NORMERS:, :] = jnp.concatenate(rows, axis=0)
 
 
-def read_kernel(query_ref, key_ref, value_ref, column_ref, row_ref, gain_ref, conv_ref, start_ref, out_ref):
+def local_kernel(query_ref, key_ref, value_ref, column_ref, row_ref, local_ref, sum_ref):
     length = query_ref.shape[0]
-    queries = query_ref[...]
     values = value_ref[...]
-    scale = DQK ** (-0.5)
-    products = scale * lax.dot_general(
-        queries, key_ref[...], (((1,), (1,)), ((), ())), preferred_element_type=F32
+    products = DQK ** (-0.5) * lax.dot_general(
+        query_ref[...], key_ref[...], (((1,), (1,)), ((), ())), preferred_element_type=F32
     )
     t = lax.broadcasted_iota(jnp.int32, (length, length), 0)
     s = lax.broadcasted_iota(jnp.int32, (length, length), 1)
+    for d in range(2):
+        running = column_ref[:, 2 + d : 3 + d]
+        seen = (t <= s) if d else (t >= s)
+        log_weight = jnp.where(
+            seen, running - row_ref[d : d + 1, :] + row_ref[2 + d : 3 + d, :], -jnp.inf
+        )
+        most = jnp.max(log_weight, axis=-1, keepdims=True)
+        scores = products * jnp.exp(log_weight - most)
+        local_ref[d] = jnp.dot(scores.astype(BF16), values, preferred_element_type=F32)
+        sum_ref[:, d : d + 1] = jnp.sum(scores, axis=-1, keepdims=True)
+        sum_ref[:, 2 + d : 3 + d] = most
+
+
+def read_kernel(query_ref, local_ref, sum_ref, column_ref, gain_ref, conv_ref, start_ref, out_ref):
+    queries = query_ref[...]
+    scale = DQK ** (-0.5)
     share = NORMERS // 2
     last = start_ref[0, NORMERS:, :].astype(F32)
     summed = None
@@ -230,21 +244,15 @@
         memory = start_ref[:, d * share : (d + 1) * share, :].reshape(DV, DQK)
         normer = last[d : d + 1]
         stable = from_terms(last, 2 + 3 * d)[:, :1]
-        running = column_ref[:, 2 + d : 3 + d]
-        seen = (t <= s) if d else (t >= s)
-        log_weight = jnp.where(
-            seen, running - row_ref[d : d + 1, :] + row_ref[2 + d : 3 + d, :], -jnp.inf
-        )
-        carried = running + stable
-        highest = jnp.maximum(carried, jnp.max(log_weight, axis=-1, keepdims=True))
-        scores = products * jnp.exp(log_weight - highest)
+        carried = column_ref[:, 2 + d : 3 + d] + stable
+        most = sum_ref[:, 2 + d : 3 + d]
+        highest = jnp.maximum(carried, most)
+        local_weight = jnp.exp(most - highest)
         carry_weight = scale * jnp.exp(carried - highest)
-        numerator = jnp.dot(scores.astype(BF16), values, preferred_element_type=F32)
-        numerator += carry_weight * lax.dot_general(
+        numerator = local_weight * local_ref[d] + carry_weight * lax.dot_general(
             queries, memory, (((1,), (1,)), ((), ())), preferred_element_type=F32
         )
-        denominator = jnp.sum(scores, axis=-1, keepdims=True)
-        denominator += carry_weight * jnp.sum(
+        denominator = local_weight * sum_ref[:, d : d + 1] + carry_weight * jnp.sum(
             queries.astype(F32) * normer, axis=-1, keepdims=True
         )
         result = numerator / jnp.maximum(jnp.abs(denominator), jnp.exp(-highest))
@@ -457,14 +465,26 @@
     )
     start = on_core(far_kernel, block, plane[None], near, far, scalars=1)
     start = swapped(start, PLANE)
-    joined = on_core(
-        read_kernel,
-        jax.ShapeDtypeStruct((4, length, 2 * DV), BF16),
+    local, sums = on_core(
+        local_kernel,
+        (
+            jax.ShapeDtypeStruct((2, length, DV), F32),
+            jax.ShapeDtypeStruct((length, 4), F32),
+        ),
         queries,
         keys,
         values,
         columns,
         rows,
+    )
+    start, local, sums = lax.optimization_barrier((start, local, sums))
+    joined = on_core(
+        read_kernel,
+        jax.ShapeDtypeStruct((4, length, 2 * DV), BF16),
+        queries,
+        local,
+        sums,
+        columns,
         head_gain[None],
         conv_out,
         start,

time: 162 us -> 167 us (1.031)
  starting transfers between devices: 60.4 us -> 63.6 us
    ppermute x2 -> x3, starting transfers between devices: 8.39 us -> 13.3 us  [body(): groups.append(lax.ppermute(group, 'sp_2', ring(2, 1)))]
    unnamed x32 -> x28, local copies, waits for them, and re-layouts: 4.32 us -> 3.21 us
    pallas_call x8 -> x9, Pallas kernels: 16.7 us -> 16.8 us  [on_core(): pl.pallas_call(kernel, out_shape=out, in_specs=[smem] * scalars + [vmem]...]
  transfers between devices with their start and end apart: 16 -> 17, of which waited for: 10 -> 10; matrix products, arithmetic and copies ran while one was open for 5% -> 5% of each run, Pallas kernels for 7% -> 7%
where the time goes in v6:
time: 167 us; the launch traced here: 166 us
  starting transfers between devices  63.6 us (38%)
  waiting for transfers between devices  36.2 us (22%)
  blocking collectives  22.8 us (14%)
  Pallas kernels  16.8 us (10%)
  between operations  13.8 us (8%)
  local copies, waits for them, and re-layouts  8.11 us (5%)
  other arithmetic  4.26 us (3%)
    all_to_all x4, starting transfers between devices, swapped(): return lax.all_to_all(value, axes, split_axis=0, concat_axis=0, tiled=True)  23.1 us
    all_to_all x1, blocking collectives, swapped(): return lax.all_to_all(value, axes, split_axis=0, concat_axis=0, tiled=True)  22.8 us
    all_to_all x4, waiting for transfers between devices, swapped(): return lax.all_to_all(value, axes, split_axis=0, concat_axis=0, tiled=True)  21.6 us
    pallas_call x9, Pallas kernels, on_core(): pl.pallas_call(kernel, out_shape=out, in_specs=[smem] * scalars + [vmem]...  16.8 us
    ppermute x3, starting transfers between devices, body(): groups.append(lax.ppermute(group, 'sp_2', ring(2, 1)))  13.3 us
    ppermute x3, starting transfers between devices, body(): down = lax.ppermute(down, 'sp_1', ring(8, -1))  13 us
    ppermute x4, waiting for transfers between devices, body(): up = lax.ppermute(up, 'sp_1', ring(8, 1))  12.3 us
    ppermute x4, starting transfers between devices, body(): up = lax.ppermute(up, 'sp_1', ring(8, 1))  9.86 us
  transfers between devices with their start and end apart: 17, of which 10 were waited for; matrix products, arithmetic and copies ran while one was open for 5% of the time, Pallas kernels for 7%

profile of v6, /device:TPU:1, one launch (start us, length us, event | category | flops | bytes accessed | tf_op | source)
XLA Modules:
  0.0 166.3 jit_solution(1485123130724460571)
XLA Ops:
  8.1 10.9 %all-to-all-start = ((bf16[8,32,384]{2,1,0:T(8,128)(2,1)}), bf16[8,32,384]{2,1,0:T(8,128)(2,1)S(1)}, u32[]{:S(2)}, u32[]{:S(2)}) async-start(bf16[8,32,384]{2,1,0:T(8,128)(2,1)} %get-tuple-element.30), calls=%async_computation | async-start | bytes 393216 | tf_op jit(solution)/shard_map/all_to_all | solution.py:27
  19.8 2.2 %fusion = f32[256]{0:T(256)S(1)} fusion(bf16[256,4096]{1,0:T(8,128)(2,1)} %param.15), kind=kLoop, calls=%fused_computation.2 | loop fusion | flops 3145472 | bytes 2098176 | tf_op jit(solution)/shard_map/reduce_sum | solution.py:22
  25.0 3.0 %all-to-all-done = bf16[8,32,384]{2,1,0:T(8,128)(2,1)S(1)} async-done(((bf16[8,32,384]{2,1,0:T(8,128)(2,1)}), bf16[8,32,384]{2,1,0:T(8,128)(2,1)S(1)}, u32[]{:S(2)}, u32[]{:S(2)}) %all-to-all-start) | async-done | bytes 196640 | tf_op jit(solution)/shard_map/all_to_all | solution.py:27
  28.0 3.2 %collective-permute-start = (bf16[8,32,384]{2,1,0:T(8,128)(2,1)S(1)}, bf16[8,32,384]{2,1,0:T(8,128)(2,1)S(1)}, u32[]{:S(2)}, u32[]{:S(2)}) collective-permute-start(bf16[8,32,384]{2,1,0:T(8,128)(2,1)S(1)} %all-to-all-done), channel_id=1, source_target_pairs={{0,8},{8,16},{16,24},{24,32},{32,40},{40,48},{48,56},{56,0},{1,9},... | collective-permute-start | bytes 589832 | tf_op jit(solution)/shard_map/ppermute | solution.py:407
  31.2 3.8 %collective-permute-start.1 = (bf16[8,32,384]{2,1,0:T(8,128)(2,1)S(1)}, bf16[8,32,384]{2,1,0:T(8,128)(2,1)S(1)}, u32[]{:S(2)}, u32[]{:S(2)}) collective-permute-start(bf16[8,32,384]{2,1,0:T(8,128)(2,1)S(1)} %all-to-all-done), channel_id=1, source_target_pairs={{0,56},{8,0},{16,8},{24,16},{32,24},{40,32},{48,40},{56,48},{1,57}... | collective-permute-start | bytes 589832 | tf_op jit(solution)/shard_map/ppermute | solution.py:410
  38.6 4.6 %collective-permute-start.3 = (bf16[8,32,384]{2,1,0:T(8,128)(2,1)S(1)}, bf16[8,32,384]{2,1,0:T(8,128)(2,1)S(1)}, u32[]{:S(2)}, u32[]{:S(2)}) collective-permute-start(bf16[8,32,384]{2,1,0:T(8,128)(2,1)S(1)} %collective-permute-done.1), channel_id=1, source_target_pairs={{0,56},{8,0},{16,8},{24,16},{32,24},{40,32},{48,40},{56,48},{1,57}... | collective-permute-start | bytes 589832 | tf_op jit(solution)/shard_map/ppermute | solution.py:410
  46.5 4.6 %collective-permute-start.5 = (bf16[8,32,384]{2,1,0:T(8,128)(2,1)S(1)}, bf16[8,32,384]{2,1,0:T(8,128)(2,1)S(1)}, u32[]{:S(2)}, u32[]{:S(2)}) collective-permute-start(bf16[8,32,384]{2,1,0:T(8,128)(2,1)S(1)} %collective-permute-done.3), channel_id=1, source_target_pairs={{0,56},{8,0},{16,8},{24,16},{32,24},{40,32},{48,40},{56,48},{1,57}... | collective-permute-start | bytes 589832 | tf_op jit(solution)/shard_map/ppermute | solution.py:410
  54.0 7.1 %collective-permute-start.8 = (bf16[4,8,32,384]{3,2,1,0:T(8,128)(2,1)S(1)}, bf16[4,8,32,384]{3,2,1,0:T(8,128)(2,1)}, u32[]{:S(2)}, u32[]{:S(2)}) collective-permute-start(bf16[4,8,32,384]{3,2,1,0:T(8,128)(2,1)S(1)} %pad_maximum_fusion.refs_1_), channel_id=1, source_target_pairs={{0,4},{4,0},{1,5},{5,1},{2,6},{6,2},{3,7},{7,3},{8,12},{12,8},{9,1... | collective-permute-start | bytes 2359304 | tf_op jit(solution)/shard_map/ppermute | solution.py:417
  62.1 1.9 %collective-permute-start.7 = (bf16[3,8,32,384]{3,2,1,0:T(8,128)(2,1)S(1)}, bf16[3,8,32,384]{3,2,1,0:T(8,128)(2,1)}, u32[]{:S(2)}, u32[]{:S(2)}) collective-permute-start(bf16[3,8,32,384]{3,2,1,0:T(8,128)(2,1)S(1)} %pad_maximum_fusion.1.refs_0_), channel_id=1, source_target_pairs={{0,4},{4,0},{1,5},{5,1},{2,6},{6,2},{3,7},{7,3},{8,12},{12,8},{9,1... | collective-permute-start | bytes 1769480 | tf_op jit(solution)/shard_map/ppermute | solution.py:417
  64.0 2.8 %collective-permute-start.6 = (bf16[8,32,384]{2,1,0:T(8,128)(2,1)S(1)}, bf16[8,32,384]{2,1,0:T(8,128)(2,1)}, u32[]{:S(2)}, u32[]{:S(2)}) collective-permute-start(bf16[8,32,384]{2,1,0:T(8,128)(2,1)S(1)} %collective-permute-done.4), channel_id=1, source_target_pairs={{0,8},{8,16},{16,24},{24,32},{32,40},{40,48},{48,56},{56,0},{1,9},... | collective-permute-start | bytes 589832 | tf_op jit(solution)/shard_map/ppermute | solution.py:407
  66.9 7.4 %collective-permute-done.6 = bf16[8,32,384]{2,1,0:T(8,128)(2,1)} collective-permute-done((bf16[8,32,384]{2,1,0:T(8,128)(2,1)S(1)}, bf16[8,32,384]{2,1,0:T(8,128)(2,1)}, u32[]{:S(2)}, u32[]{:S(2)}) %collective-permute-start.6) | collective-permute-done | bytes 196640 | tf_op jit(solution)/shard_map/ppermute | solution.py:407
  74.3 4.3 %collective-permute-start.9 = (bf16[1,8,32,384]{3,2,1,0:T(8,128)(2,1)}, bf16[1,8,32,384]{3,2,1,0:T(8,128)(2,1)}, u32[]{:S(2)}, u32[]{:S(2)}) collective-permute-start(bf16[1,8,32,384]{3,2,1,0:T(8,128)(2,1)} %bitcast.14.refs_2_), channel_id=1, source_target_pairs={{0,4},{4,0},{1,5},{5,1},{2,6},{6,2},{3,7},{7,3},{8,12},{12,8},{9,1... | collective-permute-start | bytes 589832 | tf_op jit(solution)/shard_map/ppermute | solution.py:417
  81.0 3.2 %shard_map.147 = (bf16[16,48,128]{2,1,0:T(8,128)(2,1)S(1)}, bf16[256,128]{1,0:T(8,128)(2,1)S(1)}, bf16[256,256]{1,0:T(8,128)(2,1)S(1)}) custom-call(s32[2]{0:T(128)S(1)} %pad_add_fusion.place_ref, bf16[256,4096]{1,0:T(8,128)(2,1)S(1)} %fusion.2.normed_ref, f32[256,8]{1,0:T(8,128)S(1)} %copy-done.2, f32[4,128]{1,0:T(4,128)S(1)} %get-tuple-element.36.number_ref, ...), custom_call_target="tpu_custom_call" | custom-call | tf_op jit(solution)/shard_map/pallas_call | solution.py:329
  84.3 22.8 %all_to_all.25.state_ref = bf16[16,48,128]{2,1,0:T(8,128)(2,1)S(1)} all-to-all(bf16[16,48,128]{2,1,0:T(8,128)(2,1)S(1)} %get-tuple-element.43), channel_id=1, replica_groups=mesh['sp_0'=8,'sp_1'=8,'sp_2'=2,'tp'=4] {'sp_1','sp_2'}, dimensions={0} | all-to-all | bytes 393216 | tf_op jit(solution)/shard_map/all_to_all | solution.py:27
  107.9 3.4 %all-to-all-start.2 = ((bf16[8,48,128]{2,1,0:T(8,128)(2,1)}), bf16[8,48,128]{2,1,0:T(8,128)(2,1)S(1)}, u32[]{:S(2)}, u32[]{:S(2)}) async-start(bf16[8,48,128]{2,1,0:T(8,128)(2,1)} %get-tuple-element.45), calls=%async_computation.2 | async-start | bytes 196608 | tf_op jit(solution)/shard_map/all_to_all | solution.py:27
  113.2 2.4 %collective-permute-start.11 = (bf16[1,4096]{1,0:T(2,128)(2,1)S(1)}, bf16[1,4096]{1,0:T(2,128)(2,1)S(1)}, u32[]{:S(2)}, u32[]{:S(2)}) collective-permute-start(bf16[1,4096]{1,0:T(2,128)(2,1)S(1)} %get-tuple-element.40), channel_id=1, source_target_pairs={{4,0},{8,4},{12,8},{16,12},{20,16},{24,20},{28,24},{32,28},{36,32}... | collective-permute-start | bytes 24584 | tf_op jit(solution)/shard_map/ppermute | solution.py:34
  115.7 3.1 %all-to-all-done.2.planes_ref = bf16[8,48,128]{2,1,0:T(8,128)(2,1)S(1)} async-done(((bf16[8,48,128]{2,1,0:T(8,128)(2,1)}), bf16[8,48,128]{2,1,0:T(8,128)(2,1)S(1)}, u32[]{:S(2)}, u32[]{:S(2)}) %all-to-all-start.2) | async-done | bytes 98336 | tf_op jit(solution)/shard_map/all_to_all | solution.py:27
  119.8 4.9 %all-to-all-start.3 = ((bf16[16,48,128]{2,1,0:T(8,128)(2,1)}), bf16[16,48,128]{2,1,0:T(8,128)(2,1)S(1)}, u32[]{:S(2)}, u32[]{:S(2)}) async-start(bf16[16,48,128]{2,1,0:T(8,128)(2,1)} %shard_map.150), calls=%async_computation.3 | async-start | bytes 393216 | tf_op jit(solution)/shard_map/all_to_all | solution.py:27
  124.9 5.3 %shard_map.148 = (bf16[256,128]{1,0:T(8,128)(2,1)S(1)}, bf16[256,256]{1,0:T(8,128)(2,1)S(1)}) custom-call(bf16[256,4096]{1,0:T(8,128)(2,1)S(1)} %fusion.2.normed_ref, bf16[16,4096]{1,0:T(8,128)(2,1)S(1)} %maximum_maximum_fusion.edge_ref, bf16[3,256]{1,0:T(4,128)(2,1)S(1)} %copy-done.6, bf16[4096,1408]{1,0:T(8,128)(2,1)} %all-gather.2.cloned.1.call-done.whole_ref), custom_call_target="tpu_custom_call" | custom-call | tf_op jit(solution)/shard_map/pallas_call | solution.py:329
  130.8 4.2 %all-to-all-done.3.start_ref = bf16[16,48,128]{2,1,0:T(8,128)(2,1)S(1)} async-done(((bf16[16,48,128]{2,1,0:T(8,128)(2,1)}), bf16[16,48,128]{2,1,0:T(8,128)(2,1)S(1)}, u32[]{:S(2)}, u32[]{:S(2)}) %all-to-all-start.3) | async-done | bytes 196640 | tf_op jit(solution)/shard_map/all_to_all | solution.py:27
  136.6 4.0 %all-to-all-start.4 = ((bf16[4,256,512]{2,1,0:T(8,128)(2,1)}), bf16[4,256,512]{2,1,0:T(8,128)(2,1)S(1)}, u32[]{:S(2)}, u32[]{:S(2)}) async-start(bf16[4,256,512]{2,1,0:T(8,128)(2,1)} %shard_map.152), calls=%async_computation.4 | async-start | bytes 2097152 | tf_op jit(solution)/shard_map/all_to_all | solution.py:27
  140.6 2.2 %slice-done = bf16[4096,512]{1,0:T(8,128)(2,1)S(1)} async-done(((bf16[4096,1408]{1,0:T(8,128)(2,1)}), bf16[4096,512]{1,0:T(8,128)(2,1)S(1)}, s32[]{:S(2)}) %slice-start) | async-done | bytes 4194328 | tf_op jit(solution)/shard_map/slice | solution.py:493
  144.6 11.2 %all-to-all-done.4.joined_ref = bf16[4,256,512]{2,1,0:T(8,128)(2,1)S(1)} async-done(((bf16[4,256,512]{2,1,0:T(8,128)(2,1)}), bf16[4,256,512]{2,1,0:T(8,128)(2,1)S(1)}, u32[]{:S(2)}, u32[]{:S(2)}) %all-to-all-start.4) | async-done | bytes 1048608 | tf_op jit(solution)/shard_map/all_to_all | solution.py:27
  157.4 2.0 %shard_map.153 = bf16[256,1024]{1,0:T(8,128)(2,1)} custom-call(bf16[4,256,512]{2,1,0:T(8,128)(2,1)S(1)} %all-to-all-done.4.joined_ref, bf16[4,512,512]{2,1,0:T(8,128)(2,1)S(1)} %bitcast.42, bf16[4,512,512]{2,1,0:T(8,128)(2,1)S(1)} %bitcast.41), custom_call_target="tpu_custom_call" | custom-call | tf_op jit(solution)/shard_map/pallas_call | solution.py:329
  (67 shorter events, 27.9 us)
Async XLA Ops:
  6.5 15.5 %copy-start.10 = (f32[4096]{0:T(1024)S(1)}, f32[4096]{0:T(1024)}, u32[]{:S(2)}) copy-start(f32[4096]{0:T(1024)} %param.16) | copy-start | bytes 49156
  6.5 118.4 %all-gather.2.cloned.1.call-start = ((), (), s32[]{:S(2)}) async-start(), calls=%async_computation.5 | async-start | bytes 11624448 | tf_op jit(solution)/shard_map/all_gather | solution.py:381
  8.1 19.9 %all-to-all-start = ((bf16[8,32,384]{2,1,0:T(8,128)(2,1)}), bf16[8,32,384]{2,1,0:T(8,128)(2,1)S(1)}, u32[]{:S(2)}, u32[]{:S(2)}) async-start(bf16[8,32,384]{2,1,0:T(8,128)(2,1)} %get-tuple-element.30), calls=%async_computation | async-start | bytes 393216 | tf_op jit(solution)/shard_map/all_to_all | solution.py:27
  28.0 33.1 %copy-start.9 = (bf16[8,32,384]{2,1,0:T(8,128)(2,1)}, bf16[8,32,384]{2,1,0:T(8,128)(2,1)S(1)}, u32[]{:S(2)}) copy-start(bf16[8,32,384]{2,1,0:T(8,128)(2,1)S(1)} %all-to-all-done) | copy-start | bytes 589828
  28.0 8.6 %collective-permute-start = (bf16[8,32,384]{2,1,0:T(8,128)(2,1)S(1)}, bf16[8,32,384]{2,1,0:T(8,128)(2,1)S(1)}, u32[]{:S(2)}, u32[]{:S(2)}) collective-permute-start(bf16[8,32,384]{2,1,0:T(8,128)(2,1)S(1)} %all-to-all-done), channel_id=1, source_target_pairs={{0,8},{8,16},{16,24},{24,32},{32,40},{40,48},{48,56},{56,0},{1,9},... | collective-permute-start | bytes 589832 | tf_op jit(solution)/shard_map/ppermute | solution.py:407
  31.2 7.3 %collective-permute-start.1 = (bf16[8,32,384]{2,1,0:T(8,128)(2,1)S(1)}, bf16[8,32,384]{2,1,0:T(8,128)(2,1)S(1)}, u32[]{:S(2)}, u32[]{:S(2)}) collective-permute-start(bf16[8,32,384]{2,1,0:T(8,128)(2,1)S(1)} %all-to-all-done), channel_id=1, source_target_pairs={{0,56},{8,0},{16,8},{24,16},{32,24},{40,32},{48,40},{56,48},{1,57}... | collective-permute-start | bytes 589832 | tf_op jit(solution)/shard_map/ppermute | solution.py:410
  36.6 7.9 %collective-permute-start.2 = (bf16[8,32,384]{2,1,0:T(8,128)(2,1)S(1)}, bf16[8,32,384]{2,1,0:T(8,128)(2,1)S(1)}, u32[]{:S(2)}, u32[]{:S(2)}) collective-permute-start(bf16[8,32,384]{2,1,0:T(8,128)(2,1)S(1)} %collective-permute-done), channel_id=1, source_target_pairs={{0,8},{8,16},{16,24},{24,32},{32,40},{40,48},{48,56},{56,0},{1,9},... | collective-permute-start | bytes 589832 | tf_op jit(solution)/shard_map/ppermute | solution.py:407
  38.6 7.9 %collective-permute-start.3 = (bf16[8,32,384]{2,1,0:T(8,128)(2,1)S(1)}, bf16[8,32,384]{2,1,0:T(8,128)(2,1)S(1)}, u32[]{:S(2)}, u32[]{:S(2)}) collective-permute-start(bf16[8,32,384]{2,1,0:T(8,128)(2,1)S(1)} %collective-permute-done.1), channel_id=1, source_target_pairs={{0,56},{8,0},{16,8},{24,16},{32,24},{40,32},{48,40},{56,48},{1,57}... | collective-permute-start | bytes 589832 | tf_op jit(solution)/shard_map/ppermute | solution.py:410
  44.5 8.4 %collective-permute-start.4 = (bf16[8,32,384]{2,1,0:T(8,128)(2,1)S(1)}, bf16[8,32,384]{2,1,0:T(8,128)(2,1)S(1)}, u32[]{:S(2)}, u32[]{:S(2)}) collective-permute-start(bf16[8,32,384]{2,1,0:T(8,128)(2,1)S(1)} %collective-permute-done.2), channel_id=1, source_target_pairs={{0,8},{8,16},{16,24},{24,32},{32,40},{40,48},{48,56},{56,0},{1,9},... | collective-permute-start | bytes 589832 | tf_op jit(solution)/shard_map/ppermute | solution.py:407
  46.5 7.4 %collective-permute-start.5 = (bf16[8,32,384]{2,1,0:T(8,128)(2,1)S(1)}, bf16[8,32,384]{2,1,0:T(8,128)(2,1)S(1)}, u32[]{:S(2)}, u32[]{:S(2)}) collective-permute-start(bf16[8,32,384]{2,1,0:T(8,128)(2,1)S(1)} %collective-permute-done.3), channel_id=1, source_target_pairs={{0,56},{8,0},{16,8},{24,16},{32,24},{40,32},{48,40},{56,48},{1,57}... | collective-permute-start | bytes 589832 | tf_op jit(solution)/shard_map/ppermute | solution.py:410
  54.0 26.1 %collective-permute-start.8 = (bf16[4,8,32,384]{3,2,1,0:T(8,128)(2,1)S(1)}, bf16[4,8,32,384]{3,2,1,0:T(8,128)(2,1)}, u32[]{:S(2)}, u32[]{:S(2)}) collective-permute-start(bf16[4,8,32,384]{3,2,1,0:T(8,128)(2,1)S(1)} %pad_maximum_fusion.refs_1_), channel_id=1, source_target_pairs={{0,4},{4,0},{1,5},{5,1},{2,6},{6,2},{3,7},{7,3},{8,12},{12,8},{9,1... | collective-permute-start | bytes 2359304 | tf_op jit(solution)/shard_map/ppermute | solution.py:417
  62.1 16.6 %collective-permute-start.7 = (bf16[3,8,32,384]{3,2,1,0:T(8,128)(2,1)S(1)}, bf16[3,8,32,384]{3,2,1,0:T(8,128)(2,1)}, u32[]{:S(2)}, u32[]{:S(2)}) collective-permute-start(bf16[3,8,32,384]{3,2,1,0:T(8,128)(2,1)S(1)} %pad_maximum_fusion.1.refs_0_), channel_id=1, source_target_pairs={{0,4},{4,0},{1,5},{5,1},{2,6},{6,2},{3,7},{7,3},{8,12},{12,8},{9,1... | collective-permute-start | bytes 1769480 | tf_op jit(solution)/shard_map/ppermute | solution.py:417
  64.0 10.3 %collective-permute-start.6 = (bf16[8,32,384]{2,1,0:T(8,128)(2,1)S(1)}, bf16[8,32,384]{2,1,0:T(8,128)(2,1)}, u32[]{:S(2)}, u32[]{:S(2)}) collective-permute-start(bf16[8,32,384]{2,1,0:T(8,128)(2,1)S(1)} %collective-permute-done.4), channel_id=1, source_target_pairs={{0,8},{8,16},{16,24},{24,32},{32,40},{40,48},{48,56},{56,0},{1,9},... | collective-permute-start | bytes 589832 | tf_op jit(solution)/shard_map/ppermute | solution.py:407
  74.3 5.8 %collective-permute-start.9 = (bf16[1,8,32,384]{3,2,1,0:T(8,128)(2,1)}, bf16[1,8,32,384]{3,2,1,0:T(8,128)(2,1)}, u32[]{:S(2)}, u32[]{:S(2)}) collective-permute-start(bf16[1,8,32,384]{3,2,1,0:T(8,128)(2,1)} %bitcast.14.refs_2_), channel_id=1, source_target_pairs={{0,4},{4,0},{1,5},{5,1},{2,6},{6,2},{3,7},{7,3},{8,12},{12,8},{9,1... | collective-permute-start | bytes 589832 | tf_op jit(solution)/shard_map/ppermute | solution.py:417
  84.2 23.7 %copy-start.4 = (bf16[256,256]{1,0:T(8,128)(2,1)}, bf16[256,256]{1,0:T(8,128)(2,1)S(1)}, u32[]{:S(2)}) copy-start(bf16[256,256]{1,0:T(8,128)(2,1)S(1)} %get-tuple-element.47.value_ref) | copy-start | bytes 393220
  84.2 40.7 %copy-start.6 = (bf16[3,256]{1,0:T(4,128)(2,1)S(1)}, bf16[3,256]{1,0:T(4,128)(2,1)}, u32[]{:S(2)}) copy-start(bf16[3,256]{1,0:T(4,128)(2,1)} %tap_ref.1) | copy-start | bytes 4612
  107.9 11.0 %all-to-all-start.2 = ((bf16[8,48,128]{2,1,0:T(8,128)(2,1)}), bf16[8,48,128]{2,1,0:T(8,128)(2,1)S(1)}, u32[]{:S(2)}, u32[]{:S(2)}) async-start(bf16[8,48,128]{2,1,0:T(8,128)(2,1)} %get-tuple-element.45), calls=%async_computation.2 | async-start | bytes 196608 | tf_op jit(solution)/shard_map/all_to_all | solution.py:27
  111.3 13.4 %collective-permute-start.10 = (bf16[1,4096]{1,0:T(2,128)(2,1)S(1)}, bf16[1,4096]{1,0:T(2,128)(2,1)S(1)}, u32[]{:S(2)}, u32[]{:S(2)}) collective-permute-start(bf16[1,4096]{1,0:T(2,128)(2,1)S(1)} %get-tuple-element.39), channel_id=1, source_target_pairs={{0,4},{4,8},{8,12},{12,16},{16,20},{20,24},{24,28},{28,32},{32,36}... | collective-permute-start | bytes 24584 | tf_op jit(solution)/shard_map/ppermute | solution.py:33
  113.2 11.5 %collective-permute-start.11 = (bf16[1,4096]{1,0:T(2,128)(2,1)S(1)}, bf16[1,4096]{1,0:T(2,128)(2,1)S(1)}, u32[]{:S(2)}, u32[]{:S(2)}) collective-permute-start(bf16[1,4096]{1,0:T(2,128)(2,1)S(1)} %get-tuple-element.40), channel_id=1, source_target_pairs={{4,0},{8,4},{12,8},{16,12},{20,16},{24,20},{28,24},{32,28},{36,32}... | collective-permute-start | bytes 24584 | tf_op jit(solution)/shard_map/ppermute | solution.py:34
  119.8 15.2 %all-to-all-start.3 = ((bf16[16,48,128]{2,1,0:T(8,128)(2,1)}), bf16[16,48,128]{2,1,0:T(8,128)(2,1)S(1)}, u32[]{:S(2)}, u32[]{:S(2)}) async-start(bf16[16,48,128]{2,1,0:T(8,128)(2,1)} %shard_map.150), calls=%async_computation.3 | async-start | bytes 393216 | tf_op jit(solution)/shard_map/all_to_all | solution.py:27
  124.8 5.3 %copy-start.3 = (f32[256,8]{1,0:T(8,128)S(1)}, f32[256,8]{1,0:T(8,128)}, u32[]{:S(2)}) copy-start(f32[256,8]{1,0:T(8,128)} %copy-done.1) | copy-start | bytes 24580
  124.8 5.3 %copy-start.5 = (bf16[256,256]{1,0:T(8,128)(2,1)S(1)}, bf16[256,256]{1,0:T(8,128)(2,1)}, u32[]{:S(2)}) copy-start(bf16[256,256]{1,0:T(8,128)(2,1)} %copy-done.4) | copy-start | bytes 393220
  124.9 10.1 %copy-start.7 = (f32[256]{0:T(256)S(1)}, f32[256]{0:T(256)}, u32[]{:S(2)}) copy-start(f32[256]{0:T(256)} %param.24) | copy-start | bytes 3076
  136.6 19.2 %all-to-all-start.4 = ((bf16[4,256,512]{2,1,0:T(8,128)(2,1)}), bf16[4,256,512]{2,1,0:T(8,128)(2,1)S(1)}, u32[]{:S(2)}, u32[]{:S(2)}) async-start(bf16[4,256,512]{2,1,0:T(8,128)(2,1)} %shard_map.152), calls=%async_computation.4 | async-start | bytes 2097152 | tf_op jit(solution)/shard_map/all_to_all | solution.py:27
  (8 other events, 9.8 us)
Sparse Core Ops, SparseCore 0:
  10.5 100.5 all-gather.1
